TPU v7x, 32 devices: a whole 2x2x4 slice. The times are simulated.
32 devices in a mesh: ep: 8 (over z, core), tp: 4 (over y, x).
Axes of the slice: x: 2, y: 2, z: 4, core: 2. Of those that a mesh axis runs over, the one named last changes fastest.
Arguments:
- tokens: bfloat16 [256, 2048], P('ep'), may hold values from -6 to 6
- recurrent_head_state: float32 [256, 16, 4096], P('ep', 'tp'), may hold values from -4 to 4
- first_norm_gain: float32 [2048], replicated, may hold values from 0.1 to 1.9
- receptance_matrix: bfloat16 [2048, 1024], P(None, 'tp'), may hold values from -0.125 to 0.125
- key_matrix: bfloat16 [2048, 1024], P(None, 'tp'), may hold values from -0.125 to 0.125
- value_matrix: bfloat16 [2048, 1024], P(None, 'tp'), may hold values from -0.125 to 0.125
- decay_matrix: bfloat16 [2048, 1024], P(None, 'tp'), may hold values from -0.125 to 0.125
- decay_offset: float32 [1024], P('tp'), may hold values from -3 to 0.5
- correction_offset: float32 [1024], P('tp'), may hold values from -2 to 2
- correction_key_factor: float32 [1024], P('tp'), may hold values from -1 to 1
- own_term_weight: float32 [1024], P('tp'), may hold values from -0.9 to 0.9
- head_norm_gain: float32 [1024], P('tp'), may hold values from 0.1 to 1.9
- output_matrix: bfloat16 [1024, 2048], P('tp'), may hold values from -0.1875 to 0.1875
- second_norm_gain: float32 [2048], replicated, may hold values from 0.1 to 1.9
- routing: int32 [256, 2], replicated, may hold values from 0 to 7, all different within a row; in each aligned block of 32 rows (0 to 31, 32 to 63, ...) at most 16 rows name the same one
- routing_weight: float32 [256, 2], P('ep'), may hold values from 0.1 to 1
- expert_gate_weight: bfloat16 [8, 2048, 4096], P('ep', None, 'tp'), may hold values from -0.125 to 0.125
- expert_up_weight: bfloat16 [8, 2048, 4096], P('ep', None, 'tp'), may hold values from -0.125 to 0.125
- expert_down_weight: bfloat16 [8, 4096, 2048], P('ep', 'tp'), may hold values from -0.125 to 0.125
- dense_gate_weight: bfloat16 [2048, 2816], P(None, 'ep'), may hold values from -0.125 to 0.125
- dense_up_weight: bfloat16 [2048, 2816], P(None, 'ep'), may hold values from -0.125 to 0.125
- dense_down_weight: bfloat16 [2816, 2048], P('ep'), may hold values from -0.109375 to 0.109375
- dense_gate_offset: float32 [2048], replicated, may hold values from -3 to 3
Outputs:
- layer_out: bfloat16 [256, 2048], P(('ep', 'tp'))
- next_state: float32 [256, 16, 4096], P('ep', 'tp')
Inputs may be any that keep to these rules, and one draw needn't show every extreme that they name: `routing`: each row names 2 different experts. In each aligned block of 32 rows no expert is named more than 16 times, a bound that some block reaches.
All inputs are finite; a program needn't handle non-finite values.
Results may differ from a plain program's by a relative error of at most 0.017.
Values may be sent and summed in bfloat16 or wider, within the bound.
No kernel may reach another device: no remote copies, remote signals or barrier semaphores. Data moves between devices by JAX's collectives and lax.ppermute only.
A program may use at most 64 MiB of HBM per device.

v0:
```python
import jax
import jax.numpy as jnp
from jax import lax
from jax.sharding import PartitionSpec as P

HEAD_WIDTH = 64


PRECISE = lax.Precision.HIGHEST


def rms_scale(rows, gain):
    floats = rows.astype(jnp.float32)
    return floats * lax.rsqrt(jnp.mean(floats * floats, axis=-1, keepdims=True) + 1e-06) * gain


def route_table(block_routes, experts, capacity):
    flat_routes = block_routes.reshape(-1)
    chosen = (flat_routes[:, None] == jnp.arange(experts, dtype=jnp.int32)[None, :]).astype(
        jnp.int32
    )
    before = jnp.cumsum(chosen, axis=0, dtype=jnp.int32) - chosen
    slot_index = jnp.sum(before * chosen, axis=1)
    slot_match = (slot_index[:, None] == jnp.arange(capacity, dtype=jnp.int32)[None, :]).astype(
        jnp.float32
    )
    dispatch_table = chosen.astype(jnp.float32)[:, :, None] * slot_match[:, None, :]
    return dispatch_table.reshape(block_routes.shape[0], block_routes.shape[1], experts, capacity)


def state_update(
    receptance_rows,
    key_matrix_rows,
    value_matrix_rows,
    decay_logits,
    recurrent_head_state,
    decay_offset,
    correction_offset,
    correction_key_factor,
    own_term_weight,
    head_norm_gain,
    head_width,
):
    seq_count = key_matrix_rows.shape[0]
    decay_factor = jnp.exp(-jnp.exp(decay_offset + decay_logits))
    in_rate = jax.nn.sigmoid(correction_offset + correction_key_factor * key_matrix_rows)
    key_in = key_matrix_rows * in_rate

    def split_heads(block):
        return block.reshape(seq_count, -1, head_width)

    keys_head = split_heads(key_matrix_rows)
    unit_keys = (
        keys_head
        * lax.rsqrt(jnp.mean(keys_head * keys_head, axis=-1, keepdims=True) + 1e-06)
        * head_width ** (-0.5)
    )
    rate_head = split_heads(in_rate)
    head_keys = split_heads(key_in)
    decay_head = split_heads(decay_factor)
    head_values = split_heads(value_matrix_rows)
    head_receptance = split_heads(receptance_rows)
    matrix = recurrent_head_state.reshape(seq_count, -1, head_width, head_width)
    removed = jnp.einsum("bhvk,bhk->bhv", matrix, unit_keys, precision=PRECISE)
    updated = (
        matrix * decay_head[:, :, None, :]
        - removed[..., None] * (unit_keys * rate_head)[:, :, None, :]
        + head_values[..., None] * head_keys[:, :, None, :]
    )
    readout = jnp.einsum("bhvk,bhk->bhv", updated, head_receptance, precision=PRECISE)
    center = jnp.mean(readout, axis=-1, keepdims=True)
    spread = jnp.mean(jnp.square(readout - center), axis=-1, keepdims=True)
    normalized_rows = (
        (readout - center) * lax.rsqrt(spread + 0.00064) * head_norm_gain.reshape(-1, head_width)
    )
    own_term_total = jnp.sum(
        head_receptance * head_keys * own_term_weight.reshape(-1, head_width),
        axis=-1,
        keepdims=True,
    )
    normalized_rows = normalized_rows + own_term_total * head_values
    return (
        normalized_rows.reshape(seq_count, -1).astype(jnp.bfloat16),
        updated.reshape(seq_count, -1, head_width * head_width),
    )


def local(
    tokens,
    recurrent_head_state,
    first_norm_gain,
    receptance_matrix,
    key_matrix,
    value_matrix,
    decay_matrix,
    decay_offset,
    correction_offset,
    correction_key_factor,
    own_term_weight,
    head_norm_gain,
    output_matrix,
    second_norm_gain,
    routing,
    routing_weight,
    expert_gate_weight,
    expert_up_weight,
    expert_down_weight,
    dense_gate_weight,
    dense_up_weight,
    dense_down_weight,
    dense_gate_offset,
):
    seq_count = tokens.shape[0]
    width = tokens.shape[1]
    group_index = lax.axis_index("ep")
    lane_index = lax.axis_index("tp")
    group_count = lax.axis_size("ep")
    lane_count = lax.axis_size("tp")
    normalized_rows = rms_scale(tokens, first_norm_gain).astype(jnp.bfloat16)
    receptance_rows = jnp.dot(
        normalized_rows, receptance_matrix, preferred_element_type=jnp.float32
    )
    key_matrix_rows = jnp.dot(normalized_rows, key_matrix, preferred_element_type=jnp.float32)
    value_matrix_rows = jnp.dot(normalized_rows, value_matrix, preferred_element_type=jnp.float32)
    decay_logits = jnp.dot(normalized_rows, decay_matrix, preferred_element_type=jnp.float32)
    head_outputs, next_state = state_update(
        receptance_rows,
        key_matrix_rows,
        value_matrix_rows,
        decay_logits,
        recurrent_head_state,
        decay_offset,
        correction_offset,
        correction_key_factor,
        own_term_weight,
        head_norm_gain,
        HEAD_WIDTH,
    )
    partial_out = jnp.dot(head_outputs, output_matrix, preferred_element_type=jnp.float32)
    hidden_sum = tokens.astype(jnp.float32) + lax.psum(
        partial_out.astype(jnp.bfloat16), "tp"
    ).astype(jnp.float32)
    ffn_in = rms_scale(hidden_sum, second_norm_gain).astype(jnp.bfloat16)
    local_experts = expert_gate_weight.shape[0]
    top_count = routing.shape[1]
    expert_count = local_experts * group_count
    capacity = 2 * seq_count * top_count // expert_count
    per_lane = seq_count // lane_count
    own_routes = lax.dynamic_slice_in_dim(routing, group_index * seq_count, seq_count, 0)
    own_table = route_table(own_routes, expert_count, capacity)
    send_rows = jnp.einsum(
        "bkec,bd->ecd", own_table.astype(jnp.bfloat16), ffn_in, preferred_element_type=jnp.float32
    ).astype(jnp.bfloat16)
    lane_rows = lax.dynamic_slice_in_dim(ffn_in, lane_index * per_lane, per_lane, 0)
    dense_send = jnp.broadcast_to(lane_rows[None], (group_count, per_lane, width))
    expert_in, dense_in = (
        lax.all_to_all(send_rows, "ep", split_axis=0, concat_axis=0, tiled=True),
        lax.all_to_all(dense_send, "ep", split_axis=0, concat_axis=0, tiled=True),
    )
    rows_in = expert_in.reshape(group_count, local_experts, capacity, width).transpose(1, 0, 2, 3)
    rows_in = rows_in.reshape(local_experts, group_count * capacity, width)
    gate_pre = jnp.einsum(
        "lrd,ldf->lrf", rows_in, expert_gate_weight, preferred_element_type=jnp.float32
    )
    up_pre = jnp.einsum(
        "lrd,ldf->lrf", rows_in, expert_up_weight, preferred_element_type=jnp.float32
    )
    expert_hidden = (jax.nn.silu(gate_pre) * up_pre).astype(jnp.bfloat16)
    expert_part = jnp.einsum(
        "lrf,lfd->lrd", expert_hidden, expert_down_weight, preferred_element_type=jnp.float32
    )
    expert_out = lax.psum_scatter(
        expert_part.astype(jnp.bfloat16), "tp", scatter_dimension=2, tiled=True
    )
    back_send = expert_out.reshape(local_experts, group_count, capacity, -1).transpose(1, 0, 2, 3)
    back_send = back_send.reshape(group_count * local_experts, capacity, -1)
    dense_rows = dense_in.reshape(group_count * per_lane, width)
    dense_hidden = (
        jax.nn.silu(jnp.dot(dense_rows, dense_gate_weight, preferred_element_type=jnp.float32))
        * jnp.dot(dense_rows, dense_up_weight, preferred_element_type=jnp.float32)
    ).astype(jnp.bfloat16)
    dense_part = jnp.dot(
        dense_hidden, dense_down_weight, preferred_element_type=jnp.float32
    ).astype(jnp.bfloat16)
    dense_part = dense_part.reshape(group_count, per_lane, width)
    back_experts, back_dense = (
        lax.all_to_all(back_send, "ep", split_axis=0, concat_axis=0, tiled=True),
        lax.all_to_all(dense_part, "ep", split_axis=0, concat_axis=0, tiled=True),
    )
    dense_sum = jnp.sum(back_dense.astype(jnp.float32), axis=0)
    weighted = jnp.einsum("bkec,bk->ecb", own_table, routing_weight, precision=PRECISE)
    moe_slice = jnp.einsum(
        "ecb,ecd->bd", weighted, back_experts.astype(jnp.float32), precision=PRECISE
    )
    moe_rows = lax.all_to_all(moe_slice, "tp", split_axis=0, concat_axis=1, tiled=True)
    residual_rows = lax.dynamic_slice_in_dim(hidden_sum, lane_index * per_lane, per_lane, 0)
    layer_out = (residual_rows + moe_rows + jax.nn.sigmoid(dense_gate_offset) * dense_sum).astype(
        jnp.bfloat16
    )
    return (layer_out, next_state)


def solution(mesh):
    return jax.shard_map(
        local,
        mesh=mesh,
        in_specs=(
            P("ep", None),
            P("ep", "tp", None),
            P(),
            P(None, "tp"),
            P(None, "tp"),
            P(None, "tp"),
            P(None, "tp"),
            P("tp"),
            P("tp"),
            P("tp"),
            P("tp"),
            P("tp"),
            P("tp", None),
            P(),
            P(),
            P("ep", None),
            P("ep", None, "tp"),
            P("ep", None, "tp"),
            P("ep", "tp", None),
            P(None, "ep"),
            P(None, "ep"),
            P("ep", None),
            P(),
        ),
        out_specs=(P(("ep", "tp"), None), P("ep", "tp", None)),
        check_vma=False,
    )
```

profile of v0, /device:TPU:0, one launch (start us, length us, event | category | flops | bytes accessed | tf_op | source)
XLA Modules:
  0.0 217.0 jit_solution(15776234293525649654)
XLA Ops:
  31.4 3.3 %reshape.173 = f32[32,4,64,64]{3,2,1,0:T(8,128)} reshape(f32[32,4,4096]{2,1,0:T(4,128)S(1)} %copy-done.2) | data formatting | bytes 4194304 | tf_op jit(solution)/shard_map/reshape | solution.py:63
  35.9 8.6 %fusion.70 = f32[32,4,1,64]{3,2,1,0:T(1,128)S(1)} fusion(f32[32,4,64,1]{2,3,1,0:T(1,128)S(1)} %bitcast.86, f32[32,4,64,64]{3,2,1,0:T(8,128)} %reshape.173), kind=kOutput, calls=%fused_computation.92 | convolution fusion | flops 6291456 | bytes 2162688 | tf_op jit(solution)/shard_map/bhvk,bhk->bhv/dot_general | solution.py:64
  44.5 9.0 %fusion.7 = f32[32,4,1,64]{3,2,1,0:T(1,128)} fusion(f32[32,4,64,1]{2,3,1,0:T(1,128)S(1)} %bitcast.92, f32[32,4,64,64]{3,2,1,0:T(8,128)S(1)} %copy-done.1, f32[32,4,64]{2,1,0:T(4,128)S(1)} %copy-done.6, f32[32,4,64]{2,1,0:T(4,128)S(1)} %get-tuple-element.4, f32[32,4,64]{2,1,0:T(4,128)S(1)} %bitcast.84, f32[32,4,64]{2,1,0:T(4,128)S(1)} %copy-done.8, ...), kind=kOutput, calls=%fused_computation.7 | convolution fusion | flops 8912896 | bytes 2326528 | tf_op jit(solution)/shard_map/bhvk,bhk->bhv/dot_general | solution.py:70
  71.6 34.1 %all-reduce.2.cloned.1.call-done = bf16[32,2048]{1,0:T(8,128)(2,1)} async-done(((bf16[32,2048]{1,0:T(8,128)(2,1)}), bf16[32,2048]{1,0:T(8,128)(2,1)}) %all-reduce.2.cloned.1.call-update) | async-done | bytes 131088 | tf_op jit(solution)/shard_map/psum | solution.py:140
  111.1 4.6 %all-to-all-start = ((bf16[8,16,2048]{2,1,0:T(8,128)(2,1)}), bf16[8,16,2048]{2,1,0:T(8,128)(2,1)}, u32[]{:S(2)}, u32[]{:S(2)}) async-start(bf16[8,16,2048]{2,1,0:T(8,128)(2,1)} %convolution_convert_fusion), calls=%async_computation | async-start | bytes 1048576 | tf_op jit(solution)/shard_map/all_to_all | solution.py:157
  115.8 15.4 %all-to-all-done = bf16[8,16,2048]{2,1,0:T(8,128)(2,1)} async-done(((bf16[8,16,2048]{2,1,0:T(8,128)(2,1)}), bf16[8,16,2048]{2,1,0:T(8,128)(2,1)}, u32[]{:S(2)}, u32[]{:S(2)}) %all-to-all-start) | async-done | bytes 524320 | tf_op jit(solution)/shard_map/all_to_all | solution.py:157
  131.2 3.9 %fusion.5 = f32[128,1024]{1,0:T(8,128)} fusion(bf16[128,2048]{1,0:T(8,128)(2,1)} %bitcast.9, bf16[1,2048,1024]{2,1,0:T(8,128)(2,1)} %param.39), kind=kOutput, calls=%fused_computation.5 | convolution fusion | flops 536870912 | bytes 5242880 | tf_op jit(solution)/shard_map/lrd,ldf->lrf/dot_general | solution.py:162
  135.0 6.0 %fusion.14 = bf16[1,128,2048]{2,1,0:T(8,128)(2,1)} fusion(bf16[1,1024,2048]{2,1,0:T(8,128)(2,1)} %param.41, bf16[128,2048]{1,0:T(8,128)(2,1)} %bitcast.9, bf16[1,2048,1024]{2,1,0:T(8,128)(2,1)} %param.40, f32[128,1024]{1,0:T(8,128)} %fusion.5), kind=kOutput, calls=%fused_computation.13 | convolution fusion | flops 1074790400 | bytes 9961472 | tf_op jit(solution)/shard_map/lrf,lfd->lrd/dot_general | solution.py:169
  142.5 4.2 %all-to-all-start.3 = ((bf16[8,8,2048]{2,1,0:T(8,128)(2,1)}), bf16[8,8,2048]{2,1,0:T(8,128)(2,1)}, u32[]{:S(2)}, u32[]{:S(2)}) async-start(bf16[8,8,2048]{2,1,0:T(8,128)(2,1)} %broadcast_in_dim.2), calls=%async_computation.4 | async-start | bytes 524288 | tf_op jit(solution)/shard_map/all_to_all | solution.py:158
  146.8 3.8 %broadcast_multiply_fusion = f32[32,4,64,64]{3,2,1,0:T(8,128)} fusion(f32[32,4,64]{2,1,0:T(4,128)} %mul.243, f32[32,4,64]{2,1,0:T(4,128)} %mul.240), kind=kLoop, calls=%fused_computation.18 | loop fusion | flops 524288 | bytes 2162688 | tf_op jit(solution)/shard_map/mul | solution.py:68
  150.6 5.1 %mul.277 = f32[32,4,4096]{2,1,0:T(4,128)} reshape(f32[32,4,64,64]{3,2,1,0:T(8,128)} %broadcast_multiply_fusion) | data formatting | bytes 4194304 | tf_op jit(solution)/shard_map/mul | solution.py:68
  155.6 3.8 %broadcast_multiply_fusion.1 = f32[32,4,64,64]{3,2,1,0:T(8,128)} fusion(f32[32,4,64]{2,1,0:T(4,128)} %copy-done.5, f32[32,4,64]{2,1,0:T(4,128)} %bitcast.85), kind=kLoop, calls=%fused_computation.19 | loop fusion | flops 524288 | bytes 2162688 | tf_op jit(solution)/shard_map/mul | solution.py:67
  159.4 5.0 %mul.276 = f32[32,4,4096]{2,1,0:T(4,128)} reshape(f32[32,4,64,64]{3,2,1,0:T(8,128)} %broadcast_multiply_fusion.1) | data formatting | bytes 4194304 | tf_op jit(solution)/shard_map/mul | solution.py:67
  164.5 3.0 %mul.227 = f32[32,4,64,64]{3,2,1,0:T(8,128)} broadcast(f32[32,4,64]{2,1,0:T(4,128)} %mul.226), dimensions={0,1,3} | broadcast | bytes 2129920 | tf_op jit(solution)/shard_map/mul | solution.py:66
  167.5 5.0 %mul.274 = f32[32,4,4096]{2,1,0:T(4,128)} reshape(f32[32,4,64,64]{3,2,1,0:T(8,128)} %mul.227) | data formatting | bytes 4194304 | tf_op jit(solution)/shard_map/mul | solution.py:66
  172.5 2.6 %fusion.44 = f32[64,352]{1,0:T(8,128)} fusion(bf16[2048,352]{0,1:T(8,128)(2,1)} %param.42, bf16[8,8,2048]{2,1,0:T(8,128)(2,1)} %all-to-all-done.3), kind=kOutput, calls=%fused_computation.46 | convolution fusion | flops 92274688 | bytes 1794048 | tf_op jit(solution)/shard_map/dot_general | solution.py:179
  175.2 4.8 %all-to-all-start.1 = ((bf16[8,16,512]{2,1,0:T(8,128)(2,1)}), bf16[8,16,512]{2,1,0:T(8,128)(2,1)}, u32[]{:S(2)}, u32[]{:S(2)}) async-start(bf16[8,16,512]{2,1,0:T(8,128)(2,1)} %bitcast.91), calls=%async_computation.2 | async-start | bytes 262144 | tf_op jit(solution)/shard_map/all_to_all | solution.py:187
  180.0 3.3 %fusion.17 = bf16[8,8,2048]{2,1,0:T(8,128)(2,1)} fusion(bf16[352,2048]{1,0:T(8,128)(2,1)S(1)} %copy-done, bf16[2048,352]{0,1:T(8,128)(2,1)} %param.43, bf16[8,8,2048]{2,1,0:T(8,128)(2,1)} %all-to-all-done.3, f32[64,352]{1,0:T(8,128)} %fusion.44), kind=kOutput, calls=%fused_computation.15 | convolution fusion | flops 184815616 | bytes 3497984 | tf_op jit(solution)/shard_map/dot_general | solution.py:182
  183.3 3.5 %all-to-all-done.1 = bf16[8,16,512]{2,1,0:T(8,128)(2,1)} async-done(((bf16[8,16,512]{2,1,0:T(8,128)(2,1)}), bf16[8,16,512]{2,1,0:T(8,128)(2,1)}, u32[]{:S(2)}, u32[]{:S(2)}) %all-to-all-start.1) | async-done | bytes 131104 | tf_op jit(solution)/shard_map/all_to_all | solution.py:187
  186.8 4.0 %all-to-all-start.4 = ((bf16[8,8,2048]{2,1,0:T(8,128)(2,1)}), bf16[8,8,2048]{2,1,0:T(8,128)(2,1)}, u32[]{:S(2)}, u32[]{:S(2)}) async-start(bf16[8,8,2048]{2,1,0:T(8,128)(2,1)} %fusion.17), calls=%async_computation.5 | async-start | bytes 524288 | tf_op jit(solution)/shard_map/all_to_all | solution.py:188
  190.9 4.7 %subtract_add_fusion = f32[16,8,4096]{2,1,0:T(8,128)} fusion(f32[16,8,4096]{2,1,0:T(8,128)} %bitcast.80, f32[16,8,4096]{2,1,0:T(8,128)} %bitcast.81, f32[16,8,4096]{2,1,0:T(8,128)S(1)} %bitcast.79, f32[16,8,4096]{2,1,0:T(8,128)} %bitcast.82), kind=kLoop, calls=%fused_computation.17 | loop fusion | flops 1572864 | bytes 10485760 | tf_op jit(solution)/shard_map/add | solution.py:66
  197.4 3.2 %all-to-all-done.4 = bf16[8,8,2048]{2,1,0:T(8,128)(2,1)} async-done(((bf16[8,8,2048]{2,1,0:T(8,128)(2,1)}), bf16[8,8,2048]{2,1,0:T(8,128)(2,1)}, u32[]{:S(2)}, u32[]{:S(2)}) %all-to-all-start.4) | async-done | bytes 262176 | tf_op jit(solution)/shard_map/all_to_all | solution.py:188
  200.6 3.3 %all-to-all-start.2 = ((f32[4,8,512]{2,1,0:T(8,128)}), f32[4,8,512]{2,1,0:T(8,128)S(1)}, u32[]{:S(2)}, u32[]{:S(2)}) async-start(f32[4,8,512]{2,1,0:T(8,128)} %convolution_bitcast_fusion), calls=%async_computation.3 | async-start | bytes 131072 | tf_op jit(solution)/shard_map/all_to_all | solution.py:195
  204.9 3.8 %all-to-all-done.2 = f32[4,8,512]{2,1,0:T(8,128)S(1)} async-done(((f32[4,8,512]{2,1,0:T(8,128)}), f32[4,8,512]{2,1,0:T(8,128)S(1)}, u32[]{:S(2)}, u32[]{:S(2)}) %all-to-all-start.2) | async-done | bytes 65568 | tf_op jit(solution)/shard_map/all_to_all | solution.py:195
  (80 shorter events, 54.6 us)
Async XLA Ops:
  7.2 172.8 %copy-start = (bf16[352,2048]{1,0:T(8,128)(2,1)S(1)}, bf16[352,2048]{1,0:T(8,128)(2,1)}, u32[]{:S(2)}) copy-start(bf16[352,2048]{1,0:T(8,128)(2,1)} %param.44) | copy-start | bytes 4325380
  7.2 16.7 %copy-start.10 = (f32[2048]{0:T(1024)S(1)}, f32[2048]{0:T(1024)}, u32[]{:S(2)}) copy-start(f32[2048]{0:T(1024)} %param.25) | copy-start | bytes 24580
  7.2 16.7 %copy-start.13 = (f32[256]{0:T(256)S(1)}, f32[256]{0:T(256)}, u32[]{:S(2)}) copy-start(f32[256]{0:T(256)} %param.32) | copy-start | bytes 3076
  7.2 24.2 %copy-start.2 = (f32[32,4,4096]{2,1,0:T(4,128)S(1)}, f32[32,4,4096]{2,1,0:T(4,128)}, u32[]{:S(2)}) copy-start(f32[32,4,4096]{2,1,0:T(4,128)} %param.24) | copy-start | bytes 6291460
  7.2 98.5 %all-reduce.2.cloned.1.call-start = ((), (), s32[]{:S(2)}) async-start(), calls=%async_computation.6 | async-start | bytes 262144 | tf_op jit(solution)/shard_map/psum | solution.py:140
  34.7 9.7 %copy-start.1 = (f32[32,4,64,64]{3,2,1,0:T(8,128)S(1)}, f32[32,4,64,64]{3,2,1,0:T(8,128)}, u32[]{:S(2)}) copy-start(f32[32,4,64,64]{3,2,1,0:T(8,128)} %reshape.173) | copy-start | bytes 6291460
  34.7 9.8 %copy-start.6 = (f32[32,4,64]{2,1,0:T(4,128)S(1)}, f32[32,4,64]{2,1,0:T(4,128)}, u32[]{:S(2)}) copy-start(f32[32,4,64]{2,1,0:T(4,128)} %mul.226) | copy-start | bytes 98308
  34.7 9.8 %copy-start.7 = (f32[32,4,64]{2,1,0:T(4,128)S(1)}, f32[32,4,64]{2,1,0:T(4,128)}, u32[]{:S(2)}) copy-start(f32[32,4,64]{2,1,0:T(4,128)} %mul.240) | copy-start | bytes 98308
  34.7 9.8 %copy-start.8 = (f32[32,4,64]{2,1,0:T(4,128)S(1)}, f32[32,4,64]{2,1,0:T(4,128)}, u32[]{:S(2)}) copy-start(f32[32,4,64]{2,1,0:T(4,128)} %mul.243) | copy-start | bytes 98308
  34.7 9.8 %copy-start.11 = (f32[32,4,64,1]{2,1,0,3:T(4,128)S(1)}, f32[32,4,64,1]{2,1,0,3:T(4,128)}, u32[]{:S(2)}) copy-start(f32[32,4,64,1]{2,1,0,3:T(4,128)} %reshape.185) | copy-start | bytes 98308
  35.9 17.6 %copy-start.5 = (f32[32,4,64]{2,1,0:T(4,128)}, f32[32,4,64]{2,1,0:T(4,128)S(1)}, u32[]{:S(2)}) copy-start(f32[32,4,64]{2,1,0:T(4,128)S(1)} %get-tuple-element.4) | copy-start | bytes 98308
  44.5 9.0 %copy-start.4 = (f32[32,4,1,64]{3,2,1,0:T(1,128)}, f32[32,4,1,64]{3,2,1,0:T(1,128)S(1)}, u32[]{:S(2)}) copy-start(f32[32,4,1,64]{3,2,1,0:T(1,128)S(1)} %fusion.70) | copy-start | bytes 98308
  108.6 0.7 copy-start.3
  111.1 20.0 %all-to-all-start = ((bf16[8,16,2048]{2,1,0:T(8,128)(2,1)}), bf16[8,16,2048]{2,1,0:T(8,128)(2,1)}, u32[]{:S(2)}, u32[]{:S(2)}) async-start(bf16[8,16,2048]{2,1,0:T(8,128)(2,1)} %convolution_convert_fusion), calls=%async_computation | async-start | bytes 1048576 | tf_op jit(solution)/shard_map/all_to_all | solution.py:157
  115.7 59.4 %reduce-scatter.2.cloned.1.call-start = ((), (), s32[]{:S(2)}) async-start(), calls=%async_computation.7 | async-start | bytes 655360 | tf_op jit(solution)/shard_map/reduce_scatter | solution.py:172
  142.5 30.0 %all-to-all-start.3 = ((bf16[8,8,2048]{2,1,0:T(8,128)(2,1)}), bf16[8,8,2048]{2,1,0:T(8,128)(2,1)}, u32[]{:S(2)}, u32[]{:S(2)}) async-start(bf16[8,8,2048]{2,1,0:T(8,128)(2,1)} %broadcast_in_dim.2), calls=%async_computation.4 | async-start | bytes 524288 | tf_op jit(solution)/shard_map/all_to_all | solution.py:158
  175.2 11.7 %all-to-all-start.1 = ((bf16[8,16,512]{2,1,0:T(8,128)(2,1)}), bf16[8,16,512]{2,1,0:T(8,128)(2,1)}, u32[]{:S(2)}, u32[]{:S(2)}) async-start(bf16[8,16,512]{2,1,0:T(8,128)(2,1)} %bitcast.91), calls=%async_computation.2 | async-start | bytes 262144 | tf_op jit(solution)/shard_map/all_to_all | solution.py:187
  186.8 13.8 %all-to-all-start.4 = ((bf16[8,8,2048]{2,1,0:T(8,128)(2,1)}), bf16[8,8,2048]{2,1,0:T(8,128)(2,1)}, u32[]{:S(2)}, u32[]{:S(2)}) async-start(bf16[8,8,2048]{2,1,0:T(8,128)(2,1)} %fusion.17), calls=%async_computation.5 | async-start | bytes 524288 | tf_op jit(solution)/shard_map/all_to_all | solution.py:188
  190.9 4.8 %copy-start.12 = (f32[2048]{0:T(1024)S(1)}, f32[2048]{0:T(1024)}, u32[]{:S(2)}) copy-start(f32[2048]{0:T(1024)} %param.45) | copy-start | bytes 24580
  190.9 4.8 %copy-start.9 = (f32[32,8,16]{0,2,1:T(8,128)S(1)}, f32[32,8,16]{0,2,1:T(8,128)}, u32[]{:S(2)}) copy-start(f32[32,8,16]{0,2,1:T(8,128)} %get-tuple-element.2) | copy-start | bytes 49156
  200.6 8.1 %all-to-all-start.2 = ((f32[4,8,512]{2,1,0:T(8,128)}), f32[4,8,512]{2,1,0:T(8,128)S(1)}, u32[]{:S(2)}, u32[]{:S(2)}) async-start(f32[4,8,512]{2,1,0:T(8,128)} %convolution_bitcast_fusion), calls=%async_computation.3 | async-start | bytes 131072 | tf_op jit(solution)/shard_map/all_to_all | solution.py:195
Sparse Core Ops, SparseCore 0:
  60.7 44.9 all-reduce.1
  141.2 23.0 reduce-scatter.1
where the time goes:
time: 219 us; the launch traced here: 217 us
  waiting for transfers between devices  60.1 us (27%)
  matrix products  48.1 us (22%)
  local copies, waits for them, and re-layouts  41.5 us (19%)
  other arithmetic  32 us (15%)
  starting transfers between devices  21 us (10%)
  between operations  14.3 us (7%)
    psum x1, waiting for transfers between devices, local(): lax.psum(partial_out.astype(jnp.bfloat16), 'tp').astype(jnp.float32)  34.1 us
    all_to_all x1, waiting for transfers between devices, local(): lax.all_to_all(send_rows, 'ep', split_axis=0, concat_axis=0, tiled=True)  15.4 us
    mul x3, local copies, waits for them, and re-layouts, state_update(): matrix * decay_head[:, :, None, :]  9.51 us
    dot_general x1, matrix products, state_update(): jnp.einsum('bhvk,bhk->bhv', updated, head_receptance, precision=PRECISE)  8.96 us
    dot_general x1, matrix products, state_update(): removed = jnp.einsum('bhvk,bhk->bhv', matrix, unit_keys, precision=PRECISE)  8.58 us
    mul x3, local copies, waits for them, and re-layouts, state_update(): head_values[..., None] * head_keys[:, :, None, :]  7.99 us
    dot_general x1, matrix products, local(): jnp.einsum('lrf,lfd->lrd', expert_hidden, expert_down_weight, preferred_e...  5.98 us
    reshape x4, local copies, waits for them, and re-layouts, split_heads(): return block.reshape(seq_count, -1, head_width)  5.88 us
  transfers between devices with their start and end apart: 7, of which 5 were waited for; matrix products, arithmetic and copies ran while one was open for 24% of the time, Pallas kernels for 0%

commit v1 on v0

v1 whole, which is shorter than its diff:
```python
import functools

import jax
import jax.numpy as jnp
from jax import lax
from jax.experimental import pallas as pl
from jax.experimental.pallas import tpu as pltpu
from jax.sharding import PartitionSpec as P

HEAD_WIDTH = 64
F32 = jnp.float32
BF16 = jnp.bfloat16
HIGHEST = lax.Precision.HIGHEST
VMEM = pl.BlockSpec(memory_space=pltpu.VMEM)
SMEM = pl.BlockSpec(memory_space=pltpu.SMEM)


def iota(shape, dim):
    return lax.broadcasted_iota(jnp.int32, shape, dim)


def dot(a, b):
    return jnp.dot(a, b, preferred_element_type=F32)


def dot_exact(a, b):
    return jnp.dot(a, b, preferred_element_type=F32, precision=HIGHEST)


def halves(x):
    high = x.astype(BF16)
    return high, (x - high.astype(F32)).astype(BF16)


def rms_rows(floats, gain):
    return floats * lax.rsqrt(jnp.mean(floats * floats, axis=-1, keepdims=True) + 1e-06) * gain


def silu(x):
    return x * jax.nn.sigmoid(x)


def attention_kernel(
    tokens,
    state,
    gain,
    rec_m,
    key_m,
    val_m,
    dec_m,
    dec_off,
    cor_off,
    cor_fac,
    own_w,
    head_gain,
    out_m,
    next_state,
    partial,
    rows_ref,
):
    seqs, heads, area = state.shape
    width = area // HEAD_WIDTH
    count = seqs * heads
    for b in range(seqs):
        rows_ref[b * heads : (b + 1) * heads, :] = state[b]
    normed = rms_rows(tokens[...].astype(F32), gain[...]).astype(BF16)
    rec = dot(normed, rec_m[...])
    keys = dot(normed, key_m[...])
    vals = dot(normed, val_m[...])
    decay = jnp.exp(-jnp.exp(dec_off[...] + dot(normed, dec_m[...])))
    rate = jax.nn.sigmoid(cor_off[...] + cor_fac[...] * keys)
    key_in = keys * rate

    def by_head(x):
        return jnp.concatenate([x[:, h * width : (h + 1) * width] for h in range(heads)], axis=0)

    keys_h = by_head(keys)
    unit = (
        keys_h
        * lax.rsqrt(jnp.mean(keys_h * keys_h, axis=-1, keepdims=True) + 1e-06)
        * width ** (-0.5)
    )
    erase = unit * by_head(rate)
    rec_h = by_head(rec)
    key_in_h = by_head(key_in)
    vals_h = by_head(vals)
    decay_h = by_head(decay)
    own = jnp.sum(by_head(rec * key_in * own_w[...]), axis=-1, keepdims=True)
    erase_dot = jnp.sum(erase * rec_h, axis=-1, keepdims=True)
    write_dot = jnp.sum(key_in_h * rec_h, axis=-1, keepdims=True)
    row = iota((count, count), 0)
    col = iota((count, count), 1)
    to_seq = (col == (row % heads) * seqs + row // heads).astype(F32)
    to_head = (row == (col % heads) * seqs + col // heads).astype(F32)
    packed = dot_exact(
        to_seq,
        jnp.concatenate([unit, decay_h * rec_h, decay_h, erase, key_in_h, vals_h], axis=1),
    )

    def twice(n):
        part = packed[:, n * width : (n + 1) * width]
        return jnp.concatenate([part, part], axis=1)

    chunk = 8 * width
    steps = area // chunk

    def wide(n):
        return jnp.concatenate([twice(n)] * (chunk // (2 * width)), axis=1)

    unit_w = wide(0)
    read_w = wide(1)
    sums = jnp.zeros((count, 2 * width), F32)
    lane = iota((chunk, 2 * width), 0) // width
    slot = iota((chunk, 2 * width), 1)
    for j in range(steps):
        block = rows_ref[:, j * chunk : (j + 1) * chunk]
        left = (slot == lane + 8 * j).astype(F32).astype(BF16)
        right = (slot == lane + (8 * j + width)).astype(F32).astype(BF16)
        a_hi, a_lo = halves(block * unit_w)
        b_hi, b_lo = halves(block * read_w)
        sums = sums + (dot(a_hi, left) + dot(a_lo, left)) + (dot(b_hi, right) + dot(b_lo, right))
    removed_hi, removed_lo = halves(sums[:, :width])
    removed_x = jnp.concatenate([removed_hi, removed_lo], axis=1)
    vals_hi, vals_lo = halves(packed[:, 5 * width : 6 * width])
    vals_x = jnp.concatenate([vals_hi, vals_lo], axis=1)
    decay_w = wide(2)
    erase_w = wide(3)
    key_w = wide(4)
    source = iota((2 * width, chunk), 0) % width
    target = iota((2 * width, chunk), 1) // width
    for j in range(steps):
        spread = (source == target + 8 * j).astype(F32).astype(BF16)
        block = rows_ref[:, j * chunk : (j + 1) * chunk]
        rows_ref[:, j * chunk : (j + 1) * chunk] = (
            block * decay_w - dot(removed_x, spread) * erase_w + dot(vals_x, spread) * key_w
        )
    for b in range(seqs):
        next_state[b] = rows_ref[b * heads : (b + 1) * heads, :]
    sums_h = dot_exact(to_head, sums)
    read = sums_h[:, width:] - sums_h[:, :width] * erase_dot + vals_h * write_dot
    center = jnp.mean(read, axis=-1, keepdims=True)
    shifted = read - center
    spread_sq = jnp.mean(shifted * shifted, axis=-1, keepdims=True)
    normal = shifted * lax.rsqrt(spread_sq + 0.00064)
    extra = own * vals_h

    def by_lane(x):
        return jnp.concatenate([x[h * seqs : (h + 1) * seqs] for h in range(heads)], axis=1)

    heads_out = (by_lane(normal) * head_gain[...] + by_lane(extra)).astype(BF16)
    partial[...] = dot(heads_out, out_m[...]).astype(BF16)


def dispatch_kernel(
    place, parts, tokens, gain, routing, weights, own_hidden, own_rows, table, *sends
):
    seqs, _ = tokens.shape
    groups = len(sends)
    capacity = sends[0].shape[0]
    per_lane = own_rows.shape[0]
    me = place[0]
    lane = place[1]
    hidden = tokens[...].astype(F32)
    total = parts[0].astype(F32)
    for n in range(1, parts.shape[0]):
        total = total + parts[n].astype(F32)
    hidden = hidden + total
    rows = rms_rows(hidden, gain[...]).astype(BF16)
    slots = groups * capacity
    col = iota((seqs, slots), 1)
    expert = (col // capacity) ^ me
    place_in = (col % capacity).astype(F32)
    routes = routing[pl.ds(pl.multiple_of(me * seqs, seqs), seqs), :]
    chosen = jnp.zeros((seqs, slots), F32)
    weighted = jnp.zeros((seqs, slots), F32)
    for k in range(routing.shape[1]):
        hit = (routes[:, k : k + 1] == expert).astype(F32)
        chosen = chosen + hit
        weighted = weighted + hit * weights[:, k : k + 1]
    earlier = (iota((seqs, seqs), 1) < iota((seqs, seqs), 0)).astype(F32).astype(BF16)
    before = dot(earlier, chosen.astype(BF16))
    here = (before == place_in).astype(F32)
    pick = jnp.transpose(chosen * here).astype(BF16)
    sent = dot(pick, rows).astype(BF16)
    for k in range(groups):
        sends[k][...] = sent[k * capacity : (k + 1) * capacity]
    row = iota((seqs, seqs), 0)
    shuffled = ((row // per_lane) ^ lane) * per_lane + row % per_lane
    order = (iota((seqs, seqs), 1) == shuffled).astype(F32)
    table[...] = dot_exact(order, weighted * here)
    mine = order[:per_lane]
    own_hidden[...] = dot_exact(mine, hidden)
    own_rows[...] = dot(mine.astype(BF16), rows).astype(BF16)


def dense_kernel(groups, *refs):
    rows = refs[:groups]
    gate, up, down = refs[groups : groups + 3]
    outs = refs[groups + 3 : 2 * groups + 3]
    gathered = refs[-1]
    per = rows[0].shape[0]
    for k in range(groups):
        gathered[k * per : (k + 1) * per, :] = rows[k][...].astype(F32)
    x = gathered[...].astype(BF16)
    hidden = (silu(dot(x, gate[...])) * dot(x, up[...])).astype(BF16)
    result = dot(hidden, down[...])
    for k in range(groups):
        outs[k][...] = result[k * per : (k + 1) * per].astype(BF16)


def expert_kernel(groups, *refs):
    rows = refs[:groups]
    gate, up, down = refs[groups : groups + 3]
    outs = refs[groups + 3 : 2 * groups + 3]
    gathered, total = refs[-2:]
    per = rows[0].shape[0]
    step = pl.program_id(0)

    @pl.when(step == 0)
    def _():
        for k in range(groups):
            gathered[k * per : (k + 1) * per, :] = rows[k][...].astype(F32)
        total[...] = jnp.zeros_like(total)

    x = gathered[...].astype(BF16)
    hidden = (silu(dot(x, gate[0])) * dot(x, up[0])).astype(BF16)
    total[...] += dot(hidden, down[0])

    @pl.when(step == pl.num_programs(0) - 1)
    def _():
        for k in range(groups):
            outs[k][...] = total[k * per : (k + 1) * per].astype(BF16)


def combine_kernel(groups, table, *refs):
    rows = refs[:groups]
    own = refs[groups]
    sends = refs[groups + 1 : -1]
    gathered = refs[-1]
    per = rows[0].shape[0]
    per_lane = own.shape[0]
    for k in range(groups):
        gathered[k * per : (k + 1) * per, :] = rows[k][...].astype(F32)
    x = gathered[...].astype(BF16)
    high, low = halves(table[...])
    result = dot(high, x) + dot(low, x)
    own[...] = result[:per_lane]
    for k in range(len(sends)):
        sends[k][...] = result[(k + 1) * per_lane : (k + 2) * per_lane].astype(BF16)


def final_kernel(groups, hidden, moe, offset, *refs):
    dense = refs[:groups]
    others = refs[groups:-1]
    out = refs[-1]
    block = dense[0][...].astype(F32)
    for k in range(1, groups):
        block = block + dense[k][...].astype(F32)
    total = moe[...]
    for other in others:
        total = total + other[...].astype(F32)
    out[...] = (hidden[...] + total + jax.nn.sigmoid(offset[...]) * block).astype(BF16)


def like(shape, dtype):
    return jax.ShapeDtypeStruct(shape, dtype)


def exchange(arrays, axis):
    size = lax.axis_size(axis)
    return [arrays[0]] + [
        lax.ppermute(arrays[k], axis, [(i, i ^ k) for i in range(size)]) for k in range(1, size)
    ]


def local(
    tokens,
    recurrent_head_state,
    first_norm_gain,
    receptance_matrix,
    key_matrix,
    value_matrix,
    decay_matrix,
    decay_offset,
    correction_offset,
    correction_key_factor,
    own_term_weight,
    head_norm_gain,
    output_matrix,
    second_norm_gain,
    routing,
    routing_weight,
    expert_gate_weight,
    expert_up_weight,
    expert_down_weight,
    dense_gate_weight,
    dense_up_weight,
    dense_down_weight,
    dense_gate_offset,
):
    seqs, width = tokens.shape
    heads, area = recurrent_head_state.shape[1:]
    groups = lax.axis_size("ep")
    lanes = lax.axis_size("tp")
    per_lane = seqs // lanes
    local_experts, _, units = expert_gate_weight.shape
    assert local_experts == 1
    capacity = 2 * seqs * routing.shape[1] // groups
    place = jnp.stack([lax.axis_index("ep"), lax.axis_index("tp")]).astype(jnp.int32)

    def row(x):
        return x.reshape(1, -1)

    next_state, partial = pl.pallas_call(
        attention_kernel,
        out_shape=(like(recurrent_head_state.shape, F32), like((seqs, width), BF16)),
        in_specs=[VMEM] * 13,
        out_specs=(VMEM, VMEM),
        scratch_shapes=[pltpu.VMEM((seqs * heads, area), F32)],
        name="attention",
    )(
        tokens,
        recurrent_head_state,
        row(first_norm_gain),
        receptance_matrix,
        key_matrix,
        value_matrix,
        decay_matrix,
        row(decay_offset),
        row(correction_offset),
        row(correction_key_factor),
        row(own_term_weight),
        row(head_norm_gain),
        output_matrix,
    )
    parts = lax.all_gather(partial, "tp", axis=0, tiled=False)
    own_hidden, own_rows, table, *sends = pl.pallas_call(
        dispatch_kernel,
        out_shape=(
            like((per_lane, width), F32),
            like((per_lane, width), BF16),
            like((seqs, groups * capacity), F32),
            *[like((capacity, width), BF16)] * groups,
        ),
        in_specs=[SMEM] + [VMEM] * 5,
        out_specs=[VMEM] * (3 + groups),
        name="dispatch",
    )(place, parts, tokens, row(second_norm_gain), routing, routing_weight)
    dense_in = exchange([own_rows] * groups, "ep")
    expert_in = exchange(sends, "ep")
    dense_out = pl.pallas_call(
        functools.partial(dense_kernel, groups),
        out_shape=[like((per_lane, width), BF16)] * groups,
        in_specs=[VMEM] * (groups + 3),
        out_specs=[VMEM] * groups,
        scratch_shapes=[pltpu.VMEM((groups * per_lane, width), F32)],
        name="dense",
    )(*dense_in, dense_gate_weight, dense_up_weight, dense_down_weight)
    dense_back = exchange(dense_out, "ep")
    tile = min(256, units)
    whole = pl.BlockSpec((capacity, width), lambda i: (0, 0))
    expert_out = pl.pallas_call(
        functools.partial(expert_kernel, groups),
        grid=(units // tile,),
        out_shape=[like((capacity, width), BF16)] * groups,
        in_specs=[whole] * groups
        + [
            pl.BlockSpec((1, width, tile), lambda i: (0, 0, i)),
            pl.BlockSpec((1, width, tile), lambda i: (0, 0, i)),
            pl.BlockSpec((1, tile, width), lambda i: (0, i, 0)),
        ],
        out_specs=[whole] * groups,
        scratch_shapes=[
            pltpu.VMEM((groups * capacity, width), F32),
            pltpu.VMEM((groups * capacity, width), F32),
        ],
        name="experts",
    )(*expert_in, expert_gate_weight, expert_up_weight, expert_down_weight)
    expert_back = exchange(expert_out, "ep")
    moe_own, *moe_sends = pl.pallas_call(
        functools.partial(combine_kernel, groups),
        out_shape=[like((per_lane, width), F32)] + [like((per_lane, width), BF16)] * (lanes - 1),
        in_specs=[VMEM] * (groups + 1),
        out_specs=[VMEM] * lanes,
        scratch_shapes=[pltpu.VMEM((groups * capacity, width), F32)],
        name="combine",
    )(table, *expert_back)
    moe_in = exchange([moe_own] + moe_sends, "tp")
    layer_out = pl.pallas_call(
        functools.partial(final_kernel, groups),
        out_shape=like((per_lane, width), BF16),
        in_specs=[VMEM] * (3 + groups + lanes - 1),
        out_specs=VMEM,
        name="final",
    )(own_hidden, moe_in[0], row(dense_gate_offset), *dense_back, *moe_in[1:])
    return (layer_out, next_state)


def solution(mesh):
    return jax.shard_map(
        local,
        mesh=mesh,
        in_specs=(
            P("ep", None),
            P("ep", "tp", None),
            P(),
            P(None, "tp"),
            P(None, "tp"),
            P(None, "tp"),
            P(None, "tp"),
            P("tp"),
            P("tp"),
            P("tp"),
            P("tp"),
            P("tp"),
            P("tp", None),
            P(),
            P(),
            P("ep", None),
            P("ep", None, "tp"),
            P("ep", None, "tp"),
            P("ep", "tp", None),
            P(None, "ep"),
            P(None, "ep"),
            P("ep", None),
            P(),
        ),
        out_specs=(P(("ep", "tp"), None), P("ep", "tp", None)),
        check_vma=False,
    )
```

time: 219 us -> 97.7 us (0.45)
  waiting for transfers between devices: 60.1 us -> 6.96 us
  matrix products: 48.1 us -> 0 us
  local copies, waits for them, and re-layouts: 41.5 us -> 7.04 us
  other arithmetic: 32 us -> 0.67 us
  Pallas kernels: 0 us -> 28.2 us
  starting transfers between devices: 21 us -> 40.5 us
  between operations: 14.3 us -> 0.96 us
  blocking collectives: 0 us -> 13.1 us
    dot_general x13 -> x0, matrix products: 48.1 us -> none  [the longest x1 8.96 us: state_update(): jnp.einsum('bhvk,bhk->bhv', updated, head_receptance, precision=PRECISE)]
    ppermute x0 -> x31, starting transfers between devices: none -> 40.5 us  [exchange(): lax.ppermute(arrays[k], axis, [(i, i ^ k) for i in range(size)])]
    psum x1 -> x0, waiting for transfers between devices: 34.1 us -> none  [local(): lax.psum(partial_out.astype(jnp.bfloat16), 'tp').astype(jnp.float32)]
    pallas_call x0 -> x6, Pallas kernels: none -> 28.2 us  [the longest x1 9.91 us: local(): pl.pallas_call(attention_kernel, out_shape=(like(recurrent_head_state.sha...]
    all_to_all x5 -> x0, waiting for transfers between devices: 25.9 us -> none  [the longest x1 15.4 us: local(): lax.all_to_all(send_rows, 'ep', split_axis=0, concat_axis=0, tiled=True)]
    mul x9 -> x0, local copies, waits for them, and re-layouts: 25.2 us -> none  [the longest x3 9.51 us: state_update(): matrix * decay_head[:, :, None, :]]
    all_to_all x5 -> x0, starting transfers between devices: 21 us -> none  [the longest x1 4.82 us: local(): lax.all_to_all(back_send, 'ep', split_axis=0, concat_axis=0, tiled=True)]
    all_gather x0 -> x1, blocking collectives: none -> 13.1 us  [local(): parts = lax.all_gather(partial, 'tp', axis=0, tiled=False)]
  transfers between devices with their start and end apart: 7 -> 31, of which waited for: 5 -> 6; matrix products, arithmetic and copies ran while one was open for 24% -> 3% of each run, Pallas kernels for 0% -> 14%
where the time goes in v1:
time: 97.7 us; the launch traced here: 97.4 us
  starting transfers between devices  40.5 us (41%)
  Pallas kernels  28.2 us (29%)
  blocking collectives  13.1 us (13%)
  local copies, waits for them, and re-layouts  7.04 us (7%)
  waiting for transfers between devices  6.96 us (7%)
    ppermute x31, starting transfers between devices, exchange(): lax.ppermute(arrays[k], axis, [(i, i ^ k) for i in range(size)])  40.5 us
    all_gather x1, blocking collectives, local(): parts = lax.all_gather(partial, 'tp', axis=0, tiled=False)  13.1 us
    pallas_call x1, Pallas kernels, local(): pl.pallas_call(attention_kernel, out_shape=(like(recurrent_head_state.sha...  9.91 us
    pallas_call x1, Pallas kernels, local(): pl.pallas_call(functools.partial(expert_kernel, groups), grid=(units // t...  7.91 us
    unnamed x76, local copies, waits for them, and re-layouts  7.04 us
    ppermute x31, waiting for transfers between devices, exchange(): lax.ppermute(arrays[k], axis, [(i, i ^ k) for i in range(size)])  6.96 us
    pallas_call x1, Pallas kernels, local(): pl.pallas_call(functools.partial(dense_kernel, groups), out_shape=[like((...  4.14 us
    pallas_call x1, Pallas kernels, local(): pl.pallas_call(dispatch_kernel, out_shape=(like((per_lane, width), F32),...  2.56 us
  transfers between devices with their start and end apart: 31, of which 6 were waited for; matrix products, arithmetic and copies ran while one was open for 3% of the time, Pallas kernels for 14%

profile of v1, /device:TPU:0, one launch (start us, length us, event | category | flops | bytes accessed | tf_op | source)
XLA Modules:
  0.0 97.4 jit_solution(10569059480726222187)
XLA Ops:
  0.7 9.9 %attention.1 = (f32[32,4,4096]{2,1,0:T(4,128)}, bf16[32,2048]{1,0:T(8,128)(2,1)}) custom-call(bf16[32,2048]{1,0:T(8,128)(2,1)} %tokens.3, f32[32,4,4096]{2,1,0:T(4,128)} %state.1, f32[1,2048]{1,0:T(1,128)} %bitcast.14, bf16[2048,256]{1,0:T(8,128)(2,1)} %rec_m.1, bf16[2048,256]{1,0:T(8,128)(2,1)} %key_m.1, bf16[2048,256]{1,0:T(8,128)(2,1)} %val_m.1, ...), custom_call_target="tpu_custom_call" | custom-call | tf_op jit(solution)/shard_map/attention/pallas_call | solution.py:314
  10.6 13.1 %all-gather = bf16[128,2048]{1,0:T(8,128)(2,1)} all-gather(bf16[32,2048]{1,0:T(8,128)(2,1)} %get-tuple-element.35), channel_id=2, replica_groups=mesh['ep'=8,'tp'=4] {'tp'}, dimensions={0}, use_global_device_ids=true | all-gather | bytes 655360 | tf_op jit(solution)/shard_map/all_gather | solution.py:336
  25.9 2.6 %dispatch.1 = (f32[8,2048]{1,0:T(8,128)}, bf16[8,2048]{1,0:T(8,128)(2,1)}, f32[32,128]{1,0:T(8,128)}, bf16[16,2048]{1,0:T(8,128)(2,1)}, bf16[16,2048]{1,0:T(8,12...) custom-call(s32[2]{0:T(128)} %pad_add_fusion.place, ...), custom_call_target="tpu_custom_call" | custom-call | tf_op jit(solution)/shard_map/dispatch/pallas_call | solution.py:337
  28.5 1.6 %collective-permute-start.1 = (bf16[16,2048]{1,0:T(8,128)(2,1)}, bf16[16,2048]{1,0:T(8,128)(2,1)S(1)}, u32[]{:S(2)}, u32[]{:S(2)}) collective-permute-start(bf16[16,2048]{1,0:T(8,128)(2,1)} %get-tuple-element.40), channel_id=1, source_target_pairs={{0,8},{4,12},{8,0},{12,4},{16,24},{20,28},{24,16},{28,20},{1,9},{5... | collective-permute-start | bytes 196616 | tf_op jit(solution)/shard_map/ppermute | solution.py:272
  30.4 2.6 %collective-permute-start.3 = (bf16[16,2048]{1,0:T(8,128)(2,1)}, bf16[16,2048]{1,0:T(8,128)(2,1)S(1)}, u32[]{:S(2)}, u32[]{:S(2)}) collective-permute-start(bf16[16,2048]{1,0:T(8,128)(2,1)} %get-tuple-element.42), channel_id=1, source_target_pairs={{0,16},{4,20},{8,24},{12,28},{16,0},{20,4},{24,8},{28,12},{1,17},{... | collective-permute-start | bytes 196616 | tf_op jit(solution)/shard_map/ppermute | solution.py:272
  33.0 3.6 %collective-permute-start.5 = (bf16[16,2048]{1,0:T(8,128)(2,1)}, bf16[16,2048]{1,0:T(8,128)(2,1)S(1)}, u32[]{:S(2)}, u32[]{:S(2)}) collective-permute-start(bf16[16,2048]{1,0:T(8,128)(2,1)} %get-tuple-element.44), channel_id=1, source_target_pairs={{0,24},{4,28},{8,16},{12,20},{16,8},{20,12},{24,0},{28,4},{1,25},{... | collective-permute-start | bytes 196616 | tf_op jit(solution)/shard_map/ppermute | solution.py:272
  37.5 4.6 %collective-permute-start.15 = (bf16[8,2048]{1,0:T(8,128)(2,1)}, bf16[8,2048]{1,0:T(8,128)(2,1)S(1)}, u32[]{:S(2)}, u32[]{:S(2)}) collective-permute-start(bf16[8,2048]{1,0:T(8,128)(2,1)} %get-tuple-element.55.refs_0_), channel_id=1, source_target_pairs={{0,8},{4,12},{8,0},{12,4},{16,24},{20,28},{24,16},{28,20},{1,9},{5... | collective-permute-start | bytes 98312 | tf_op jit(solution)/shard_map/ppermute | solution.py:272
  42.1 1.6 %collective-permute-done.4.refs_5_ = bf16[16,2048]{1,0:T(8,128)(2,1)S(1)} collective-permute-done((bf16[16,2048]{1,0:T(8,128)(2,1)}, bf16[16,2048]{1,0:T(8,128)(2,1)S(1)}, u32[]{:S(2)}, u32[]{:S(2)}) %collective-permute-start.4) | collective-permute-done | bytes 65568 | tf_op jit(solution)/shard_map/ppermute | solution.py:272
  43.8 3.3 %collective-permute-start.17 = (bf16[8,2048]{1,0:T(8,128)(2,1)}, bf16[8,2048]{1,0:T(8,128)(2,1)S(1)}, u32[]{:S(2)}, u32[]{:S(2)}) collective-permute-start(bf16[8,2048]{1,0:T(8,128)(2,1)} %get-tuple-element.55.refs_0_), channel_id=1, source_target_pairs={{0,16},{4,20},{8,24},{12,28},{16,0},{20,4},{24,8},{28,12},{1,17},{... | collective-permute-start | bytes 98312 | tf_op jit(solution)/shard_map/ppermute | solution.py:272
  47.6 7.9 %experts.1 = (bf16[16,2048]{1,0:T(8,128)(2,1)}, bf16[16,2048]{1,0:T(8,128)(2,1)}, bf16[16,2048]{1,0:T(8,128)(2,1)}, bf16[16,2048]{1,0:T(8,128)(2,1)}, bf16[16,20...) custom-call(bf16[16,2048]{1,0:T(8,128)(2,1)} %get-tuple-element.38.refs_0_, ...), custom_call_target="tpu_custom_call" | custom-call | tf_op jit(solution)/shard_map/experts/pallas_call | solution.py:362
  57.4 2.6 %collective-permute-start.19 = (bf16[8,2048]{1,0:T(8,128)(2,1)S(1)}, bf16[8,2048]{1,0:T(8,128)(2,1)S(1)}, u32[]{:S(2)}, u32[]{:S(2)}) collective-permute-start(bf16[8,2048]{1,0:T(8,128)(2,1)S(1)} %copy-done.16), channel_id=1, source_target_pairs={{0,24},{4,28},{8,16},{12,20},{16,8},{20,12},{24,0},{28,4},{1,25},{... | collective-permute-start | bytes 98312 | tf_op jit(solution)/shard_map/ppermute | solution.py:272
  65.9 2.6 %collective-permute-start.12 = (bf16[16,2048]{1,0:T(8,128)(2,1)}, bf16[16,2048]{1,0:T(8,128)(2,1)S(1)}, u32[]{:S(2)}, u32[]{:S(2)}) collective-permute-start(bf16[16,2048]{1,0:T(8,128)(2,1)} %get-tuple-element.52), channel_id=1, source_target_pairs={{0,24},{4,28},{8,16},{12,20},{16,8},{20,12},{24,0},{28,4},{1,25},{... | collective-permute-start | bytes 196616 | tf_op jit(solution)/shard_map/ppermute | solution.py:272
  68.4 2.0 %collective-permute-start.13 = (bf16[16,2048]{1,0:T(8,128)(2,1)}, bf16[16,2048]{1,0:T(8,128)(2,1)S(1)}, u32[]{:S(2)}, u32[]{:S(2)}) collective-permute-start(bf16[16,2048]{1,0:T(8,128)(2,1)} %get-tuple-element.53), channel_id=1, source_target_pairs={{0,28},{4,24},{8,20},{12,16},{16,12},{20,8},{24,4},{28,0},{1,29},{... | collective-permute-start | bytes 196616 | tf_op jit(solution)/shard_map/ppermute | solution.py:272
  70.5 1.6 %copy.27.refs_8_ = bf16[2048,352]{1,0:T(8,128)(2,1)} copy(bf16[2048,352]{0,1:T(8,128)(2,1)S(1)} %copy-done) | data formatting | bytes 2883584 | tf_op args[19]
  72.1 1.6 %copy.28.refs_9_ = bf16[2048,352]{1,0:T(8,128)(2,1)} copy(bf16[2048,352]{0,1:T(8,128)(2,1)S(1)} %copy-done.1) | data formatting | bytes 2883584 | tf_op args[20]
  73.7 4.1 %dense.1 = (bf16[8,2048]{1,0:T(8,128)(2,1)}, bf16[8,2048]{1,0:T(8,128)(2,1)}, bf16[8,2048]{1,0:T(8,128)(2,1)}, bf16[8,2048]{1,0:T(8,128)(2,1)}, bf16[8,2048]{1,0...) custom-call(bf16[8,2048]{1,0:T(8,128)(2,1)} %get-tuple-element.55.refs_0_, ...), custom_call_target="tpu_custom_call" | custom-call | tf_op jit(solution)/shard_map/dense/pallas_call | solution.py:351
  78.0 1.7 %collective-permute-start.23 = (bf16[8,2048]{1,0:T(8,128)(2,1)}, bf16[8,2048]{1,0:T(8,128)(2,1)S(1)}, u32[]{:S(2)}, u32[]{:S(2)}) collective-permute-start(bf16[8,2048]{1,0:T(8,128)(2,1)} %get-tuple-element.59), channel_id=1, source_target_pairs={{0,12},{4,8},{8,4},{12,0},{16,28},{20,24},{24,20},{28,16},{1,13},{... | collective-permute-start | bytes 98312 | tf_op jit(solution)/shard_map/ppermute | solution.py:272
  79.8 1.5 %collective-permute-start.24 = (bf16[8,2048]{1,0:T(8,128)(2,1)}, bf16[8,2048]{1,0:T(8,128)(2,1)S(1)}, u32[]{:S(2)}, u32[]{:S(2)}) collective-permute-start(bf16[8,2048]{1,0:T(8,128)(2,1)} %get-tuple-element.60), channel_id=1, source_target_pairs={{0,16},{4,20},{8,24},{12,28},{16,0},{20,4},{24,8},{28,12},{1,17},{... | collective-permute-start | bytes 98312 | tf_op jit(solution)/shard_map/ppermute | solution.py:272
  82.4 2.0 %combine.1 = (f32[8,2048]{1,0:T(8,128)}, bf16[8,2048]{1,0:T(8,128)(2,1)}, bf16[8,2048]{1,0:T(8,128)(2,1)}, bf16[8,2048]{1,0:T(8,128)(2,1)}) custom-call(f32[32,128]{1,0:T(8,128)} %get-tuple-element.37.table, bf16[16,2048]{1,0:T(8,128)(2,1)} %get-tuple-element.46.refs_0_, bf16[16,2048]{1,0:T(8,128)(2,1)} %copy-done.9, bf16[16,2048]{1,0:T(8,128)(2,1)} %copy-done.10, ...), custom_call_target="tpu_custom_call" | custom-call | tf_op jit(solution)/shard_map/combine/pallas_call | solution.py:380
  84.4 2.6 %collective-permute-start.26 = (bf16[8,2048]{1,0:T(8,128)(2,1)}, bf16[8,2048]{1,0:T(8,128)(2,1)S(1)}, u32[]{:S(2)}, u32[]{:S(2)}) collective-permute-start(bf16[8,2048]{1,0:T(8,128)(2,1)} %get-tuple-element.62), channel_id=1, source_target_pairs={{0,24},{4,28},{8,16},{12,20},{16,8},{20,12},{24,0},{28,4},{1,25},{... | collective-permute-start | bytes 98312 | tf_op jit(solution)/shard_map/ppermute | solution.py:272
  88.6 1.5 %collective-permute-start.29 = (bf16[8,2048]{1,0:T(8,128)(2,1)}, bf16[8,2048]{1,0:T(8,128)(2,1)S(1)}, u32[]{:S(2)}, u32[]{:S(2)}) collective-permute-start(bf16[8,2048]{1,0:T(8,128)(2,1)} %get-tuple-element.65), channel_id=1, source_target_pairs={{0,2},{1,3},{2,0},{3,1},{4,6},{5,7},{6,4},{7,5},{8,10},{9,11},{10,... | collective-permute-start | bytes 98312 | tf_op jit(solution)/shard_map/ppermute | solution.py:272
  90.1 1.5 %collective-permute-start.30 = (bf16[8,2048]{1,0:T(8,128)(2,1)}, bf16[8,2048]{1,0:T(8,128)(2,1)S(1)}, u32[]{:S(2)}, u32[]{:S(2)}) collective-permute-start(bf16[8,2048]{1,0:T(8,128)(2,1)} %get-tuple-element.66), channel_id=1, source_target_pairs={{0,3},{1,2},{2,1},{3,0},{4,7},{5,6},{6,5},{7,4},{8,11},{9,10},{10,... | collective-permute-start | bytes 98312 | tf_op jit(solution)/shard_map/ppermute | solution.py:272
  92.7 2.4 %collective-permute-done.30.refs_10_ = bf16[8,2048]{1,0:T(8,128)(2,1)S(1)} collective-permute-done((bf16[8,2048]{1,0:T(8,128)(2,1)}, bf16[8,2048]{1,0:T(8,128)(2,1)S(1)}, u32[]{:S(2)}, u32[]{:S(2)}) %collective-permute-start.30) | collective-permute-done | bytes 32800 | tf_op jit(solution)/shard_map/ppermute | solution.py:272
  95.7 1.7 %final.1 = bf16[8,2048]{1,0:T(8,128)(2,1)} custom-call(f32[8,2048]{1,0:T(8,128)} %get-tuple-element.36.hidden, f32[8,2048]{1,0:T(8,128)} %get-tuple-element.54.moe, f32[1,2048]{1,0:T(1,128)} %bitcast.13, bf16[8,2048]{1,0:T(8,128)(2,1)} %get-tuple-element.56.refs_0_, bf16[8,2048]{1,0:T(8,128)(2,1)} %copy-done.24, bf16[8,2048]{1,0:T(8,128)(2,1)} %copy-done.25, ...), custom_call_target="tpu_custom_call" | custom-call | tf_op jit(solution)/shard_map/final/pallas_call | solution.py:389
  (122 shorter events, 16.3 us)
Async XLA Ops:
  28.5 8.1 %collective-permute-start.1 = (bf16[16,2048]{1,0:T(8,128)(2,1)}, bf16[16,2048]{1,0:T(8,128)(2,1)S(1)}, u32[]{:S(2)}, u32[]{:S(2)}) collective-permute-start(bf16[16,2048]{1,0:T(8,128)(2,1)} %get-tuple-element.40), channel_id=1, source_target_pairs={{0,8},{4,12},{8,0},{12,4},{16,24},{20,28},{24,16},{28,20},{1,9},{5... | collective-permute-start | bytes 196616 | tf_op jit(solution)/shard_map/ppermute | solution.py:272
  30.1 6.6 %collective-permute-start.2 = (bf16[16,2048]{1,0:T(8,128)(2,1)}, bf16[16,2048]{1,0:T(8,128)(2,1)S(1)}, u32[]{:S(2)}, u32[]{:S(2)}) collective-permute-start(bf16[16,2048]{1,0:T(8,128)(2,1)} %get-tuple-element.41), channel_id=1, source_target_pairs={{0,12},{4,8},{8,4},{12,0},{16,28},{20,24},{24,20},{28,16},{1,13},{... | collective-permute-start | bytes 196616 | tf_op jit(solution)/shard_map/ppermute | solution.py:272
  30.4 7.1 %collective-permute-start.3 = (bf16[16,2048]{1,0:T(8,128)(2,1)}, bf16[16,2048]{1,0:T(8,128)(2,1)S(1)}, u32[]{:S(2)}, u32[]{:S(2)}) collective-permute-start(bf16[16,2048]{1,0:T(8,128)(2,1)} %get-tuple-element.42), channel_id=1, source_target_pairs={{0,16},{4,20},{8,24},{12,28},{16,0},{20,4},{24,8},{28,12},{1,17},{... | collective-permute-start | bytes 196616 | tf_op jit(solution)/shard_map/ppermute | solution.py:272
  32.9 10.8 %collective-permute-start.4 = (bf16[16,2048]{1,0:T(8,128)(2,1)}, bf16[16,2048]{1,0:T(8,128)(2,1)S(1)}, u32[]{:S(2)}, u32[]{:S(2)}) collective-permute-start(bf16[16,2048]{1,0:T(8,128)(2,1)} %get-tuple-element.43), channel_id=1, source_target_pairs={{0,20},{4,16},{8,28},{12,24},{16,4},{20,0},{24,12},{28,8},{1,21},{... | collective-permute-start | bytes 196616 | tf_op jit(solution)/shard_map/ppermute | solution.py:272
  33.0 10.8 %collective-permute-start.5 = (bf16[16,2048]{1,0:T(8,128)(2,1)}, bf16[16,2048]{1,0:T(8,128)(2,1)S(1)}, u32[]{:S(2)}, u32[]{:S(2)}) collective-permute-start(bf16[16,2048]{1,0:T(8,128)(2,1)} %get-tuple-element.44), channel_id=1, source_target_pairs={{0,24},{4,28},{8,16},{12,20},{16,8},{20,12},{24,0},{28,4},{1,25},{... | collective-permute-start | bytes 196616 | tf_op jit(solution)/shard_map/ppermute | solution.py:272
  36.6 10.4 %collective-permute-start.6 = (bf16[16,2048]{1,0:T(8,128)(2,1)}, bf16[16,2048]{1,0:T(8,128)(2,1)S(1)}, u32[]{:S(2)}, u32[]{:S(2)}) collective-permute-start(bf16[16,2048]{1,0:T(8,128)(2,1)} %get-tuple-element.45), channel_id=1, source_target_pairs={{0,28},{4,24},{8,20},{12,16},{16,12},{20,8},{24,4},{28,0},{1,29},{... | collective-permute-start | bytes 196616 | tf_op jit(solution)/shard_map/ppermute | solution.py:272
  36.7 18.9 %collective-permute-start.14 = (bf16[8,2048]{1,0:T(8,128)(2,1)}, bf16[8,2048]{1,0:T(8,128)(2,1)S(1)}, u32[]{:S(2)}, u32[]{:S(2)}) collective-permute-start(bf16[8,2048]{1,0:T(8,128)(2,1)} %get-tuple-element.55.refs_0_), channel_id=1, source_target_pairs={{0,4},{4,0},{8,12},{12,8},{16,20},{20,16},{24,28},{28,24},{1,5},{5... | collective-permute-start | bytes 98312 | tf_op jit(solution)/shard_map/ppermute | solution.py:272
  37.5 18.7 %collective-permute-start.15 = (bf16[8,2048]{1,0:T(8,128)(2,1)}, bf16[8,2048]{1,0:T(8,128)(2,1)S(1)}, u32[]{:S(2)}, u32[]{:S(2)}) collective-permute-start(bf16[8,2048]{1,0:T(8,128)(2,1)} %get-tuple-element.55.refs_0_), channel_id=1, source_target_pairs={{0,8},{4,12},{8,0},{12,4},{16,24},{20,28},{24,16},{28,20},{1,9},{5... | collective-permute-start | bytes 98312 | tf_op jit(solution)/shard_map/ppermute | solution.py:272
  43.7 13.6 %collective-permute-start.16 = (bf16[8,2048]{1,0:T(8,128)(2,1)}, bf16[8,2048]{1,0:T(8,128)(2,1)S(1)}, u32[]{:S(2)}, u32[]{:S(2)}) collective-permute-start(bf16[8,2048]{1,0:T(8,128)(2,1)} %get-tuple-element.55.refs_0_), channel_id=1, source_target_pairs={{0,12},{4,8},{8,4},{12,0},{16,28},{20,24},{24,20},{28,16},{1,13},{... | collective-permute-start | bytes 98312 | tf_op jit(solution)/shard_map/ppermute | solution.py:272
  43.8 16.2 %collective-permute-start.17 = (bf16[8,2048]{1,0:T(8,128)(2,1)}, bf16[8,2048]{1,0:T(8,128)(2,1)S(1)}, u32[]{:S(2)}, u32[]{:S(2)}) collective-permute-start(bf16[8,2048]{1,0:T(8,128)(2,1)} %get-tuple-element.55.refs_0_), channel_id=1, source_target_pairs={{0,16},{4,20},{8,24},{12,28},{16,0},{20,4},{24,8},{28,12},{1,17},{... | collective-permute-start | bytes 98312 | tf_op jit(solution)/shard_map/ppermute | solution.py:272
  55.6 10.3 %collective-permute-start.7 = (bf16[16,2048]{1,0:T(8,128)(2,1)}, bf16[16,2048]{1,0:T(8,128)(2,1)S(1)}, u32[]{:S(2)}, u32[]{:S(2)}) collective-permute-start(bf16[16,2048]{1,0:T(8,128)(2,1)} %get-tuple-element.47), channel_id=1, source_target_pairs={{0,4},{4,0},{8,12},{12,8},{16,20},{20,16},{24,28},{28,24},{1,5},{5... | collective-permute-start | bytes 196616 | tf_op jit(solution)/shard_map/ppermute | solution.py:272
  55.7 12.8 %collective-permute-start.8 = (bf16[16,2048]{1,0:T(8,128)(2,1)}, bf16[16,2048]{1,0:T(8,128)(2,1)S(1)}, u32[]{:S(2)}, u32[]{:S(2)}) collective-permute-start(bf16[16,2048]{1,0:T(8,128)(2,1)} %get-tuple-element.48), channel_id=1, source_target_pairs={{0,8},{4,12},{8,0},{12,4},{16,24},{20,28},{24,16},{28,20},{1,9},{5... | collective-permute-start | bytes 196616 | tf_op jit(solution)/shard_map/ppermute | solution.py:272
  57.4 5.7 %collective-permute-start.19 = (bf16[8,2048]{1,0:T(8,128)(2,1)S(1)}, bf16[8,2048]{1,0:T(8,128)(2,1)S(1)}, u32[]{:S(2)}, u32[]{:S(2)}) collective-permute-start(bf16[8,2048]{1,0:T(8,128)(2,1)S(1)} %copy-done.16), channel_id=1, source_target_pairs={{0,24},{4,28},{8,16},{12,20},{16,8},{20,12},{24,0},{28,4},{1,25},{... | collective-permute-start | bytes 98312 | tf_op jit(solution)/shard_map/ppermute | solution.py:272
  60.9 16.9 %collective-permute-start.9 = (bf16[16,2048]{1,0:T(8,128)(2,1)}, bf16[16,2048]{1,0:T(8,128)(2,1)S(1)}, u32[]{:S(2)}, u32[]{:S(2)}) collective-permute-start(bf16[16,2048]{1,0:T(8,128)(2,1)} %get-tuple-element.49), channel_id=1, source_target_pairs={{0,12},{4,8},{8,4},{12,0},{16,28},{20,24},{24,20},{28,16},{1,13},{... | collective-permute-start | bytes 196616 | tf_op jit(solution)/shard_map/ppermute | solution.py:272
  63.7 14.2 %collective-permute-start.10 = (bf16[16,2048]{1,0:T(8,128)(2,1)}, bf16[16,2048]{1,0:T(8,128)(2,1)S(1)}, u32[]{:S(2)}, u32[]{:S(2)}) collective-permute-start(bf16[16,2048]{1,0:T(8,128)(2,1)} %get-tuple-element.50), channel_id=1, source_target_pairs={{0,16},{4,20},{8,24},{12,28},{16,0},{20,4},{24,8},{28,12},{1,17},{... | collective-permute-start | bytes 196616 | tf_op jit(solution)/shard_map/ppermute | solution.py:272
  65.8 12.2 %collective-permute-start.11 = (bf16[16,2048]{1,0:T(8,128)(2,1)}, bf16[16,2048]{1,0:T(8,128)(2,1)S(1)}, u32[]{:S(2)}, u32[]{:S(2)}) collective-permute-start(bf16[16,2048]{1,0:T(8,128)(2,1)} %get-tuple-element.51), channel_id=1, source_target_pairs={{0,20},{4,16},{8,28},{12,24},{16,4},{20,0},{24,12},{28,8},{1,21},{... | collective-permute-start | bytes 196616 | tf_op jit(solution)/shard_map/ppermute | solution.py:272
  65.9 13.9 %collective-permute-start.12 = (bf16[16,2048]{1,0:T(8,128)(2,1)}, bf16[16,2048]{1,0:T(8,128)(2,1)S(1)}, u32[]{:S(2)}, u32[]{:S(2)}) collective-permute-start(bf16[16,2048]{1,0:T(8,128)(2,1)} %get-tuple-element.52), channel_id=1, source_target_pairs={{0,24},{4,28},{8,16},{12,20},{16,8},{20,12},{24,0},{28,4},{1,25},{... | collective-permute-start | bytes 196616 | tf_op jit(solution)/shard_map/ppermute | solution.py:272
  68.4 12.8 %collective-permute-start.13 = (bf16[16,2048]{1,0:T(8,128)(2,1)}, bf16[16,2048]{1,0:T(8,128)(2,1)S(1)}, u32[]{:S(2)}, u32[]{:S(2)}) collective-permute-start(bf16[16,2048]{1,0:T(8,128)(2,1)} %get-tuple-element.53), channel_id=1, source_target_pairs={{0,28},{4,24},{8,20},{12,16},{16,12},{20,8},{24,4},{28,0},{1,29},{... | collective-permute-start | bytes 196616 | tf_op jit(solution)/shard_map/ppermute | solution.py:272
  77.8 6.6 %collective-permute-start.21 = (bf16[8,2048]{1,0:T(8,128)(2,1)}, bf16[8,2048]{1,0:T(8,128)(2,1)S(1)}, u32[]{:S(2)}, u32[]{:S(2)}) collective-permute-start(bf16[8,2048]{1,0:T(8,128)(2,1)} %get-tuple-element.57), channel_id=1, source_target_pairs={{0,4},{4,0},{8,12},{12,8},{16,20},{20,16},{24,28},{28,24},{1,5},{5... | collective-permute-start | bytes 98312 | tf_op jit(solution)/shard_map/ppermute | solution.py:272
  77.9 9.1 %collective-permute-start.22 = (bf16[8,2048]{1,0:T(8,128)(2,1)}, bf16[8,2048]{1,0:T(8,128)(2,1)S(1)}, u32[]{:S(2)}, u32[]{:S(2)}) collective-permute-start(bf16[8,2048]{1,0:T(8,128)(2,1)} %get-tuple-element.58), channel_id=1, source_target_pairs={{0,8},{4,12},{8,0},{12,4},{16,24},{20,28},{24,16},{28,20},{1,9},{5... | collective-permute-start | bytes 98312 | tf_op jit(solution)/shard_map/ppermute | solution.py:272
  78.0 10.0 %collective-permute-start.23 = (bf16[8,2048]{1,0:T(8,128)(2,1)}, bf16[8,2048]{1,0:T(8,128)(2,1)S(1)}, u32[]{:S(2)}, u32[]{:S(2)}) collective-permute-start(bf16[8,2048]{1,0:T(8,128)(2,1)} %get-tuple-element.59), channel_id=1, source_target_pairs={{0,12},{4,8},{8,4},{12,0},{16,28},{20,24},{24,20},{28,16},{1,13},{... | collective-permute-start | bytes 98312 | tf_op jit(solution)/shard_map/ppermute | solution.py:272
  79.8 8.8 %collective-permute-start.24 = (bf16[8,2048]{1,0:T(8,128)(2,1)}, bf16[8,2048]{1,0:T(8,128)(2,1)S(1)}, u32[]{:S(2)}, u32[]{:S(2)}) collective-permute-start(bf16[8,2048]{1,0:T(8,128)(2,1)} %get-tuple-element.60), channel_id=1, source_target_pairs={{0,16},{4,20},{8,24},{12,28},{16,0},{20,4},{24,8},{28,12},{1,17},{... | collective-permute-start | bytes 98312 | tf_op jit(solution)/shard_map/ppermute | solution.py:272
  81.2 8.9 %collective-permute-start.25 = (bf16[8,2048]{1,0:T(8,128)(2,1)}, bf16[8,2048]{1,0:T(8,128)(2,1)S(1)}, u32[]{:S(2)}, u32[]{:S(2)}) collective-permute-start(bf16[8,2048]{1,0:T(8,128)(2,1)} %get-tuple-element.61), channel_id=1, source_target_pairs={{0,20},{4,16},{8,28},{12,24},{16,4},{20,0},{24,12},{28,8},{1,21},{... | collective-permute-start | bytes 98312 | tf_op jit(solution)/shard_map/ppermute | solution.py:272
  84.4 7.1 %collective-permute-start.26 = (bf16[8,2048]{1,0:T(8,128)(2,1)}, bf16[8,2048]{1,0:T(8,128)(2,1)S(1)}, u32[]{:S(2)}, u32[]{:S(2)}) collective-permute-start(bf16[8,2048]{1,0:T(8,128)(2,1)} %get-tuple-element.62), channel_id=1, source_target_pairs={{0,24},{4,28},{8,16},{12,20},{16,8},{20,12},{24,0},{28,4},{1,25},{... | collective-permute-start | bytes 98312 | tf_op jit(solution)/shard_map/ppermute | solution.py:272
  (43 other events, 339.3 us)

commit v2 on v1

v2 whole, which is shorter than its diff:
```python
import functools

import jax
import jax.numpy as jnp
from jax import lax
from jax.experimental import pallas as pl
from jax.experimental.pallas import tpu as pltpu
from jax.sharding import PartitionSpec as P

HEAD_WIDTH = 64
F32 = jnp.float32
BF16 = jnp.bfloat16
MIB = 1 << 20
HIGHEST = lax.Precision.HIGHEST
HBM = pl.BlockSpec(memory_space=pltpu.HBM)
VMEM = pl.BlockSpec(memory_space=pltpu.VMEM)


def iota(shape, dim):
    return lax.broadcasted_iota(jnp.int32, shape, dim)


def dot(a, b):
    return jnp.dot(a, b, preferred_element_type=F32)


def dot_exact(a, b):
    return jnp.dot(a, b, preferred_element_type=F32, precision=HIGHEST)


def halves(x):
    high = x.astype(BF16)
    return high, (x - high.astype(F32)).astype(BF16)


def rms_rows(floats, gain):
    return floats * lax.rsqrt(jnp.mean(floats * floats, axis=-1, keepdims=True) + 1e-06) * gain


def silu(x):
    return x * jax.nn.sigmoid(x)


def attention_kernel(
    tokens,
    gain,
    dec_off,
    cor_off,
    cor_fac,
    own_w,
    head_gain,
    routing,
    weights,
    second_gain,
    state,
    rec_m,
    key_m,
    val_m,
    dec_m,
    out_m,
    *refs,
):
    ahead = refs[: (len(refs) - 17) // 2]
    refs = refs[len(ahead) :]
    next_state, partial, pick, table, tokens_near, gain_near = refs[:6]
    ahead_near = refs[6 : 6 + len(ahead)]
    rows_ref, stage, rec_v, key_v, val_v, dec_v, out_v, mat_sem, in_sem, out_sem, far_sem = refs[
        6 + len(ahead) :
    ]
    seqs, heads, area = state.shape
    width = HEAD_WIDTH
    count = seqs * heads
    chunk = 8 * width
    steps = area // chunk
    mats = [
        pltpu.make_async_copy(source, target, mat_sem.at[n])
        for n, (source, target) in enumerate(
            [(key_m, key_v), (rec_m, rec_v), (val_m, val_v), (dec_m, dec_v), (out_m, out_v)]
        )
    ]
    loads = [
        pltpu.make_async_copy(
            state.at[:, :, pl.ds(j * chunk, chunk)],
            stage.at[:, :, pl.ds(j * chunk, chunk)],
            in_sem.at[j],
        )
        for j in range(steps)
    ]
    stores = [
        pltpu.make_async_copy(
            stage.at[:, :, pl.ds(j * chunk, chunk)],
            next_state.at[:, :, pl.ds(j * chunk, chunk)],
            out_sem.at[j],
        )
        for j in range(steps)
    ]
    fetches = [
        pltpu.make_async_copy(source, target, far_sem.at[n])
        for n, (source, target) in enumerate(zip(ahead, ahead_near))
    ]
    for copy in [*mats[:4], *loads, mats[4], *fetches]:
        copy.start()
    route_tables(routing, weights, pick, table)
    tokens_near[...] = tokens[...]
    gain_near[...] = second_gain[...]
    normed = rms_rows(tokens[...].astype(F32), gain[...]).astype(BF16)
    for copy in mats[:4]:
        copy.wait()
    keys = dot(normed, key_v[...])
    rec = dot(normed, rec_v[...])
    vals = dot(normed, val_v[...])
    decay = jnp.exp(-jnp.exp(dec_off[...] + dot(normed, dec_v[...])))
    rate = jax.nn.sigmoid(cor_off[...] + cor_fac[...] * keys)
    key_in = keys * rate

    def by_head(x):
        return jnp.concatenate([x[:, h * width : (h + 1) * width] for h in range(heads)], axis=0)

    keys_h = by_head(keys)
    unit = (
        keys_h
        * lax.rsqrt(jnp.mean(keys_h * keys_h, axis=-1, keepdims=True) + 1e-06)
        * width ** (-0.5)
    )
    erase = unit * by_head(rate)
    rec_h = by_head(rec)
    key_in_h = by_head(key_in)
    vals_h = by_head(vals)
    decay_h = by_head(decay)
    own = jnp.sum(by_head(rec * key_in * own_w[...]), axis=-1, keepdims=True)
    erase_dot = jnp.sum(erase * rec_h, axis=-1, keepdims=True)
    write_dot = jnp.sum(key_in_h * rec_h, axis=-1, keepdims=True)
    row = iota((count, count), 0)
    col = iota((count, count), 1)
    to_seq = (col == (row % heads) * seqs + row // heads).astype(F32)
    to_head = (row == (col % heads) * seqs + col // heads).astype(F32)
    packed = dot_exact(
        to_seq,
        jnp.concatenate([unit, decay_h * rec_h, decay_h, erase, key_in_h, vals_h], axis=1),
    )

    def twice(n):
        part = packed[:, n * width : (n + 1) * width]
        return jnp.concatenate([part, part], axis=1)

    def wide(n):
        return jnp.concatenate([twice(n)] * (chunk // (2 * width)), axis=1)

    unit_w = wide(0)
    read_w = wide(1)
    sums = jnp.zeros((count, 2 * width), F32)
    lane = iota((chunk, 2 * width), 0) // width
    slot = iota((chunk, 2 * width), 1)
    for j in range(steps):
        part = slice(j * chunk, (j + 1) * chunk)
        loads[j].wait()
        for b in range(seqs):
            rows_ref[b * heads : (b + 1) * heads, part] = stage[b, :, part]
        block = rows_ref[:, part]
        left = (slot == lane + 8 * j).astype(F32).astype(BF16)
        right = (slot == lane + (8 * j + width)).astype(F32).astype(BF16)
        a_hi, a_lo = halves(block * unit_w)
        b_hi, b_lo = halves(block * read_w)
        sums = sums + (dot(a_hi, left) + dot(a_lo, left)) + (dot(b_hi, right) + dot(b_lo, right))
    removed_hi, removed_lo = halves(sums[:, :width])
    removed_x = jnp.concatenate([removed_hi, removed_lo], axis=1)
    vals_hi, vals_lo = halves(packed[:, 5 * width : 6 * width])
    vals_x = jnp.concatenate([vals_hi, vals_lo], axis=1)
    sums_h = dot_exact(to_head, sums)
    read = sums_h[:, width:] - sums_h[:, :width] * erase_dot + vals_h * write_dot
    center = jnp.mean(read, axis=-1, keepdims=True)
    shifted = read - center
    spread_sq = jnp.mean(shifted * shifted, axis=-1, keepdims=True)
    normal = shifted * lax.rsqrt(spread_sq + 0.00064)
    extra = own * vals_h

    def by_lane(x):
        return jnp.concatenate([x[h * seqs : (h + 1) * seqs] for h in range(heads)], axis=1)

    heads_out = (by_lane(normal) * head_gain[...] + by_lane(extra)).astype(BF16)
    mats[4].wait()
    partial[...] = dot(heads_out, out_v[...]).astype(BF16)
    decay_w = wide(2)
    erase_w = wide(3)
    key_w = wide(4)
    source = iota((2 * width, chunk), 0) % width
    target = iota((2 * width, chunk), 1) // width
    for j in range(steps):
        part = slice(j * chunk, (j + 1) * chunk)
        spread = (source == target + 8 * j).astype(F32).astype(BF16)
        rows_ref[:, part] = (
            rows_ref[:, part] * decay_w
            - dot(removed_x, spread) * erase_w
            + dot(vals_x, spread) * key_w
        )
        for b in range(seqs):
            stage[b, :, part] = rows_ref[b * heads : (b + 1) * heads, part]
        stores[j].start()
    for copy in [*fetches, *stores]:
        copy.wait()


def lane_order(seqs):
    per_lane = seqs // lax.axis_size("tp")
    row = iota((seqs, seqs), 0)
    shuffled = ((row // per_lane) ^ lax.axis_index("tp")) * per_lane + row % per_lane
    return (iota((seqs, seqs), 1) == shuffled).astype(F32)


def route_tables(routing, weights, pick, table):
    slots, seqs = pick.shape
    me = lax.axis_index("ep")
    capacity = slots // lax.axis_size("ep")
    slot_row = iota((slots, seqs), 0)
    expert = ((slot_row // capacity) ^ me).astype(F32)
    place_in = (slot_row % capacity).astype(F32)
    every = routing.shape[1]
    mine = iota((every, seqs), 0) == iota((every, seqs), 1) + me * seqs
    routes = dot(routing[...].astype(F32).astype(BF16), mine.astype(F32).astype(BF16))
    chosen = jnp.zeros((slots, seqs), F32)
    weighted = jnp.zeros((slots, seqs), F32)
    for k in range(routing.shape[0]):
        hit = (routes[k : k + 1, :] == expert).astype(F32)
        chosen = chosen + hit
        weighted = weighted + hit * weights[k : k + 1, :]
    earlier = (iota((seqs, seqs), 0) < iota((seqs, seqs), 1)).astype(F32).astype(BF16)
    before = dot(chosen.astype(BF16), earlier)
    here = (before == place_in).astype(F32)
    pick[...] = (chosen * here).astype(BF16)
    table[...] = lax.dot_general(
        lane_order(seqs),
        weighted * here,
        (((1,), (1,)), ((), ())),
        precision=HIGHEST,
        preferred_element_type=F32,
    )


def dispatch_kernel(parts, tokens, gain, pick, own_hidden, *sends):
    seqs, _ = tokens.shape
    groups = len(sends)
    per_lane = own_hidden.shape[0]
    capacity = sends[0].shape[0] - per_lane
    total = parts[0].astype(F32)
    for n in range(1, parts.shape[0]):
        total = total + parts[n].astype(F32)
    hidden = tokens[...].astype(F32) + total
    rows = rms_rows(hidden, gain[...]).astype(BF16)
    sent = dot(pick[...], rows).astype(BF16)
    mine = lane_order(seqs)[:per_lane]
    own_hidden[...] = dot_exact(mine, hidden)
    own_rows = dot(mine.astype(BF16), rows).astype(BF16)
    for send, k in zip(sends, peers(groups)):
        send[:capacity, :] = sent[k * capacity : (k + 1) * capacity]
        send[capacity:, :] = own_rows


def dot_nt(a, b):
    return lax.dot_general(a, b, (((1,), (1,)), ((), ())), preferred_element_type=F32)


def units_kernel(groups, capacity, tile, *refs):
    rows = refs[:groups]
    gate, up, down, dense_gate, dense_up, dense_down = refs[groups : groups + 6]
    outs = refs[groups + 6 : 2 * groups + 6]
    routed, shared = refs[-2:]
    per_lane = rows[0].shape[0] - capacity
    for k in range(groups):
        block = rows[k][...].astype(F32)
        routed[k * capacity : (k + 1) * capacity, :] = block[:capacity]
        shared[k * per_lane : (k + 1) * per_lane, :] = block[capacity:]
    y = shared[...].astype(BF16)
    dense_hidden = (silu(dot_nt(y, dense_gate[...])) * dot_nt(y, dense_up[...])).astype(BF16)
    shared[...] = dot(dense_hidden, dense_down[...])
    x = routed[...].astype(BF16)
    total = jnp.zeros(routed.shape, F32)
    for j in range(gate.shape[2] // tile):
        part = pl.ds(j * tile, tile)
        hidden = (silu(dot(x, gate[0, :, part])) * dot(x, up[0, :, part])).astype(BF16)
        total = total + dot(hidden, down[0, part, :])
    for k in range(groups):
        outs[k][:capacity, :] = total[k * capacity : (k + 1) * capacity].astype(BF16)
        outs[k][capacity:, :] = shared[k * per_lane : (k + 1) * per_lane, :].astype(BF16)


def combine_kernel(groups, table, *refs):
    rows = refs[:groups]
    own, dense = refs[groups : groups + 2]
    sends = refs[groups + 2 : -1]
    gathered = refs[-1]
    per_lane = own.shape[0]
    capacity = rows[0].shape[0] - per_lane
    block = jnp.zeros(own.shape, F32)
    for message, k in zip(rows, peers(groups)):
        values = message[...].astype(F32)
        gathered[k * capacity : (k + 1) * capacity, :] = values[:capacity]
        block = block + values[capacity:]
    dense[...] = block
    x = gathered[...].astype(BF16)
    high, low = halves(table[...])
    result = dot(high, x) + dot(low, x)
    own[...] = result[:per_lane]
    for send, k in zip(sends, peers(len(sends) + 1)[1:]):
        send[...] = result[k * per_lane : (k + 1) * per_lane].astype(BF16)


def final_kernel(hidden, moe, dense, offset, *refs):
    total = moe[...]
    for other in refs[:-1]:
        total = total + other[...].astype(F32)
    out = refs[-1]
    out[...] = (hidden[...] + total + jax.nn.sigmoid(offset[...]) * dense[...]).astype(BF16)


def like(shape, dtype):
    return jax.ShapeDtypeStruct(shape, dtype)


def near(shape, dtype):
    return pltpu.VMEM(shape, dtype)


def far(arrays):
    return [pltpu.with_memory_space_constraint(x, pltpu.HBM) for x in arrays]


def bring(arrays):
    return [pltpu.with_memory_space_constraint(x, pltpu.VMEM) for x in arrays]


def peers(size):
    return sorted(range(size), key=lambda k: -k.bit_length() if k else -size)


def exchange(arrays, axis):
    size = lax.axis_size(axis)
    return [
        lax.ppermute(array, axis, [(i, i ^ k) for i in range(size)]) if k else array
        for k, array in zip(peers(size), arrays)
    ]


def local(
    tokens,
    recurrent_head_state,
    first_norm_gain,
    receptance_matrix,
    key_matrix,
    value_matrix,
    decay_matrix,
    decay_offset,
    correction_offset,
    correction_key_factor,
    own_term_weight,
    head_norm_gain,
    output_matrix,
    second_norm_gain,
    routing,
    routing_weight,
    expert_gate_weight,
    expert_up_weight,
    expert_down_weight,
    dense_gate_weight,
    dense_up_weight,
    dense_down_weight,
    dense_gate_offset,
):
    seqs, width = tokens.shape
    heads, area = recurrent_head_state.shape[1:]
    groups = lax.axis_size("ep")
    lanes = lax.axis_size("tp")
    per_lane = seqs // lanes
    local_experts, _, units = expert_gate_weight.shape
    assert local_experts == 1
    capacity = 2 * seqs * routing.shape[1] // groups

    def row(x):
        return x.reshape(1, -1)

    ahead = []
    steps = area // (8 * HEAD_WIDTH)
    next_state, partial, pick, table, tokens_near, gain_near, *ahead = pl.pallas_call(
        attention_kernel,
        out_shape=(
            like(recurrent_head_state.shape, F32),
            near((seqs, width), BF16),
            near((groups * capacity, seqs), BF16),
            near((seqs, groups * capacity), F32),
            near((seqs, width), BF16),
            near((1, width), F32),
            *[near(x.shape, x.dtype) for x in ahead],
        ),
        in_specs=[VMEM] * 10 + [HBM] * (6 + len(ahead)),
        out_specs=[HBM] + [VMEM] * (5 + len(ahead)),
        scratch_shapes=[
            pltpu.VMEM((seqs * heads, area), F32),
            pltpu.VMEM((seqs, heads, area), F32),
            *[pltpu.VMEM(receptance_matrix.shape, BF16)] * 4,
            pltpu.VMEM(output_matrix.shape, BF16),
            pltpu.SemaphoreType.DMA((5,)),
            pltpu.SemaphoreType.DMA((steps,)),
            pltpu.SemaphoreType.DMA((steps,)),
            pltpu.SemaphoreType.DMA((1,)),
        ],
        compiler_params=pltpu.CompilerParams(vmem_limit_bytes=54 * MIB),
        name="attention",
    )(
        *far(
            [
                tokens,
                row(first_norm_gain),
                row(decay_offset),
                row(correction_offset),
                row(correction_key_factor),
                row(own_term_weight),
                row(head_norm_gain),
                routing.T,
                routing_weight.T,
                row(second_norm_gain),
                recurrent_head_state,
                receptance_matrix,
                key_matrix,
                value_matrix,
                decay_matrix,
                output_matrix,
                *ahead,
            ]
        )
    )
    parts = lax.all_gather(partial, "tp", axis=0, tiled=False)
    message = near((capacity + per_lane, width), BF16)
    own_hidden, *sends = pl.pallas_call(
        dispatch_kernel,
        out_shape=(near((per_lane, width), F32), *[message] * groups),
        in_specs=[VMEM] * 4,
        out_specs=[VMEM] * (1 + groups),
        compiler_params=pltpu.CompilerParams(vmem_limit_bytes=8 * MIB),
        cost_estimate=pl.CostEstimate(flops=20 * 10**9, bytes_accessed=1 << 20, transcendentals=0),
        name="dispatch",
    )(*bring([parts, tokens_near, gain_near, pick]))
    received = exchange(sends, "ep")
    computed = pl.pallas_call(
        functools.partial(units_kernel, groups, capacity, min(256, units)),
        out_shape=[message] * groups,
        in_specs=[VMEM] * (groups + 6),
        out_specs=[VMEM] * groups,
        scratch_shapes=[
            pltpu.VMEM((groups * capacity, width), F32),
            pltpu.VMEM((groups * per_lane, width), F32),
        ],
        compiler_params=pltpu.CompilerParams(vmem_limit_bytes=14 * MIB),
        name="units",
    )(
        *bring(received),
        *bring([expert_gate_weight, expert_up_weight, expert_down_weight]),
        *bring([dense_gate_weight.T, dense_up_weight.T, dense_down_weight]),
    )
    returned = exchange(computed, "ep")
    moe_own, dense_sum, *moe_sends = pl.pallas_call(
        functools.partial(combine_kernel, groups),
        out_shape=[near((per_lane, width), F32)] * 2 + [near((per_lane, width), BF16)] * (lanes - 1),
        in_specs=[VMEM] * (groups + 1),
        out_specs=[VMEM] * (lanes + 1),
        scratch_shapes=[pltpu.VMEM((groups * capacity, width), F32)],
        compiler_params=pltpu.CompilerParams(vmem_limit_bytes=8 * MIB),
        name="combine",
    )(*bring([table, *returned]))
    moe_in = exchange([moe_own] + moe_sends, "tp")
    layer_out = pl.pallas_call(
        final_kernel,
        out_shape=like((per_lane, width), BF16),
        in_specs=[VMEM] * (3 + lanes),
        out_specs=VMEM,
        compiler_params=pltpu.CompilerParams(vmem_limit_bytes=4 * MIB),
        name="final",
    )(*bring([own_hidden, moe_in[0], dense_sum, row(dense_gate_offset), *moe_in[1:]]))
    return (layer_out, next_state)


def solution(mesh):
    return jax.shard_map(
        local,
        mesh=mesh,
        in_specs=(
            P("ep", None),
            P("ep", "tp", None),
            P(),
            P(None, "tp"),
            P(None, "tp"),
            P(None, "tp"),
            P(None, "tp"),
            P("tp"),
            P("tp"),
            P("tp"),
            P("tp"),
            P("tp"),
            P("tp", None),
            P(),
            P(),
            P("ep", None),
            P("ep", None, "tp"),
            P("ep", None, "tp"),
            P("ep", "tp", None),
            P(None, "ep"),
            P(None, "ep"),
            P("ep", None),
            P(),
        ),
        out_specs=(P(("ep", "tp"), None), P("ep", "tp", None)),
        check_vma=False,
    )
```

time: 97.7 us -> 73.6 us (0.75)
  starting transfers between devices: 40.5 us -> 18.6 us
  waiting for transfers between devices: 6.96 us -> 27.3 us
  Pallas kernels: 28.2 us -> 15.2 us
  local copies, waits for them, and re-layouts: 7.04 us -> 0.04 us
  blocking collectives: 13.1 us -> 11.5 us
    ppermute x31 -> x17, starting transfers between devices: 40.5 us -> 18.6 us  [exchange(): lax.ppermute(array, axis, [(i, i ^ k) for i in range(size)])]
    ppermute x31 -> x17, waiting for transfers between devices: 6.96 us -> 27.3 us  [exchange(): lax.ppermute(array, axis, [(i, i ^ k) for i in range(size)])]
    pallas_call x5 -> x4, Pallas kernels: 18.3 us -> 4.94 us  [the longest x1 3.38 us: local(): pl.pallas_call(functools.partial(units_kernel, groups, capacity, min(256,...]
    unnamed x76 -> x14, local copies, waits for them, and re-layouts: 7.04 us -> 0.04 us
    all_gather x1, blocking collectives: 13.1 us -> 11.5 us  [local(): parts = lax.all_gather(partial, 'tp', axis=0, tiled=False)]
  transfers between devices with their start and end apart: 31 -> 17, of which waited for: 6 -> 10; matrix products, arithmetic and copies ran while one was open for 3% -> 0% of each run, Pallas kernels for 14% -> 0%
where the time goes in v2:
time: 73.6 us; the launch traced here: 73.4 us
  waiting for transfers between devices  27.3 us (37%)
  starting transfers between devices  18.6 us (25%)
  Pallas kernels  15.2 us (21%)
  blocking collectives  11.5 us (16%)
  between operations  0.77 us (1%)
    ppermute x17, waiting for transfers between devices, exchange(): lax.ppermute(array, axis, [(i, i ^ k) for i in range(size)])  27.3 us
    ppermute x17, starting transfers between devices, exchange(): lax.ppermute(array, axis, [(i, i ^ k) for i in range(size)])  18.6 us
    all_gather x1, blocking collectives, local(): parts = lax.all_gather(partial, 'tp', axis=0, tiled=False)  11.5 us
    pallas_call x1, Pallas kernels, local(): pl.pallas_call(attention_kernel, out_shape=(like(recurrent_head_state.sha...  10.2 us
    pallas_call x1, Pallas kernels, local(): pl.pallas_call(functools.partial(units_kernel, groups, capacity, min(256,...  3.38 us
  transfers between devices with their start and end apart: 17, of which 10 were waited for; matrix products, arithmetic and copies ran while one was open for 0% of the time, Pallas kernels for 0%

profile of v2, /device:TPU:0, one launch (start us, length us, event | category | flops | bytes accessed | tf_op | source)
XLA Modules:
  0.0 73.4 jit_solution(2163823716574481153)
XLA Ops:
  0.6 10.2 %attention.1 = (f32[32,4,4096]{2,1,0:T(4,128)}, bf16[32,2048]{1,0:T(8,128)(2,1)S(1)}, bf16[128,32]{1,0:T(8,128)(2,1)S(1)}, f32[32,128]{1,0:T(8,128)S(1)}, bf16[3...) custom-call(bf16[32,2048]{1,0:T(8,128)(2,1)} %tokens.1, f32[1,2048]{1,0:T(1,128)} %bitcast.17, f32[1,256]{1,0:T(1,128)} %bitcast.20, ...), custom_call_target="tpu_custom_call" | custom-call | tf_op jit(solution)/shard_map/attention/pallas_call | solution.py:382
  10.9 11.5 %all-gather = bf16[128,2048]{1,0:T(8,128)(2,1)S(1)} all-gather(bf16[32,2048]{1,0:T(8,128)(2,1)S(1)} %get-tuple-element.30), channel_id=2, replica_groups=mesh['ep'=8,'tp'=4] {'tp'}, dimensions={0}, use_global_device_ids=true | all-gather | bytes 655360 | tf_op jit(solution)/shard_map/all_gather | solution.py:430
  22.4 0.6 dispatch.1
  23.1 2.7 %collective-permute-start = (bf16[24,2048]{1,0:T(8,128)(2,1)S(1)}, bf16[24,2048]{1,0:T(8,128)(2,1)S(1)}, u32[]{:S(2)}, u32[]{:S(2)}) collective-permute-start(bf16[24,2048]{1,0:T(8,128)(2,1)S(1)} %get-tuple-element.37), channel_id=1, source_target_pairs={{0,16},{4,20},{8,24},{12,28},{16,0},{20,4},{24,8},{28,12},{1,17},{... | collective-permute-start | bytes 294920 | tf_op jit(solution)/shard_map/ppermute | solution.py:338
  25.7 1.4 %collective-permute-start.2 = (bf16[24,2048]{1,0:T(8,128)(2,1)S(1)}, bf16[24,2048]{1,0:T(8,128)(2,1)S(1)}, u32[]{:S(2)}, u32[]{:S(2)}) collective-permute-start(bf16[24,2048]{1,0:T(8,128)(2,1)S(1)} %get-tuple-element.39), channel_id=1, source_target_pairs={{0,24},{4,28},{8,16},{12,20},{16,8},{20,12},{24,0},{28,4},{1,25},{... | collective-permute-start | bytes 294920 | tf_op jit(solution)/shard_map/ppermute | solution.py:338
  27.1 2.3 %collective-permute-start.3 = (bf16[24,2048]{1,0:T(8,128)(2,1)S(1)}, bf16[24,2048]{1,0:T(8,128)(2,1)S(1)}, u32[]{:S(2)}, u32[]{:S(2)}) collective-permute-start(bf16[24,2048]{1,0:T(8,128)(2,1)S(1)} %get-tuple-element.40), channel_id=1, source_target_pairs={{0,28},{4,24},{8,20},{12,16},{16,12},{20,8},{24,4},{28,0},{1,29},{... | collective-permute-start | bytes 294920 | tf_op jit(solution)/shard_map/ppermute | solution.py:338
  29.4 1.6 %collective-permute-start.5 = (bf16[24,2048]{1,0:T(8,128)(2,1)S(1)}, bf16[24,2048]{1,0:T(8,128)(2,1)S(1)}, u32[]{:S(2)}, u32[]{:S(2)}) collective-permute-start(bf16[24,2048]{1,0:T(8,128)(2,1)S(1)} %get-tuple-element.42), channel_id=1, source_target_pairs={{0,12},{4,8},{8,4},{12,0},{16,28},{20,24},{24,20},{28,16},{1,13},{... | collective-permute-start | bytes 294920 | tf_op jit(solution)/shard_map/ppermute | solution.py:338
  31.0 7.2 %collective-permute-done.1.refs_2_ = bf16[24,2048]{1,0:T(8,128)(2,1)S(1)} collective-permute-done((bf16[24,2048]{1,0:T(8,128)(2,1)S(1)}, bf16[24,2048]{1,0:T(8,128)(2,1)S(1)}, u32[]{:S(2)}, u32[]{:S(2)}) %collective-permute-start.1) | collective-permute-done | bytes 98336 | tf_op jit(solution)/shard_map/ppermute | solution.py:338
  38.2 2.1 %collective-permute-done.4.refs_5_ = bf16[24,2048]{1,0:T(8,128)(2,1)S(1)} collective-permute-done((bf16[24,2048]{1,0:T(8,128)(2,1)S(1)}, bf16[24,2048]{1,0:T(8,128)(2,1)S(1)}, u32[]{:S(2)}, u32[]{:S(2)}) %collective-permute-start.4) | collective-permute-done | bytes 98336 | tf_op jit(solution)/shard_map/ppermute | solution.py:338
  40.3 1.6 %collective-permute-done.5.refs_6_ = bf16[24,2048]{1,0:T(8,128)(2,1)S(1)} collective-permute-done((bf16[24,2048]{1,0:T(8,128)(2,1)S(1)}, bf16[24,2048]{1,0:T(8,128)(2,1)S(1)}, u32[]{:S(2)}, u32[]{:S(2)}) %collective-permute-start.5) | collective-permute-done | bytes 98336 | tf_op jit(solution)/shard_map/ppermute | solution.py:338
  42.0 3.4 %units.1 = (bf16[24,2048]{1,0:T(8,128)(2,1)S(1)}, bf16[24,2048]{1,0:T(8,128)(2,1)S(1)}, bf16[24,2048]{1,0:T(8,128)(2,1)S(1)}, bf16[24,2048]{1,0:T(8,128)(2,1)S(1...) custom-call(bf16[24,2048]{1,0:T(8,128)(2,1)S(1)} %get-tuple-element., ...), custom_call_target="tpu_custom_call" | custom-call | tf_op jit(solution)/shard_map/units/pallas_call | solution.py:442
  45.4 1.9 %collective-permute-start.7 = (bf16[24,2048]{1,0:T(8,128)(2,1)S(1)}, bf16[24,2048]{1,0:T(8,128)(2,1)S(1)}, u32[]{:S(2)}, u32[]{:S(2)}) collective-permute-start(bf16[24,2048]{1,0:T(8,128)(2,1)S(1)} %get-tuple-element.45), channel_id=1, source_target_pairs={{0,16},{4,20},{8,24},{12,28},{16,0},{20,4},{24,8},{28,12},{1,17},{... | collective-permute-start | bytes 294920 | tf_op jit(solution)/shard_map/ppermute | solution.py:338
  47.8 2.8 %collective-permute-start.9 = (bf16[24,2048]{1,0:T(8,128)(2,1)S(1)}, bf16[24,2048]{1,0:T(8,128)(2,1)S(1)}, u32[]{:S(2)}, u32[]{:S(2)}) collective-permute-start(bf16[24,2048]{1,0:T(8,128)(2,1)S(1)} %get-tuple-element.47), channel_id=1, source_target_pairs={{0,24},{4,28},{8,16},{12,20},{16,8},{20,12},{24,0},{28,4},{1,25},{... | collective-permute-start | bytes 294920 | tf_op jit(solution)/shard_map/ppermute | solution.py:338
  50.6 1.0 %collective-permute-start.10 = (bf16[24,2048]{1,0:T(8,128)(2,1)S(1)}, bf16[24,2048]{1,0:T(8,128)(2,1)S(1)}, u32[]{:S(2)}, u32[]{:S(2)}) collective-permute-start(bf16[24,2048]{1,0:T(8,128)(2,1)S(1)} %get-tuple-element.48), channel_id=1, source_target_pairs={{0,28},{4,24},{8,20},{12,16},{16,12},{20,8},{24,4},{28,0},{1,29},{... | collective-permute-start | bytes 294920 | tf_op jit(solution)/shard_map/ppermute | solution.py:338
  51.6 8.6 %collective-permute-done.7.refs_1_ = bf16[24,2048]{1,0:T(8,128)(2,1)S(1)} collective-permute-done((bf16[24,2048]{1,0:T(8,128)(2,1)S(1)}, bf16[24,2048]{1,0:T(8,128)(2,1)S(1)}, u32[]{:S(2)}, u32[]{:S(2)}) %collective-permute-start.7) | collective-permute-done | bytes 98336 | tf_op jit(solution)/shard_map/ppermute | solution.py:338
  60.2 1.0 %collective-permute-done.8.refs_2_ = bf16[24,2048]{1,0:T(8,128)(2,1)S(1)} collective-permute-done((bf16[24,2048]{1,0:T(8,128)(2,1)S(1)}, bf16[24,2048]{1,0:T(8,128)(2,1)S(1)}, u32[]{:S(2)}, u32[]{:S(2)}) %collective-permute-start.8) | collective-permute-done | bytes 98336 | tf_op jit(solution)/shard_map/ppermute | solution.py:338
  61.2 0.9 %collective-permute-start.13 = (bf16[24,2048]{1,0:T(8,128)(2,1)S(1)}, bf16[24,2048]{1,0:T(8,128)(2,1)S(1)}, u32[]{:S(2)}, u32[]{:S(2)}) collective-permute-start(bf16[24,2048]{1,0:T(8,128)(2,1)S(1)} %get-tuple-element.51), channel_id=1, source_target_pairs={{0,4},{4,0},{8,12},{12,8},{16,20},{20,16},{24,28},{28,24},{1,5},{5... | collective-permute-start | bytes 294920 | tf_op jit(solution)/shard_map/ppermute | solution.py:338
  62.1 1.8 %collective-permute-done.11.refs_5_ = bf16[24,2048]{1,0:T(8,128)(2,1)S(1)} collective-permute-done((bf16[24,2048]{1,0:T(8,128)(2,1)S(1)}, bf16[24,2048]{1,0:T(8,128)(2,1)S(1)}, u32[]{:S(2)}, u32[]{:S(2)}) %collective-permute-start.11) | collective-permute-done | bytes 98336 | tf_op jit(solution)/shard_map/ppermute | solution.py:338
  63.9 1.6 %collective-permute-done.12.refs_6_ = bf16[24,2048]{1,0:T(8,128)(2,1)S(1)} collective-permute-done((bf16[24,2048]{1,0:T(8,128)(2,1)S(1)}, bf16[24,2048]{1,0:T(8,128)(2,1)S(1)}, u32[]{:S(2)}, u32[]{:S(2)}) %collective-permute-start.12) | collective-permute-done | bytes 98336 | tf_op jit(solution)/shard_map/ppermute | solution.py:338
  65.8 1.6 %collective-permute-start.14 = (bf16[8,2048]{1,0:T(8,128)(2,1)S(1)}, bf16[8,2048]{1,0:T(8,128)(2,1)S(1)}, u32[]{:S(2)}, u32[]{:S(2)}) collective-permute-start(bf16[8,2048]{1,0:T(8,128)(2,1)S(1)} %get-tuple-element.54), channel_id=1, source_target_pairs={{0,2},{1,3},{2,0},{3,1},{4,6},{5,7},{6,4},{7,5},{8,10},{9,11},{10,... | collective-permute-start | bytes 98312 | tf_op jit(solution)/shard_map/ppermute | solution.py:338
  67.4 1.5 %collective-permute-start.15 = (bf16[8,2048]{1,0:T(8,128)(2,1)S(1)}, bf16[8,2048]{1,0:T(8,128)(2,1)S(1)}, u32[]{:S(2)}, u32[]{:S(2)}) collective-permute-start(bf16[8,2048]{1,0:T(8,128)(2,1)S(1)} %get-tuple-element.55), channel_id=1, source_target_pairs={{0,3},{1,2},{2,1},{3,0},{4,7},{5,6},{6,5},{7,4},{8,11},{9,10},{10,... | collective-permute-start | bytes 98312 | tf_op jit(solution)/shard_map/ppermute | solution.py:338
  69.8 2.4 %collective-permute-done.15.refs_1_ = bf16[8,2048]{1,0:T(8,128)(2,1)S(1)} collective-permute-done((bf16[8,2048]{1,0:T(8,128)(2,1)S(1)}, bf16[8,2048]{1,0:T(8,128)(2,1)S(1)}, u32[]{:S(2)}, u32[]{:S(2)}) %collective-permute-start.15) | collective-permute-done | bytes 32800 | tf_op jit(solution)/shard_map/ppermute | solution.py:338
  72.2 0.6 collective-permute-done.16.refs_2_
  72.8 0.6 final.1
  (30 shorter events, 1.8 us)
Async XLA Ops:
  22.4 19.5 %copy-start = (bf16[1,2048,1024]{2,1,0:T(8,128)(2,1)S(1)}, bf16[1,2048,1024]{2,1,0:T(8,128)(2,1)}, u32[]{:S(2)}) copy-start(bf16[1,2048,1024]{2,1,0:T(8,128)(2,1)} %refs_8_.1) | copy-start | bytes 12582916
  22.4 19.5 %copy-start.1 = (bf16[1,2048,1024]{2,1,0:T(8,128)(2,1)S(1)}, bf16[1,2048,1024]{2,1,0:T(8,128)(2,1)}, u32[]{:S(2)}) copy-start(bf16[1,2048,1024]{2,1,0:T(8,128)(2,1)} %refs_9_.1) | copy-start | bytes 12582916
  22.4 19.5 %copy-start.2 = (bf16[1,1024,2048]{2,1,0:T(8,128)(2,1)S(1)}, bf16[1,1024,2048]{2,1,0:T(8,128)(2,1)}, u32[]{:S(2)}) copy-start(bf16[1,1024,2048]{2,1,0:T(8,128)(2,1)} %refs_10_.1) | copy-start | bytes 12582916
  22.4 19.5 %copy-start.3 = (bf16[2048,352]{0,1:T(8,128)(2,1)S(1)}, bf16[2048,352]{0,1:T(8,128)(2,1)}, u32[]{:S(2)}) copy-start(bf16[2048,352]{0,1:T(8,128)(2,1)} %param.42) | copy-start | bytes 4325380
  22.4 19.5 %copy-start.4 = (bf16[2048,352]{0,1:T(8,128)(2,1)S(1)}, bf16[2048,352]{0,1:T(8,128)(2,1)}, u32[]{:S(2)}) copy-start(bf16[2048,352]{0,1:T(8,128)(2,1)} %param.43) | copy-start | bytes 4325380
  22.4 19.5 %copy-start.5 = (bf16[352,2048]{1,0:T(8,128)(2,1)S(1)}, bf16[352,2048]{1,0:T(8,128)(2,1)}, u32[]{:S(2)}) copy-start(bf16[352,2048]{1,0:T(8,128)(2,1)} %refs_13_.1) | copy-start | bytes 4325380
  23.1 6.3 %collective-permute-start = (bf16[24,2048]{1,0:T(8,128)(2,1)S(1)}, bf16[24,2048]{1,0:T(8,128)(2,1)S(1)}, u32[]{:S(2)}, u32[]{:S(2)}) collective-permute-start(bf16[24,2048]{1,0:T(8,128)(2,1)S(1)} %get-tuple-element.37), channel_id=1, source_target_pairs={{0,16},{4,20},{8,24},{12,28},{16,0},{20,4},{24,8},{28,12},{1,17},{... | collective-permute-start | bytes 294920 | tf_op jit(solution)/shard_map/ppermute | solution.py:338
  25.7 12.5 %collective-permute-start.1 = (bf16[24,2048]{1,0:T(8,128)(2,1)S(1)}, bf16[24,2048]{1,0:T(8,128)(2,1)S(1)}, u32[]{:S(2)}, u32[]{:S(2)}) collective-permute-start(bf16[24,2048]{1,0:T(8,128)(2,1)S(1)} %get-tuple-element.38), channel_id=1, source_target_pairs={{0,20},{4,16},{8,28},{12,24},{16,4},{20,0},{24,12},{28,8},{1,21},{... | collective-permute-start | bytes 294920 | tf_op jit(solution)/shard_map/ppermute | solution.py:338
  25.7 12.5 %collective-permute-start.2 = (bf16[24,2048]{1,0:T(8,128)(2,1)S(1)}, bf16[24,2048]{1,0:T(8,128)(2,1)S(1)}, u32[]{:S(2)}, u32[]{:S(2)}) collective-permute-start(bf16[24,2048]{1,0:T(8,128)(2,1)S(1)} %get-tuple-element.39), channel_id=1, source_target_pairs={{0,24},{4,28},{8,16},{12,20},{16,8},{20,12},{24,0},{28,4},{1,25},{... | collective-permute-start | bytes 294920 | tf_op jit(solution)/shard_map/ppermute | solution.py:338
  27.1 11.2 %collective-permute-start.3 = (bf16[24,2048]{1,0:T(8,128)(2,1)S(1)}, bf16[24,2048]{1,0:T(8,128)(2,1)S(1)}, u32[]{:S(2)}, u32[]{:S(2)}) collective-permute-start(bf16[24,2048]{1,0:T(8,128)(2,1)S(1)} %get-tuple-element.40), channel_id=1, source_target_pairs={{0,28},{4,24},{8,20},{12,16},{16,12},{20,8},{24,4},{28,0},{1,29},{... | collective-permute-start | bytes 294920 | tf_op jit(solution)/shard_map/ppermute | solution.py:338
  29.4 10.9 %collective-permute-start.4 = (bf16[24,2048]{1,0:T(8,128)(2,1)S(1)}, bf16[24,2048]{1,0:T(8,128)(2,1)S(1)}, u32[]{:S(2)}, u32[]{:S(2)}) collective-permute-start(bf16[24,2048]{1,0:T(8,128)(2,1)S(1)} %get-tuple-element.41), channel_id=1, source_target_pairs={{0,8},{4,12},{8,0},{12,4},{16,24},{20,28},{24,16},{28,20},{1,9},{5... | collective-permute-start | bytes 294920 | tf_op jit(solution)/shard_map/ppermute | solution.py:338
  29.4 12.5 %collective-permute-start.5 = (bf16[24,2048]{1,0:T(8,128)(2,1)S(1)}, bf16[24,2048]{1,0:T(8,128)(2,1)S(1)}, u32[]{:S(2)}, u32[]{:S(2)}) collective-permute-start(bf16[24,2048]{1,0:T(8,128)(2,1)S(1)} %get-tuple-element.42), channel_id=1, source_target_pairs={{0,12},{4,8},{8,4},{12,0},{16,28},{20,24},{24,20},{28,16},{1,13},{... | collective-permute-start | bytes 294920 | tf_op jit(solution)/shard_map/ppermute | solution.py:338
  38.2 3.7 %collective-permute-start.6 = (bf16[24,2048]{1,0:T(8,128)(2,1)S(1)}, bf16[24,2048]{1,0:T(8,128)(2,1)S(1)}, u32[]{:S(2)}, u32[]{:S(2)}) collective-permute-start(bf16[24,2048]{1,0:T(8,128)(2,1)S(1)} %get-tuple-element.43), channel_id=1, source_target_pairs={{0,4},{4,0},{8,12},{12,8},{16,20},{20,16},{24,28},{28,24},{1,5},{5... | collective-permute-start | bytes 294920 | tf_op jit(solution)/shard_map/ppermute | solution.py:338
  42.0 30.8 %copy-start.6 = (f32[2048]{0:T(1024)S(1)}, f32[2048]{0:T(1024)}, u32[]{:S(2)}) copy-start(f32[2048]{0:T(1024)} %param.45) | copy-start | bytes 24580
  45.4 14.9 %collective-permute-start.7 = (bf16[24,2048]{1,0:T(8,128)(2,1)S(1)}, bf16[24,2048]{1,0:T(8,128)(2,1)S(1)}, u32[]{:S(2)}, u32[]{:S(2)}) collective-permute-start(bf16[24,2048]{1,0:T(8,128)(2,1)S(1)} %get-tuple-element.45), channel_id=1, source_target_pairs={{0,16},{4,20},{8,24},{12,28},{16,0},{20,4},{24,8},{28,12},{1,17},{... | collective-permute-start | bytes 294920 | tf_op jit(solution)/shard_map/ppermute | solution.py:338
  47.2 14.0 %collective-permute-start.8 = (bf16[24,2048]{1,0:T(8,128)(2,1)S(1)}, bf16[24,2048]{1,0:T(8,128)(2,1)S(1)}, u32[]{:S(2)}, u32[]{:S(2)}) collective-permute-start(bf16[24,2048]{1,0:T(8,128)(2,1)S(1)} %get-tuple-element.46), channel_id=1, source_target_pairs={{0,20},{4,16},{8,28},{12,24},{16,4},{20,0},{24,12},{28,8},{1,21},{... | collective-permute-start | bytes 294920 | tf_op jit(solution)/shard_map/ppermute | solution.py:338
  47.8 14.3 %collective-permute-start.9 = (bf16[24,2048]{1,0:T(8,128)(2,1)S(1)}, bf16[24,2048]{1,0:T(8,128)(2,1)S(1)}, u32[]{:S(2)}, u32[]{:S(2)}) collective-permute-start(bf16[24,2048]{1,0:T(8,128)(2,1)S(1)} %get-tuple-element.47), channel_id=1, source_target_pairs={{0,24},{4,28},{8,16},{12,20},{16,8},{20,12},{24,0},{28,4},{1,25},{... | collective-permute-start | bytes 294920 | tf_op jit(solution)/shard_map/ppermute | solution.py:338
  50.6 11.5 %collective-permute-start.10 = (bf16[24,2048]{1,0:T(8,128)(2,1)S(1)}, bf16[24,2048]{1,0:T(8,128)(2,1)S(1)}, u32[]{:S(2)}, u32[]{:S(2)}) collective-permute-start(bf16[24,2048]{1,0:T(8,128)(2,1)S(1)} %get-tuple-element.48), channel_id=1, source_target_pairs={{0,28},{4,24},{8,20},{12,16},{16,12},{20,8},{24,4},{28,0},{1,29},{... | collective-permute-start | bytes 294920 | tf_op jit(solution)/shard_map/ppermute | solution.py:338
  51.6 12.3 %collective-permute-start.11 = (bf16[24,2048]{1,0:T(8,128)(2,1)S(1)}, bf16[24,2048]{1,0:T(8,128)(2,1)S(1)}, u32[]{:S(2)}, u32[]{:S(2)}) collective-permute-start(bf16[24,2048]{1,0:T(8,128)(2,1)S(1)} %get-tuple-element.49), channel_id=1, source_target_pairs={{0,8},{4,12},{8,0},{12,4},{16,24},{20,28},{24,16},{28,20},{1,9},{5... | collective-permute-start | bytes 294920 | tf_op jit(solution)/shard_map/ppermute | solution.py:338
  60.2 5.3 %collective-permute-start.12 = (bf16[24,2048]{1,0:T(8,128)(2,1)S(1)}, bf16[24,2048]{1,0:T(8,128)(2,1)S(1)}, u32[]{:S(2)}, u32[]{:S(2)}) collective-permute-start(bf16[24,2048]{1,0:T(8,128)(2,1)S(1)} %get-tuple-element.50), channel_id=1, source_target_pairs={{0,12},{4,8},{8,4},{12,0},{16,28},{20,24},{24,20},{28,16},{1,13},{... | collective-permute-start | bytes 294920 | tf_op jit(solution)/shard_map/ppermute | solution.py:338
  61.2 4.3 %collective-permute-start.13 = (bf16[24,2048]{1,0:T(8,128)(2,1)S(1)}, bf16[24,2048]{1,0:T(8,128)(2,1)S(1)}, u32[]{:S(2)}, u32[]{:S(2)}) collective-permute-start(bf16[24,2048]{1,0:T(8,128)(2,1)S(1)} %get-tuple-element.51), channel_id=1, source_target_pairs={{0,4},{4,0},{8,12},{12,8},{16,20},{20,16},{24,28},{28,24},{1,5},{5... | collective-permute-start | bytes 294920 | tf_op jit(solution)/shard_map/ppermute | solution.py:338
  65.8 4.0 %collective-permute-start.14 = (bf16[8,2048]{1,0:T(8,128)(2,1)S(1)}, bf16[8,2048]{1,0:T(8,128)(2,1)S(1)}, u32[]{:S(2)}, u32[]{:S(2)}) collective-permute-start(bf16[8,2048]{1,0:T(8,128)(2,1)S(1)} %get-tuple-element.54), channel_id=1, source_target_pairs={{0,2},{1,3},{2,0},{3,1},{4,6},{5,7},{6,4},{7,5},{8,10},{9,11},{10,... | collective-permute-start | bytes 98312 | tf_op jit(solution)/shard_map/ppermute | solution.py:338
  67.4 4.8 %collective-permute-start.15 = (bf16[8,2048]{1,0:T(8,128)(2,1)S(1)}, bf16[8,2048]{1,0:T(8,128)(2,1)S(1)}, u32[]{:S(2)}, u32[]{:S(2)}) collective-permute-start(bf16[8,2048]{1,0:T(8,128)(2,1)S(1)} %get-tuple-element.55), channel_id=1, source_target_pairs={{0,3},{1,2},{2,1},{3,0},{4,7},{5,6},{6,5},{7,4},{8,11},{9,10},{10,... | collective-permute-start | bytes 98312 | tf_op jit(solution)/shard_map/ppermute | solution.py:338
  68.8 3.9 %collective-permute-start.16 = (bf16[8,2048]{1,0:T(8,128)(2,1)S(1)}, bf16[8,2048]{1,0:T(8,128)(2,1)S(1)}, u32[]{:S(2)}, u32[]{:S(2)}) collective-permute-start(bf16[8,2048]{1,0:T(8,128)(2,1)S(1)} %get-tuple-element.56), channel_id=1, source_target_pairs={{0,1},{1,0},{2,3},{3,2},{4,5},{5,4},{6,7},{7,6},{8,9},{9,8},{10,11... | collective-permute-start | bytes 98312 | tf_op jit(solution)/shard_map/ppermute | solution.py:338

commit v3 on v2

--- a/solution.py
+++ b/solution.py
@@ -6,6 +6,7 @@
 from jax.experimental import pallas as pl
 from jax.experimental.pallas import tpu as pltpu
 from jax.sharding import PartitionSpec as P
+
 
 HEAD_WIDTH = 64
 F32 = jnp.float32
@@ -60,13 +61,8 @@
     out_m,
     *refs,
 ):
-    ahead = refs[: (len(refs) - 17) // 2]
-    refs = refs[len(ahead) :]
-    next_state, partial, pick, table, tokens_near, gain_near = refs[:6]
-    ahead_near = refs[6 : 6 + len(ahead)]
-    rows_ref, stage, rec_v, key_v, val_v, dec_v, out_v, mat_sem, in_sem, out_sem, far_sem = refs[
-        6 + len(ahead) :
-    ]
+    partial, pick, table, tokens_near, gain_near, rows_ref, packed_ref, removed_ref = refs[:8]
+    stage, rec_v, key_v, val_v, dec_v, out_v, mat_sem, in_sem = refs[8:]
     seqs, heads, area = state.shape
     width = HEAD_WIDTH
     count = seqs * heads
@@ -86,29 +82,19 @@
         )
         for j in range(steps)
     ]
-    stores = [
-        pltpu.make_async_copy(
-            stage.at[:, :, pl.ds(j * chunk, chunk)],
-            next_state.at[:, :, pl.ds(j * chunk, chunk)],
-            out_sem.at[j],
-        )
-        for j in range(steps)
-    ]
-    fetches = [
-        pltpu.make_async_copy(source, target, far_sem.at[n])
-        for n, (source, target) in enumerate(zip(ahead, ahead_near))
-    ]
-    for copy in [*mats[:4], *loads, mats[4], *fetches]:
+    for copy in [*mats[:4], *loads, mats[4]]:
         copy.start()
     route_tables(routing, weights, pick, table)
     tokens_near[...] = tokens[...]
     gain_near[...] = second_gain[...]
     normed = rms_rows(tokens[...].astype(F32), gain[...]).astype(BF16)
-    for copy in mats[:4]:
-        copy.wait()
+    mats[0].wait()
     keys = dot(normed, key_v[...])
+    mats[1].wait()
     rec = dot(normed, rec_v[...])
+    mats[2].wait()
     vals = dot(normed, val_v[...])
+    mats[3].wait()
     decay = jnp.exp(-jnp.exp(dec_off[...] + dot(normed, dec_v[...])))
     rate = jax.nn.sigmoid(cor_off[...] + cor_fac[...] * keys)
     key_in = keys * rate
@@ -162,10 +148,8 @@
         a_hi, a_lo = halves(block * unit_w)
         b_hi, b_lo = halves(block * read_w)
         sums = sums + (dot(a_hi, left) + dot(a_lo, left)) + (dot(b_hi, right) + dot(b_lo, right))
-    removed_hi, removed_lo = halves(sums[:, :width])
-    removed_x = jnp.concatenate([removed_hi, removed_lo], axis=1)
-    vals_hi, vals_lo = halves(packed[:, 5 * width : 6 * width])
-    vals_x = jnp.concatenate([vals_hi, vals_lo], axis=1)
+    packed_ref[...] = packed[:, 2 * width :]
+    removed_ref[...] = sums
     sums_h = dot_exact(to_head, sums)
     read = sums_h[:, width:] - sums_h[:, :width] * erase_dot + vals_h * write_dot
     center = jnp.mean(read, axis=-1, keepdims=True)
@@ -180,23 +164,48 @@
     heads_out = (by_lane(normal) * head_gain[...] + by_lane(extra)).astype(BF16)
     mats[4].wait()
     partial[...] = dot(heads_out, out_v[...]).astype(BF16)
-    decay_w = wide(2)
-    erase_w = wide(3)
-    key_w = wide(4)
+
+
+def update_kernel(rows_ref, packed_ref, removed_ref, next_state, stage, out_sem):
+    seqs, heads, area = next_state.shape
+    width = HEAD_WIDTH
+    chunk = 8 * width
+    steps = area // chunk
+    stores = [
+        pltpu.make_async_copy(
+            stage.at[:, :, pl.ds(j * chunk, chunk)],
+            next_state.at[:, :, pl.ds(j * chunk, chunk)],
+            out_sem.at[j],
+        )
+        for j in range(steps)
+    ]
+    packed = packed_ref[...]
+
+    def wide(n):
+        part = packed[:, n * width : (n + 1) * width]
+        return jnp.concatenate([part, part] * (chunk // (2 * width)), axis=1)
+
+    decay_w = wide(0)
+    erase_w = wide(1)
+    key_w = wide(2)
+    removed_hi, removed_lo = halves(removed_ref[:, :width])
+    removed_x = jnp.concatenate([removed_hi, removed_lo], axis=1)
+    vals_hi, vals_lo = halves(packed[:, 3 * width :])
+    vals_x = jnp.concatenate([vals_hi, vals_lo], axis=1)
     source = iota((2 * width, chunk), 0) % width
     target = iota((2 * width, chunk), 1) // width
     for j in range(steps):
         part = slice(j * chunk, (j + 1) * chunk)
         spread = (source == target + 8 * j).astype(F32).astype(BF16)
-        rows_ref[:, part] = (
+        block = (
             rows_ref[:, part] * decay_w
             - dot(removed_x, spread) * erase_w
             + dot(vals_x, spread) * key_w
         )
         for b in range(seqs):
-            stage[b, :, part] = rows_ref[b * heads : (b + 1) * heads, part]
+            stage[b, :, part] = block[b * heads : (b + 1) * heads]
         stores[j].start()
-    for copy in [*fetches, *stores]:
+    for copy in stores:
         copy.wait()
 
 
@@ -236,42 +245,38 @@
     )
 
 
-def dispatch_kernel(parts, tokens, gain, pick, own_hidden, *sends):
+def dispatch_kernel(lanes, *refs):
+    parts = refs[:lanes]
+    tokens, gain, pick, own_hidden, own_rows, *sends = refs[lanes:]
     seqs, _ = tokens.shape
     groups = len(sends)
     per_lane = own_hidden.shape[0]
-    capacity = sends[0].shape[0] - per_lane
-    total = parts[0].astype(F32)
-    for n in range(1, parts.shape[0]):
-        total = total + parts[n].astype(F32)
+    capacity = sends[0].shape[0]
+    total = parts[0][...].astype(F32)
+    for part in parts[1:]:
+        total = total + part[...].astype(F32)
     hidden = tokens[...].astype(F32) + total
     rows = rms_rows(hidden, gain[...]).astype(BF16)
     sent = dot(pick[...], rows).astype(BF16)
     mine = lane_order(seqs)[:per_lane]
     own_hidden[...] = dot_exact(mine, hidden)
-    own_rows = dot(mine.astype(BF16), rows).astype(BF16)
+    own_rows[...] = dot(mine.astype(BF16), rows).astype(BF16)
     for send, k in zip(sends, peers(groups)):
-        send[:capacity, :] = sent[k * capacity : (k + 1) * capacity]
-        send[capacity:, :] = own_rows
+        send[...] = sent[k * capacity : (k + 1) * capacity]
 
 
 def dot_nt(a, b):
     return lax.dot_general(a, b, (((1,), (1,)), ((), ())), preferred_element_type=F32)
 
 
-def units_kernel(groups, capacity, tile, *refs):
+def expert_kernel(groups, tile, *refs):
     rows = refs[:groups]
-    gate, up, down, dense_gate, dense_up, dense_down = refs[groups : groups + 6]
-    outs = refs[groups + 6 : 2 * groups + 6]
-    routed, shared = refs[-2:]
-    per_lane = rows[0].shape[0] - capacity
+    gate, up, down = refs[groups : groups + 3]
+    outs = refs[groups + 3 : 2 * groups + 3]
+    routed = refs[-1]
+    capacity = rows[0].shape[0]
     for k in range(groups):
-        block = rows[k][...].astype(F32)
-        routed[k * capacity : (k + 1) * capacity, :] = block[:capacity]
-        shared[k * per_lane : (k + 1) * per_lane, :] = block[capacity:]
-    y = shared[...].astype(BF16)
-    dense_hidden = (silu(dot_nt(y, dense_gate[...])) * dot_nt(y, dense_up[...])).astype(BF16)
-    shared[...] = dot(dense_hidden, dense_down[...])
+        routed[k * capacity : (k + 1) * capacity, :] = rows[k][...].astype(F32)
     x = routed[...].astype(BF16)
     total = jnp.zeros(routed.shape, F32)
     for j in range(gate.shape[2] // tile):
@@ -279,23 +284,33 @@
         hidden = (silu(dot(x, gate[0, :, part])) * dot(x, up[0, :, part])).astype(BF16)
         total = total + dot(hidden, down[0, part, :])
     for k in range(groups):
-        outs[k][:capacity, :] = total[k * capacity : (k + 1) * capacity].astype(BF16)
-        outs[k][capacity:, :] = shared[k * per_lane : (k + 1) * per_lane, :].astype(BF16)
+        outs[k][...] = total[k * capacity : (k + 1) * capacity].astype(BF16)
+
+
+def dense_kernel(groups, *refs):
+    rows = refs[:groups]
+    gate, up, down = refs[groups : groups + 3]
+    outs = refs[groups + 3 : 2 * groups + 3]
+    shared = refs[-1]
+    per_lane = rows[0].shape[0]
+    for k in range(groups):
+        shared[k * per_lane : (k + 1) * per_lane, :] = rows[k][...].astype(F32)
+    y = shared[...].astype(BF16)
+    hidden = (silu(dot_nt(y, gate[...])) * dot_nt(y, up[...])).astype(BF16)
+    result = dot(hidden, down[...])
+    for k in range(groups):
+        outs[k][...] = result[k * per_lane : (k + 1) * per_lane].astype(BF16)
 
 
 def combine_kernel(groups, table, *refs):
     rows = refs[:groups]
-    own, dense = refs[groups : groups + 2]
-    sends = refs[groups + 2 : -1]
+    own = refs[groups]
+    sends = refs[groups + 1 : -1]
     gathered = refs[-1]
     per_lane = own.shape[0]
-    capacity = rows[0].shape[0] - per_lane
-    block = jnp.zeros(own.shape, F32)
+    capacity = rows[0].shape[0]
     for message, k in zip(rows, peers(groups)):
-        values = message[...].astype(F32)
-        gathered[k * capacity : (k + 1) * capacity, :] = values[:capacity]
-        block = block + values[capacity:]
-    dense[...] = block
+        gathered[k * capacity : (k + 1) * capacity, :] = message[...].astype(F32)
     x = gathered[...].astype(BF16)
     high, low = halves(table[...])
     result = dot(high, x) + dot(low, x)
@@ -304,12 +319,16 @@
         send[...] = result[k * per_lane : (k + 1) * per_lane].astype(BF16)
 
 
-def final_kernel(hidden, moe, dense, offset, *refs):
+def final_kernel(groups, hidden, moe, offset, *refs):
     total = moe[...]
-    for other in refs[:-1]:
+    for other in refs[:-1 - groups]:
         total = total + other[...].astype(F32)
+    blocks = refs[-1 - groups : -1]
+    block = blocks[0][...].astype(F32)
+    for part in blocks[1:]:
+        block = block + part[...].astype(F32)
     out = refs[-1]
-    out[...] = (hidden[...] + total + jax.nn.sigmoid(offset[...]) * dense[...]).astype(BF16)
+    out[...] = (hidden[...] + total + jax.nn.sigmoid(offset[...]) * block).astype(BF16)
 
 
 def like(shape, dtype):
@@ -334,10 +353,12 @@
 
 def exchange(arrays, axis):
     size = lax.axis_size(axis)
-    return [
-        lax.ppermute(array, axis, [(i, i ^ k) for i in range(size)]) if k else array
-        for k, array in zip(peers(size), arrays)
-    ]
+    got = []
+    for k, array in zip(peers(size), arrays):
+        if k:
+            array = lax.ppermute(array, axis, [(i, i ^ k) for i in range(size)])
+        got.append(array)
+    return got
 
 
 def local(
@@ -377,32 +398,30 @@
     def row(x):
         return x.reshape(1, -1)
 
-    ahead = []
     steps = area // (8 * HEAD_WIDTH)
-    next_state, partial, pick, table, tokens_near, gain_near, *ahead = pl.pallas_call(
+    count = seqs * heads
+    partial, pick, table, tokens_near, gain_near, rows, packed, removed = pl.pallas_call(
         attention_kernel,
         out_shape=(
-            like(recurrent_head_state.shape, F32),
             near((seqs, width), BF16),
             near((groups * capacity, seqs), BF16),
             near((seqs, groups * capacity), F32),
             near((seqs, width), BF16),
             near((1, width), F32),
-            *[near(x.shape, x.dtype) for x in ahead],
+            near((count, area), F32),
+            near((count, 4 * HEAD_WIDTH), F32),
+            near((count, 2 * HEAD_WIDTH), F32),
         ),
-        in_specs=[VMEM] * 10 + [HBM] * (6 + len(ahead)),
-        out_specs=[HBM] + [VMEM] * (5 + len(ahead)),
+        in_specs=[VMEM] * 10 + [HBM] * 6,
+        out_specs=[VMEM] * 8,
         scratch_shapes=[
-            pltpu.VMEM((seqs * heads, area), F32),
             pltpu.VMEM((seqs, heads, area), F32),
             *[pltpu.VMEM(receptance_matrix.shape, BF16)] * 4,
             pltpu.VMEM(output_matrix.shape, BF16),
             pltpu.SemaphoreType.DMA((5,)),
             pltpu.SemaphoreType.DMA((steps,)),
-            pltpu.SemaphoreType.DMA((steps,)),
-            pltpu.SemaphoreType.DMA((1,)),
         ],
-        compiler_params=pltpu.CompilerParams(vmem_limit_bytes=54 * MIB),
+        compiler_params=pltpu.CompilerParams(vmem_limit_bytes=50 * MIB),
         name="attention",
     )(
         *far(
@@ -423,57 +442,75 @@
                 value_matrix,
                 decay_matrix,
                 output_matrix,
-                *ahead,
             ]
         )
     )
-    parts = lax.all_gather(partial, "tp", axis=0, tiled=False)
-    message = near((capacity + per_lane, width), BF16)
-    own_hidden, *sends = pl.pallas_call(
-        dispatch_kernel,
-        out_shape=(near((per_lane, width), F32), *[message] * groups),
-        in_specs=[VMEM] * 4,
-        out_specs=[VMEM] * (1 + groups),
+    parts = exchange([partial] * lanes, "tp")
+    next_state = pl.pallas_call(
+        update_kernel,
+        out_shape=like(recurrent_head_state.shape, F32),
+        in_specs=[VMEM] * 3,
+        out_specs=HBM,
+        scratch_shapes=[
+            pltpu.VMEM((seqs, heads, area), F32),
+            pltpu.SemaphoreType.DMA((steps,)),
+        ],
+        compiler_params=pltpu.CompilerParams(vmem_limit_bytes=46 * MIB),
+        name="update",
+    )(*bring([rows, packed, removed]))
+    message = near((capacity, width), BF16)
+    shared = near((per_lane, width), BF16)
+    own_hidden, own_rows, *sends = pl.pallas_call(
+        functools.partial(dispatch_kernel, lanes),
+        out_shape=(near((per_lane, width), F32), shared, *[message] * groups),
+        in_specs=[VMEM] * (3 + lanes),
+        out_specs=[VMEM] * (2 + groups),
         compiler_params=pltpu.CompilerParams(vmem_limit_bytes=8 * MIB),
-        cost_estimate=pl.CostEstimate(flops=20 * 10**9, bytes_accessed=1 << 20, transcendentals=0),
+        cost_estimate=pl.CostEstimate(
+            flops=20 * 10**9, bytes_accessed=1 << 20, transcendentals=0
+        ),
         name="dispatch",
-    )(*bring([parts, tokens_near, gain_near, pick]))
+    )(*bring([*parts, tokens_near, gain_near, pick]))
     received = exchange(sends, "ep")
+    shared_rows = exchange([own_rows] * groups, "ep")
     computed = pl.pallas_call(
-        functools.partial(units_kernel, groups, capacity, min(256, units)),
+        functools.partial(expert_kernel, groups, min(256, units)),
         out_shape=[message] * groups,
-        in_specs=[VMEM] * (groups + 6),
+        in_specs=[VMEM] * (groups + 3),
         out_specs=[VMEM] * groups,
-        scratch_shapes=[
-            pltpu.VMEM((groups * capacity, width), F32),
-            pltpu.VMEM((groups * per_lane, width), F32),
-        ],
-        compiler_params=pltpu.CompilerParams(vmem_limit_bytes=14 * MIB),
-        name="units",
-    )(
-        *bring(received),
-        *bring([expert_gate_weight, expert_up_weight, expert_down_weight]),
-        *bring([dense_gate_weight.T, dense_up_weight.T, dense_down_weight]),
-    )
+        scratch_shapes=[pltpu.VMEM((groups * capacity, width), F32)],
+        compiler_params=pltpu.CompilerParams(vmem_limit_bytes=12 * MIB),
+        name="experts",
+    )(*bring([*received, expert_gate_weight, expert_up_weight, expert_down_weight]))
     returned = exchange(computed, "ep")
-    moe_own, dense_sum, *moe_sends = pl.pallas_call(
+    blocks = pl.pallas_call(
+        functools.partial(dense_kernel, groups),
+        out_shape=[shared] * groups,
+        in_specs=[VMEM] * (groups + 3),
+        out_specs=[VMEM] * groups,
+        scratch_shapes=[pltpu.VMEM((groups * per_lane, width), F32)],
+        compiler_params=pltpu.CompilerParams(vmem_limit_bytes=8 * MIB),
+        name="dense",
+    )(*bring([*shared_rows, dense_gate_weight.T, dense_up_weight.T, dense_down_weight]))
+    blocks = exchange(blocks, "ep")
+    moe_own, *moe_sends = pl.pallas_call(
         functools.partial(combine_kernel, groups),
-        out_shape=[near((per_lane, width), F32)] * 2 + [near((per_lane, width), BF16)] * (lanes - 1),
+        out_shape=[near((per_lane, width), F32)] + [near((per_lane, width), BF16)] * (lanes - 1),
         in_specs=[VMEM] * (groups + 1),
-        out_specs=[VMEM] * (lanes + 1),
+        out_specs=[VMEM] * lanes,
         scratch_shapes=[pltpu.VMEM((groups * capacity, width), F32)],
         compiler_params=pltpu.CompilerParams(vmem_limit_bytes=8 * MIB),
         name="combine",
     )(*bring([table, *returned]))
     moe_in = exchange([moe_own] + moe_sends, "tp")
     layer_out = pl.pallas_call(
-        final_kernel,
+        functools.partial(final_kernel, groups),
         out_shape=like((per_lane, width), BF16),
-        in_specs=[VMEM] * (3 + lanes),
+        in_specs=[VMEM] * (2 + lanes + groups),
         out_specs=VMEM,
         compiler_params=pltpu.CompilerParams(vmem_limit_bytes=4 * MIB),
         name="final",
-    )(*bring([own_hidden, moe_in[0], dense_sum, row(dense_gate_offset), *moe_in[1:]]))
+    )(*bring([own_hidden, moe_in[0], row(dense_gate_offset), *moe_in[1:], *blocks]))
     return (layer_out, next_state)
 
 

time: 73.6 us -> 77.4 us (1.052)
  starting transfers between devices: 18.6 us -> 40.6 us
  blocking collectives: 11.5 us -> 0 us
  waiting for transfers between devices: 27.3 us -> 20.1 us
    ppermute x17 -> x34, starting transfers between devices: 18.6 us -> 40.6 us  [exchange(): array = lax.ppermute(array, axis, [(i, i ^ k) for i in range(size)])]
    all_gather x1 -> x0, blocking collectives: 11.5 us -> none  [local(): parts = lax.all_gather(partial, 'tp', axis=0, tiled=False)]
    ppermute x17 -> x34, waiting for transfers between devices: 27.3 us -> 20.1 us  [exchange(): array = lax.ppermute(array, axis, [(i, i ^ k) for i in range(size)])]
    pallas_call x4 -> x6, Pallas kernels: 14.9 us -> 15.4 us  [the longest x1 8.83 us: local(): pl.pallas_call(attention_kernel, out_shape=(near((seqs, width), BF16), ne...]
  transfers between devices with their start and end apart: 17 -> 34, of which waited for: 10 -> 10; matrix products, arithmetic and copies ran while one was open for 0% -> 0% of each run, Pallas kernels for 0% -> 7%
where the time goes in v3:
time: 77.4 us; the launch traced here: 77.2 us
  starting transfers between devices  40.6 us (52%)
  waiting for transfers between devices  20.1 us (26%)
  Pallas kernels  15.7 us (20%)
  between operations  0.8 us (1%)
    ppermute x34, starting transfers between devices, exchange(): array = lax.ppermute(array, axis, [(i, i ^ k) for i in range(size)])  40.6 us
    ppermute x34, waiting for transfers between devices, exchange(): array = lax.ppermute(array, axis, [(i, i ^ k) for i in range(size)])  20.1 us
    pallas_call x1, Pallas kernels, local(): pl.pallas_call(attention_kernel, out_shape=(near((seqs, width), BF16), ne...  8.83 us
    pallas_call x1, Pallas kernels, local(): pl.pallas_call(functools.partial(expert_kernel, groups, min(256, units)),...  2.24 us
    pallas_call x1, Pallas kernels, local(): pl.pallas_call(update_kernel, out_shape=like(recurrent_head_state.shape,...  1.75 us
  transfers between devices with their start and end apart: 34, of which 10 were waited for; matrix products, arithmetic and copies ran while one was open for 0% of the time, Pallas kernels for 7%

profile of v3, /device:TPU:0, one launch (start us, length us, event | category | flops | bytes accessed | tf_op | source)
XLA Modules:
  0.0 77.2 jit_solution(15151351201765603323)
XLA Ops:
  0.6 8.8 %attention.1 = (bf16[32,2048]{1,0:T(8,128)(2,1)S(1)}, bf16[128,32]{1,0:T(8,128)(2,1)S(1)}, f32[32,128]{1,0:T(8,128)S(1)}, bf16[32,2048]{1,0:T(8,128)(2,1)S(1)}, ...) custom-call(bf16[32,2048]{1,0:T(8,128)(2,1)} %tokens.1, ...), custom_call_target="tpu_custom_call" | custom-call | tf_op jit(solution)/shard_map/attention/pallas_call | solution.py:403
  9.5 3.0 %collective-permute-start.2 = (bf16[32,2048]{1,0:T(8,128)(2,1)S(1)}, bf16[32,2048]{1,0:T(8,128)(2,1)S(1)}, u32[]{:S(2)}, u32[]{:S(2)}) collective-permute-start(bf16[32,2048]{1,0:T(8,128)(2,1)S(1)} %get-tuple-element.40.refs_0_), channel_id=1, source_target_pairs={{0,1},{1,0},{2,3},{3,2},{4,5},{5,4},{6,7},{7,6},{8,9},{9,8},{10,11... | collective-permute-start | bytes 393224 | tf_op jit(solution)/shard_map/ppermute | solution.py:359
  12.5 1.5 %collective-permute-start.1 = (bf16[32,2048]{1,0:T(8,128)(2,1)S(1)}, bf16[32,2048]{1,0:T(8,128)(2,1)S(1)}, u32[]{:S(2)}, u32[]{:S(2)}) collective-permute-start(bf16[32,2048]{1,0:T(8,128)(2,1)S(1)} %get-tuple-element.40.refs_0_), channel_id=1, source_target_pairs={{0,3},{1,2},{2,1},{3,0},{4,7},{5,6},{6,5},{7,4},{8,11},{9,10},{10,... | collective-permute-start | bytes 393224 | tf_op jit(solution)/shard_map/ppermute | solution.py:359
  14.0 2.3 %collective-permute-done.2.refs_3_ = bf16[32,2048]{1,0:T(8,128)(2,1)S(1)} collective-permute-done((bf16[32,2048]{1,0:T(8,128)(2,1)S(1)}, bf16[32,2048]{1,0:T(8,128)(2,1)S(1)}, u32[]{:S(2)}, u32[]{:S(2)}) %collective-permute-start.2) | collective-permute-done | bytes 131104 | tf_op jit(solution)/shard_map/ppermute | solution.py:359
  16.4 3.7 %collective-permute-done.1.refs_2_ = bf16[32,2048]{1,0:T(8,128)(2,1)S(1)} collective-permute-done((bf16[32,2048]{1,0:T(8,128)(2,1)S(1)}, bf16[32,2048]{1,0:T(8,128)(2,1)S(1)}, u32[]{:S(2)}, u32[]{:S(2)}) %collective-permute-start.1) | collective-permute-done | bytes 131104 | tf_op jit(solution)/shard_map/ppermute | solution.py:359
  20.1 1.4 %collective-permute-done.refs_1_ = bf16[32,2048]{1,0:T(8,128)(2,1)S(1)} collective-permute-done((bf16[32,2048]{1,0:T(8,128)(2,1)S(1)}, bf16[32,2048]{1,0:T(8,128)(2,1)S(1)}, u32[]{:S(2)}, u32[]{:S(2)}) %collective-permute-start) | collective-permute-done | bytes 131104 | tf_op jit(solution)/shard_map/ppermute | solution.py:359
  22.1 2.6 %collective-permute-start.3 = (bf16[16,2048]{1,0:T(8,128)(2,1)S(1)}, bf16[16,2048]{1,0:T(8,128)(2,1)S(1)}, u32[]{:S(2)}, u32[]{:S(2)}) collective-permute-start(bf16[16,2048]{1,0:T(8,128)(2,1)S(1)} %get-tuple-element.47), channel_id=1, source_target_pairs={{0,16},{4,20},{8,24},{12,28},{16,0},{20,4},{24,8},{28,12},{1,17},{... | collective-permute-start | bytes 196616 | tf_op jit(solution)/shard_map/ppermute | solution.py:359
  24.8 2.4 %collective-permute-start.5 = (bf16[16,2048]{1,0:T(8,128)(2,1)S(1)}, bf16[16,2048]{1,0:T(8,128)(2,1)S(1)}, u32[]{:S(2)}, u32[]{:S(2)}) collective-permute-start(bf16[16,2048]{1,0:T(8,128)(2,1)S(1)} %get-tuple-element.49), channel_id=1, source_target_pairs={{0,24},{4,28},{8,16},{12,20},{16,8},{20,12},{24,0},{28,4},{1,25},{... | collective-permute-start | bytes 196616 | tf_op jit(solution)/shard_map/ppermute | solution.py:359
  28.4 1.6 %collective-permute-start.8 = (bf16[16,2048]{1,0:T(8,128)(2,1)S(1)}, bf16[16,2048]{1,0:T(8,128)(2,1)S(1)}, u32[]{:S(2)}, u32[]{:S(2)}) collective-permute-start(bf16[16,2048]{1,0:T(8,128)(2,1)S(1)} %get-tuple-element.52), channel_id=1, source_target_pairs={{0,12},{4,8},{8,4},{12,0},{16,28},{20,24},{24,20},{28,16},{1,13},{... | collective-permute-start | bytes 196616 | tf_op jit(solution)/shard_map/ppermute | solution.py:359
  30.1 3.5 %collective-permute-done.4.refs_2_ = bf16[16,2048]{1,0:T(8,128)(2,1)S(1)} collective-permute-done((bf16[16,2048]{1,0:T(8,128)(2,1)S(1)}, bf16[16,2048]{1,0:T(8,128)(2,1)S(1)}, u32[]{:S(2)}, u32[]{:S(2)}) %collective-permute-start.4) | collective-permute-done | bytes 65568 | tf_op jit(solution)/shard_map/ppermute | solution.py:359
  34.1 2.7 %collective-permute-start.25 = (bf16[8,2048]{1,0:T(8,128)(2,1)S(1)}, bf16[8,2048]{1,0:T(8,128)(2,1)S(1)}, u32[]{:S(2)}, u32[]{:S(2)}) collective-permute-start(bf16[8,2048]{1,0:T(8,128)(2,1)S(1)} %get-tuple-element.66.refs_0_), channel_id=1, source_target_pairs={{0,12},{4,8},{8,4},{12,0},{16,28},{20,24},{24,20},{28,16},{1,13},{... | collective-permute-start | bytes 98312 | tf_op jit(solution)/shard_map/ppermute | solution.py:359
  37.4 2.2 %collective-permute-start.23 = (bf16[8,2048]{1,0:T(8,128)(2,1)S(1)}, bf16[8,2048]{1,0:T(8,128)(2,1)S(1)}, u32[]{:S(2)}, u32[]{:S(2)}) collective-permute-start(bf16[8,2048]{1,0:T(8,128)(2,1)S(1)} %get-tuple-element.66.refs_0_), channel_id=1, source_target_pairs={{0,28},{4,24},{8,20},{12,16},{16,12},{20,8},{24,4},{28,0},{1,29},{... | collective-permute-start | bytes 98312 | tf_op jit(solution)/shard_map/ppermute | solution.py:359
  39.6 2.2 %experts.1 = (bf16[16,2048]{1,0:T(8,128)(2,1)S(1)}, bf16[16,2048]{1,0:T(8,128)(2,1)S(1)}, bf16[16,2048]{1,0:T(8,128)(2,1)S(1)}, bf16[16,2048]{1,0:T(8,128)(2,1)S...) custom-call(bf16[16,2048]{1,0:T(8,128)(2,1)S(1)} %get-tuple-element., ...), custom_call_target="tpu_custom_call" | custom-call | tf_op jit(solution)/shard_map/experts/pallas_call | solution.py:476
  42.7 2.0 %collective-permute-start.11 = (bf16[16,2048]{1,0:T(8,128)(2,1)S(1)}, bf16[16,2048]{1,0:T(8,128)(2,1)S(1)}, u32[]{:S(2)}, u32[]{:S(2)}) collective-permute-start(bf16[16,2048]{1,0:T(8,128)(2,1)S(1)} %get-tuple-element.56), channel_id=1, source_target_pairs={{0,20},{4,16},{8,28},{12,24},{16,4},{20,0},{24,12},{28,8},{1,21},{... | collective-permute-start | bytes 196616 | tf_op jit(solution)/shard_map/ppermute | solution.py:359
  46.4 2.2 %collective-permute-start.20 = (bf16[8,2048]{1,0:T(8,128)(2,1)S(1)}, bf16[8,2048]{1,0:T(8,128)(2,1)S(1)}, u32[]{:S(2)}, u32[]{:S(2)}) collective-permute-start(bf16[8,2048]{1,0:T(8,128)(2,1)S(1)} %get-tuple-element.66.refs_0_), channel_id=1, source_target_pairs={{0,16},{4,20},{8,24},{12,28},{16,0},{20,4},{24,8},{28,12},{1,17},{... | collective-permute-start | bytes 98312 | tf_op jit(solution)/shard_map/ppermute | solution.py:359
  48.7 1.8 %collective-permute-done.22.refs_3_ = bf16[8,2048]{1,0:T(8,128)(2,1)S(1)} collective-permute-done((bf16[8,2048]{1,0:T(8,128)(2,1)S(1)}, bf16[8,2048]{1,0:T(8,128)(2,1)S(1)}, u32[]{:S(2)}, u32[]{:S(2)}) %collective-permute-start.22) | collective-permute-done | bytes 32800 | tf_op jit(solution)/shard_map/ppermute | solution.py:359
  50.5 1.4 %collective-permute-start.12 = (bf16[16,2048]{1,0:T(8,128)(2,1)S(1)}, bf16[16,2048]{1,0:T(8,128)(2,1)S(1)}, u32[]{:S(2)}, u32[]{:S(2)}) collective-permute-start(bf16[16,2048]{1,0:T(8,128)(2,1)S(1)} %get-tuple-element.57), channel_id=1, source_target_pairs={{0,24},{4,28},{8,16},{12,20},{16,8},{20,12},{24,0},{28,4},{1,25},{... | collective-permute-start | bytes 196616 | tf_op jit(solution)/shard_map/ppermute | solution.py:359
  51.8 3.6 %collective-permute-done.21.refs_2_ = bf16[8,2048]{1,0:T(8,128)(2,1)S(1)} collective-permute-done((bf16[8,2048]{1,0:T(8,128)(2,1)S(1)}, bf16[8,2048]{1,0:T(8,128)(2,1)S(1)}, u32[]{:S(2)}, u32[]{:S(2)}) %collective-permute-start.21) | collective-permute-done | bytes 32800 | tf_op jit(solution)/shard_map/ppermute | solution.py:359
  60.8 1.5 %collective-permute-start.27 = (bf16[8,2048]{1,0:T(8,128)(2,1)S(1)}, bf16[8,2048]{1,0:T(8,128)(2,1)S(1)}, u32[]{:S(2)}, u32[]{:S(2)}) collective-permute-start(bf16[8,2048]{1,0:T(8,128)(2,1)S(1)} %get-tuple-element.68), channel_id=1, source_target_pairs={{0,16},{4,20},{8,24},{12,28},{16,0},{20,4},{24,8},{28,12},{1,17},{... | collective-permute-start | bytes 98312 | tf_op jit(solution)/shard_map/ppermute | solution.py:359
  63.1 2.8 %collective-permute-start.29 = (bf16[8,2048]{1,0:T(8,128)(2,1)S(1)}, bf16[8,2048]{1,0:T(8,128)(2,1)S(1)}, u32[]{:S(2)}, u32[]{:S(2)}) collective-permute-start(bf16[8,2048]{1,0:T(8,128)(2,1)S(1)} %get-tuple-element.70), channel_id=1, source_target_pairs={{0,24},{4,28},{8,16},{12,20},{16,8},{20,12},{24,0},{28,4},{1,25},{... | collective-permute-start | bytes 98312 | tf_op jit(solution)/shard_map/ppermute | solution.py:359
  67.3 1.5 %collective-permute-start.32 = (bf16[8,2048]{1,0:T(8,128)(2,1)S(1)}, bf16[8,2048]{1,0:T(8,128)(2,1)S(1)}, u32[]{:S(2)}, u32[]{:S(2)}) collective-permute-start(bf16[8,2048]{1,0:T(8,128)(2,1)S(1)} %get-tuple-element.73), channel_id=1, source_target_pairs={{0,12},{4,8},{8,4},{12,0},{16,28},{20,24},{24,20},{28,16},{1,13},{... | collective-permute-start | bytes 98312 | tf_op jit(solution)/shard_map/ppermute | solution.py:359
  69.9 1.3 %collective-permute-done.30.refs_7_ = bf16[8,2048]{1,0:T(8,128)(2,1)S(1)} collective-permute-done((bf16[8,2048]{1,0:T(8,128)(2,1)S(1)}, bf16[8,2048]{1,0:T(8,128)(2,1)S(1)}, u32[]{:S(2)}, u32[]{:S(2)}) %collective-permute-start.30) | collective-permute-done | bytes 32800 | tf_op jit(solution)/shard_map/ppermute | solution.py:359
  71.2 1.4 %collective-permute-start.18 = (bf16[8,2048]{1,0:T(8,128)(2,1)S(1)}, bf16[8,2048]{1,0:T(8,128)(2,1)S(1)}, u32[]{:S(2)}, u32[]{:S(2)}) collective-permute-start(bf16[8,2048]{1,0:T(8,128)(2,1)S(1)} %get-tuple-element.64), channel_id=1, source_target_pairs={{0,3},{1,2},{2,1},{3,0},{4,7},{5,6},{6,5},{7,4},{8,11},{9,10},{10,... | collective-permute-start | bytes 98312 | tf_op jit(solution)/shard_map/ppermute | solution.py:359
  73.0 1.8 %update.1 = f32[32,4,4096]{2,1,0:T(4,128)} custom-call(f32[128,4096]{1,0:T(8,128)S(1)} %get-tuple-element.75.rows_ref, f32[128,256]{1,0:T(8,128)S(1)} %get-tuple-element.76.packed_ref, f32[128,128]{1,0:T(8,128)S(1)} %get-tuple-element.77.removed_ref), custom_call_target="tpu_custom_call" | custom-call | tf_op jit(solution)/shard_map/update/pallas_call | solution.py:449
  (65 shorter events, 17.0 us)
Async XLA Ops:
  9.5 6.9 %collective-permute-start.2 = (bf16[32,2048]{1,0:T(8,128)(2,1)S(1)}, bf16[32,2048]{1,0:T(8,128)(2,1)S(1)}, u32[]{:S(2)}, u32[]{:S(2)}) collective-permute-start(bf16[32,2048]{1,0:T(8,128)(2,1)S(1)} %get-tuple-element.40.refs_0_), channel_id=1, source_target_pairs={{0,1},{1,0},{2,3},{3,2},{4,5},{5,4},{6,7},{7,6},{8,9},{9,8},{10,11... | collective-permute-start | bytes 393224 | tf_op jit(solution)/shard_map/ppermute | solution.py:359
  12.5 7.6 %collective-permute-start.1 = (bf16[32,2048]{1,0:T(8,128)(2,1)S(1)}, bf16[32,2048]{1,0:T(8,128)(2,1)S(1)}, u32[]{:S(2)}, u32[]{:S(2)}) collective-permute-start(bf16[32,2048]{1,0:T(8,128)(2,1)S(1)} %get-tuple-element.40.refs_0_), channel_id=1, source_target_pairs={{0,3},{1,2},{2,1},{3,0},{4,7},{5,6},{6,5},{7,4},{8,11},{9,10},{10,... | collective-permute-start | bytes 393224 | tf_op jit(solution)/shard_map/ppermute | solution.py:359
  14.0 7.5 %collective-permute-start = (bf16[32,2048]{1,0:T(8,128)(2,1)S(1)}, bf16[32,2048]{1,0:T(8,128)(2,1)S(1)}, u32[]{:S(2)}, u32[]{:S(2)}) collective-permute-start(bf16[32,2048]{1,0:T(8,128)(2,1)S(1)} %get-tuple-element.40.refs_0_), channel_id=1, source_target_pairs={{0,2},{1,3},{2,0},{3,1},{4,6},{5,7},{6,4},{7,5},{8,10},{9,11},{10,... | collective-permute-start | bytes 393224 | tf_op jit(solution)/shard_map/ppermute | solution.py:359
  24.8 8.8 %collective-permute-start.4 = (bf16[16,2048]{1,0:T(8,128)(2,1)S(1)}, bf16[16,2048]{1,0:T(8,128)(2,1)S(1)}, u32[]{:S(2)}, u32[]{:S(2)}) collective-permute-start(bf16[16,2048]{1,0:T(8,128)(2,1)S(1)} %get-tuple-element.48), channel_id=1, source_target_pairs={{0,20},{4,16},{8,28},{12,24},{16,4},{20,0},{24,12},{28,8},{1,21},{... | collective-permute-start | bytes 196616 | tf_op jit(solution)/shard_map/ppermute | solution.py:359
  24.8 8.8 %collective-permute-start.5 = (bf16[16,2048]{1,0:T(8,128)(2,1)S(1)}, bf16[16,2048]{1,0:T(8,128)(2,1)S(1)}, u32[]{:S(2)}, u32[]{:S(2)}) collective-permute-start(bf16[16,2048]{1,0:T(8,128)(2,1)S(1)} %get-tuple-element.49), channel_id=1, source_target_pairs={{0,24},{4,28},{8,16},{12,20},{16,8},{20,12},{24,0},{28,4},{1,25},{... | collective-permute-start | bytes 196616 | tf_op jit(solution)/shard_map/ppermute | solution.py:359
  27.2 6.9 %collective-permute-start.6 = (bf16[16,2048]{1,0:T(8,128)(2,1)S(1)}, bf16[16,2048]{1,0:T(8,128)(2,1)S(1)}, u32[]{:S(2)}, u32[]{:S(2)}) collective-permute-start(bf16[16,2048]{1,0:T(8,128)(2,1)S(1)} %get-tuple-element.50), channel_id=1, source_target_pairs={{0,28},{4,24},{8,20},{12,16},{16,12},{20,8},{24,4},{28,0},{1,29},{... | collective-permute-start | bytes 196616 | tf_op jit(solution)/shard_map/ppermute | solution.py:359
  28.4 8.4 %collective-permute-start.7 = (bf16[16,2048]{1,0:T(8,128)(2,1)S(1)}, bf16[16,2048]{1,0:T(8,128)(2,1)S(1)}, u32[]{:S(2)}, u32[]{:S(2)}) collective-permute-start(bf16[16,2048]{1,0:T(8,128)(2,1)S(1)} %get-tuple-element.51), channel_id=1, source_target_pairs={{0,8},{4,12},{8,0},{12,4},{16,24},{20,28},{24,16},{28,20},{1,9},{5... | collective-permute-start | bytes 196616 | tf_op jit(solution)/shard_map/ppermute | solution.py:359
  28.4 8.9 %collective-permute-start.8 = (bf16[16,2048]{1,0:T(8,128)(2,1)S(1)}, bf16[16,2048]{1,0:T(8,128)(2,1)S(1)}, u32[]{:S(2)}, u32[]{:S(2)}) collective-permute-start(bf16[16,2048]{1,0:T(8,128)(2,1)S(1)} %get-tuple-element.52), channel_id=1, source_target_pairs={{0,12},{4,8},{8,4},{12,0},{16,28},{20,24},{24,20},{28,16},{1,13},{... | collective-permute-start | bytes 196616 | tf_op jit(solution)/shard_map/ppermute | solution.py:359
  33.6 9.1 %collective-permute-start.26 = (bf16[8,2048]{1,0:T(8,128)(2,1)S(1)}, bf16[8,2048]{1,0:T(8,128)(2,1)S(1)}, u32[]{:S(2)}, u32[]{:S(2)}) collective-permute-start(bf16[8,2048]{1,0:T(8,128)(2,1)S(1)} %get-tuple-element.66.refs_0_), channel_id=1, source_target_pairs={{0,4},{4,0},{8,12},{12,8},{16,20},{20,16},{24,28},{28,24},{1,5},{5... | collective-permute-start | bytes 98312 | tf_op jit(solution)/shard_map/ppermute | solution.py:359
  34.1 10.6 %collective-permute-start.25 = (bf16[8,2048]{1,0:T(8,128)(2,1)S(1)}, bf16[8,2048]{1,0:T(8,128)(2,1)S(1)}, u32[]{:S(2)}, u32[]{:S(2)}) collective-permute-start(bf16[8,2048]{1,0:T(8,128)(2,1)S(1)} %get-tuple-element.66.refs_0_), channel_id=1, source_target_pairs={{0,12},{4,8},{8,4},{12,0},{16,28},{20,24},{24,20},{28,16},{1,13},{... | collective-permute-start | bytes 98312 | tf_op jit(solution)/shard_map/ppermute | solution.py:359
  36.8 9.2 %collective-permute-start.24 = (bf16[8,2048]{1,0:T(8,128)(2,1)S(1)}, bf16[8,2048]{1,0:T(8,128)(2,1)S(1)}, u32[]{:S(2)}, u32[]{:S(2)}) collective-permute-start(bf16[8,2048]{1,0:T(8,128)(2,1)S(1)} %get-tuple-element.66.refs_0_), channel_id=1, source_target_pairs={{0,8},{4,12},{8,0},{12,4},{16,24},{20,28},{24,16},{28,20},{1,9},{5... | collective-permute-start | bytes 98312 | tf_op jit(solution)/shard_map/ppermute | solution.py:359
  37.4 9.0 %collective-permute-start.23 = (bf16[8,2048]{1,0:T(8,128)(2,1)S(1)}, bf16[8,2048]{1,0:T(8,128)(2,1)S(1)}, u32[]{:S(2)}, u32[]{:S(2)}) collective-permute-start(bf16[8,2048]{1,0:T(8,128)(2,1)S(1)} %get-tuple-element.66.refs_0_), channel_id=1, source_target_pairs={{0,28},{4,24},{8,20},{12,16},{16,12},{20,8},{24,4},{28,0},{1,29},{... | collective-permute-start | bytes 98312 | tf_op jit(solution)/shard_map/ppermute | solution.py:359
  41.9 15.4 %collective-permute-start.10 = (bf16[16,2048]{1,0:T(8,128)(2,1)S(1)}, bf16[16,2048]{1,0:T(8,128)(2,1)S(1)}, u32[]{:S(2)}, u32[]{:S(2)}) collective-permute-start(bf16[16,2048]{1,0:T(8,128)(2,1)S(1)} %get-tuple-element.55), channel_id=1, source_target_pairs={{0,16},{4,20},{8,24},{12,28},{16,0},{20,4},{24,8},{28,12},{1,17},{... | collective-permute-start | bytes 196616 | tf_op jit(solution)/shard_map/ppermute | solution.py:359
  42.7 15.7 %collective-permute-start.11 = (bf16[16,2048]{1,0:T(8,128)(2,1)S(1)}, bf16[16,2048]{1,0:T(8,128)(2,1)S(1)}, u32[]{:S(2)}, u32[]{:S(2)}) collective-permute-start(bf16[16,2048]{1,0:T(8,128)(2,1)S(1)} %get-tuple-element.56), channel_id=1, source_target_pairs={{0,20},{4,16},{8,28},{12,24},{16,4},{20,0},{24,12},{28,8},{1,21},{... | collective-permute-start | bytes 196616 | tf_op jit(solution)/shard_map/ppermute | solution.py:359
  45.9 9.5 %collective-permute-start.21 = (bf16[8,2048]{1,0:T(8,128)(2,1)S(1)}, bf16[8,2048]{1,0:T(8,128)(2,1)S(1)}, u32[]{:S(2)}, u32[]{:S(2)}) collective-permute-start(bf16[8,2048]{1,0:T(8,128)(2,1)S(1)} %get-tuple-element.66.refs_0_), channel_id=1, source_target_pairs={{0,20},{4,16},{8,28},{12,24},{16,4},{20,0},{24,12},{28,8},{1,21},{... | collective-permute-start | bytes 98312 | tf_op jit(solution)/shard_map/ppermute | solution.py:359
  46.4 10.9 %collective-permute-start.20 = (bf16[8,2048]{1,0:T(8,128)(2,1)S(1)}, bf16[8,2048]{1,0:T(8,128)(2,1)S(1)}, u32[]{:S(2)}, u32[]{:S(2)}) collective-permute-start(bf16[8,2048]{1,0:T(8,128)(2,1)S(1)} %get-tuple-element.66.refs_0_), channel_id=1, source_target_pairs={{0,16},{4,20},{8,24},{12,28},{16,0},{20,4},{24,8},{28,12},{1,17},{... | collective-permute-start | bytes 98312 | tf_op jit(solution)/shard_map/ppermute | solution.py:359
  50.5 10.3 %collective-permute-start.12 = (bf16[16,2048]{1,0:T(8,128)(2,1)S(1)}, bf16[16,2048]{1,0:T(8,128)(2,1)S(1)}, u32[]{:S(2)}, u32[]{:S(2)}) collective-permute-start(bf16[16,2048]{1,0:T(8,128)(2,1)S(1)} %get-tuple-element.57), channel_id=1, source_target_pairs={{0,24},{4,28},{8,16},{12,20},{16,8},{20,12},{24,0},{28,4},{1,25},{... | collective-permute-start | bytes 196616 | tf_op jit(solution)/shard_map/ppermute | solution.py:359
  55.4 6.8 %collective-permute-start.13 = (bf16[16,2048]{1,0:T(8,128)(2,1)S(1)}, bf16[16,2048]{1,0:T(8,128)(2,1)S(1)}, u32[]{:S(2)}, u32[]{:S(2)}) collective-permute-start(bf16[16,2048]{1,0:T(8,128)(2,1)S(1)} %get-tuple-element.58), channel_id=1, source_target_pairs={{0,28},{4,24},{8,20},{12,16},{16,12},{20,8},{24,4},{28,0},{1,29},{... | collective-permute-start | bytes 196616 | tf_op jit(solution)/shard_map/ppermute | solution.py:359
  57.3 8.7 %collective-permute-start.15 = (bf16[16,2048]{1,0:T(8,128)(2,1)S(1)}, bf16[16,2048]{1,0:T(8,128)(2,1)S(1)}, u32[]{:S(2)}, u32[]{:S(2)}) collective-permute-start(bf16[16,2048]{1,0:T(8,128)(2,1)S(1)} %get-tuple-element.60), channel_id=1, source_target_pairs={{0,12},{4,8},{8,4},{12,0},{16,28},{20,24},{24,20},{28,16},{1,13},{... | collective-permute-start | bytes 196616 | tf_op jit(solution)/shard_map/ppermute | solution.py:359
  58.4 8.6 %collective-permute-start.16 = (bf16[16,2048]{1,0:T(8,128)(2,1)S(1)}, bf16[16,2048]{1,0:T(8,128)(2,1)S(1)}, u32[]{:S(2)}, u32[]{:S(2)}) collective-permute-start(bf16[16,2048]{1,0:T(8,128)(2,1)S(1)} %get-tuple-element.61), channel_id=1, source_target_pairs={{0,4},{4,0},{8,12},{12,8},{16,20},{20,16},{24,28},{28,24},{1,5},{5... | collective-permute-start | bytes 196616 | tf_op jit(solution)/shard_map/ppermute | solution.py:359
  60.8 6.5 %collective-permute-start.27 = (bf16[8,2048]{1,0:T(8,128)(2,1)S(1)}, bf16[8,2048]{1,0:T(8,128)(2,1)S(1)}, u32[]{:S(2)}, u32[]{:S(2)}) collective-permute-start(bf16[8,2048]{1,0:T(8,128)(2,1)S(1)} %get-tuple-element.68), channel_id=1, source_target_pairs={{0,16},{4,20},{8,24},{12,28},{16,0},{20,4},{24,8},{28,12},{1,17},{... | collective-permute-start | bytes 98312 | tf_op jit(solution)/shard_map/ppermute | solution.py:359
  62.3 6.5 %collective-permute-start.28 = (bf16[8,2048]{1,0:T(8,128)(2,1)S(1)}, bf16[8,2048]{1,0:T(8,128)(2,1)S(1)}, u32[]{:S(2)}, u32[]{:S(2)}) collective-permute-start(bf16[8,2048]{1,0:T(8,128)(2,1)S(1)} %get-tuple-element.69), channel_id=1, source_target_pairs={{0,20},{4,16},{8,28},{12,24},{16,4},{20,0},{24,12},{28,8},{1,21},{... | collective-permute-start | bytes 98312 | tf_op jit(solution)/shard_map/ppermute | solution.py:359
  63.1 6.4 %collective-permute-start.29 = (bf16[8,2048]{1,0:T(8,128)(2,1)S(1)}, bf16[8,2048]{1,0:T(8,128)(2,1)S(1)}, u32[]{:S(2)}, u32[]{:S(2)}) collective-permute-start(bf16[8,2048]{1,0:T(8,128)(2,1)S(1)} %get-tuple-element.70), channel_id=1, source_target_pairs={{0,24},{4,28},{8,16},{12,20},{16,8},{20,12},{24,0},{28,4},{1,25},{... | collective-permute-start | bytes 98312 | tf_op jit(solution)/shard_map/ppermute | solution.py:359
  67.3 7.5 %collective-permute-start.32 = (bf16[8,2048]{1,0:T(8,128)(2,1)S(1)}, bf16[8,2048]{1,0:T(8,128)(2,1)S(1)}, u32[]{:S(2)}, u32[]{:S(2)}) collective-permute-start(bf16[8,2048]{1,0:T(8,128)(2,1)S(1)} %get-tuple-element.73), channel_id=1, source_target_pairs={{0,12},{4,8},{8,4},{12,0},{16,28},{20,24},{24,20},{28,16},{1,13},{... | collective-permute-start | bytes 98312 | tf_op jit(solution)/shard_map/ppermute | solution.py:359
  (17 other events, 172.0 us)

commit v4 on v3

--- a/solution.py
+++ b/solution.py
@@ -42,27 +42,17 @@
     return x * jax.nn.sigmoid(x)
 
 
-def attention_kernel(
-    tokens,
-    gain,
-    dec_off,
-    cor_off,
-    cor_fac,
-    own_w,
-    head_gain,
-    routing,
-    weights,
-    second_gain,
-    state,
-    rec_m,
-    key_m,
-    val_m,
-    dec_m,
-    out_m,
-    *refs,
-):
-    partial, pick, table, tokens_near, gain_near, rows_ref, packed_ref, removed_ref = refs[:8]
-    stage, rec_v, key_v, val_v, dec_v, out_v, mat_sem, in_sem = refs[8:]
+def attention_kernel(*refs):
+    small, large, outs = refs[:10], refs[10:16], refs[16:24]
+    stage, rec_v, key_v, val_v, dec_v, out_v, mat_sem, in_sem, small_sem = refs[24:33]
+    small_v = refs[33:]
+    state, rec_m, key_m, val_m, dec_m, out_m = large
+    partial, pick, table, tokens_near, gain_near, rows_ref, packed_ref, removed_ref = outs
+    tokens, gain, dec_off, cor_off, cor_fac, own_w, head_gain, routing, weights, second_gain = small_v
+    first = [
+        pltpu.make_async_copy(source, target, small_sem.at[n])
+        for n, (source, target) in enumerate(zip(small, small_v))
+    ]
     seqs, heads, area = state.shape
     width = HEAD_WIDTH
     count = seqs * heads
@@ -82,12 +72,19 @@
         )
         for j in range(steps)
     ]
-    for copy in [*mats[:4], *loads, mats[4]]:
+    for copy in [*first, *loads, *mats]:
         copy.start()
+    for copy in first:
+        copy.wait()
     route_tables(routing, weights, pick, table)
     tokens_near[...] = tokens[...]
     gain_near[...] = second_gain[...]
     normed = rms_rows(tokens[...].astype(F32), gain[...]).astype(BF16)
+    for j in range(steps):
+        part = slice(j * chunk, (j + 1) * chunk)
+        loads[j].wait()
+        for b in range(seqs):
+            rows_ref[b * heads : (b + 1) * heads, part] = stage[b, :, part]
     mats[0].wait()
     keys = dot(normed, key_v[...])
     mats[1].wait()
@@ -139,9 +136,6 @@
     slot = iota((chunk, 2 * width), 1)
     for j in range(steps):
         part = slice(j * chunk, (j + 1) * chunk)
-        loads[j].wait()
-        for b in range(seqs):
-            rows_ref[b * heads : (b + 1) * heads, part] = stage[b, :, part]
         block = rows_ref[:, part]
         left = (slot == lane + 8 * j).astype(F32).astype(BF16)
         right = (slot == lane + (8 * j + width)).astype(F32).astype(BF16)
@@ -400,6 +394,18 @@
 
     steps = area // (8 * HEAD_WIDTH)
     count = seqs * heads
+    small = [
+        tokens,
+        row(first_norm_gain),
+        row(decay_offset),
+        row(correction_offset),
+        row(correction_key_factor),
+        row(own_term_weight),
+        row(head_norm_gain),
+        routing.T,
+        routing_weight.T,
+        row(second_norm_gain),
+    ]
     partial, pick, table, tokens_near, gain_near, rows, packed, removed = pl.pallas_call(
         attention_kernel,
         out_shape=(
@@ -412,7 +418,7 @@
             near((count, 4 * HEAD_WIDTH), F32),
             near((count, 2 * HEAD_WIDTH), F32),
         ),
-        in_specs=[VMEM] * 10 + [HBM] * 6,
+        in_specs=[HBM] * 16,
         out_specs=[VMEM] * 8,
         scratch_shapes=[
             pltpu.VMEM((seqs, heads, area), F32),
@@ -420,22 +426,15 @@
             pltpu.VMEM(output_matrix.shape, BF16),
             pltpu.SemaphoreType.DMA((5,)),
             pltpu.SemaphoreType.DMA((steps,)),
+            pltpu.SemaphoreType.DMA((len(small),)),
+            *[pltpu.VMEM(x.shape, x.dtype) for x in small],
         ],
         compiler_params=pltpu.CompilerParams(vmem_limit_bytes=50 * MIB),
         name="attention",
     )(
         *far(
             [
-                tokens,
-                row(first_norm_gain),
-                row(decay_offset),
-                row(correction_offset),
-                row(correction_key_factor),
-                row(own_term_weight),
-                row(head_norm_gain),
-                routing.T,
-                routing_weight.T,
-                row(second_norm_gain),
+                *small,
                 recurrent_head_state,
                 receptance_matrix,
                 key_matrix,

time: 77.4 us -> 77.3 us (level)
  no operation moved by 1% of the time
where the time goes in v4:
time: 77.3 us; the launch traced here: 77.1 us
  starting transfers between devices  40.8 us (53%)
  waiting for transfers between devices  20.1 us (26%)
  Pallas kernels  15.4 us (20%)
  between operations  0.8 us (1%)
    ppermute x34, starting transfers between devices, exchange(): array = lax.ppermute(array, axis, [(i, i ^ k) for i in range(size)])  40.8 us
    ppermute x34, waiting for transfers between devices, exchange(): array = lax.ppermute(array, axis, [(i, i ^ k) for i in range(size)])  20.1 us
    pallas_call x1, Pallas kernels, local(): pl.pallas_call(attention_kernel, out_shape=(near((seqs, width), BF16), ne...  8.57 us
    pallas_call x1, Pallas kernels, local(): pl.pallas_call(functools.partial(expert_kernel, groups, min(256, units)),...  2.24 us
    pallas_call x1, Pallas kernels, local(): pl.pallas_call(update_kernel, out_shape=like(recurrent_head_state.shape,...  1.75 us
  transfers between devices with their start and end apart: 34, of which 10 were waited for; matrix products, arithmetic and copies ran while one was open for 0% of the time, Pallas kernels for 7%

profile of v4, /device:TPU:0, one launch (start us, length us, event | category | flops | bytes accessed | tf_op | source)
XLA Modules:
  0.0 77.1 jit_solution(1467211909856010257)
XLA Ops:
  0.6 8.6 %attention.1 = (bf16[32,2048]{1,0:T(8,128)(2,1)S(1)}, bf16[128,32]{1,0:T(8,128)(2,1)S(1)}, f32[32,128]{1,0:T(8,128)S(1)}, bf16[32,2048]{1,0:T(8,128)(2,1)S(1)}, ...) custom-call(bf16[32,2048]{1,0:T(8,128)(2,1)} %refs_0_.1, ...), custom_call_target="tpu_custom_call" | custom-call | tf_op jit(solution)/shard_map/attention/pallas_call | solution.py:409
  9.2 3.0 %collective-permute-start.2 = (bf16[32,2048]{1,0:T(8,128)(2,1)S(1)}, bf16[32,2048]{1,0:T(8,128)(2,1)S(1)}, u32[]{:S(2)}, u32[]{:S(2)}) collective-permute-start(bf16[32,2048]{1,0:T(8,128)(2,1)S(1)} %get-tuple-element.40.refs_0_), channel_id=1, source_target_pairs={{0,1},{1,0},{2,3},{3,2},{4,5},{5,4},{6,7},{7,6},{8,9},{9,8},{10,11... | collective-permute-start | bytes 393224 | tf_op jit(solution)/shard_map/ppermute | solution.py:353
  12.2 1.5 %collective-permute-start.1 = (bf16[32,2048]{1,0:T(8,128)(2,1)S(1)}, bf16[32,2048]{1,0:T(8,128)(2,1)S(1)}, u32[]{:S(2)}, u32[]{:S(2)}) collective-permute-start(bf16[32,2048]{1,0:T(8,128)(2,1)S(1)} %get-tuple-element.40.refs_0_), channel_id=1, source_target_pairs={{0,3},{1,2},{2,1},{3,0},{4,7},{5,6},{6,5},{7,4},{8,11},{9,10},{10,... | collective-permute-start | bytes 393224 | tf_op jit(solution)/shard_map/ppermute | solution.py:353
  13.8 2.3 %collective-permute-done.2.refs_3_ = bf16[32,2048]{1,0:T(8,128)(2,1)S(1)} collective-permute-done((bf16[32,2048]{1,0:T(8,128)(2,1)S(1)}, bf16[32,2048]{1,0:T(8,128)(2,1)S(1)}, u32[]{:S(2)}, u32[]{:S(2)}) %collective-permute-start.2) | collective-permute-done | bytes 131104 | tf_op jit(solution)/shard_map/ppermute | solution.py:353
  16.1 3.7 %collective-permute-done.1.refs_2_ = bf16[32,2048]{1,0:T(8,128)(2,1)S(1)} collective-permute-done((bf16[32,2048]{1,0:T(8,128)(2,1)S(1)}, bf16[32,2048]{1,0:T(8,128)(2,1)S(1)}, u32[]{:S(2)}, u32[]{:S(2)}) %collective-permute-start.1) | collective-permute-done | bytes 131104 | tf_op jit(solution)/shard_map/ppermute | solution.py:353
  19.9 1.4 %collective-permute-done.refs_1_ = bf16[32,2048]{1,0:T(8,128)(2,1)S(1)} collective-permute-done((bf16[32,2048]{1,0:T(8,128)(2,1)S(1)}, bf16[32,2048]{1,0:T(8,128)(2,1)S(1)}, u32[]{:S(2)}, u32[]{:S(2)}) %collective-permute-start) | collective-permute-done | bytes 131104 | tf_op jit(solution)/shard_map/ppermute | solution.py:353
  21.9 2.6 %collective-permute-start.3 = (bf16[16,2048]{1,0:T(8,128)(2,1)S(1)}, bf16[16,2048]{1,0:T(8,128)(2,1)S(1)}, u32[]{:S(2)}, u32[]{:S(2)}) collective-permute-start(bf16[16,2048]{1,0:T(8,128)(2,1)S(1)} %get-tuple-element.47), channel_id=1, source_target_pairs={{0,16},{4,20},{8,24},{12,28},{16,0},{20,4},{24,8},{28,12},{1,17},{... | collective-permute-start | bytes 196616 | tf_op jit(solution)/shard_map/ppermute | solution.py:353
  24.5 2.4 %collective-permute-start.5 = (bf16[16,2048]{1,0:T(8,128)(2,1)S(1)}, bf16[16,2048]{1,0:T(8,128)(2,1)S(1)}, u32[]{:S(2)}, u32[]{:S(2)}) collective-permute-start(bf16[16,2048]{1,0:T(8,128)(2,1)S(1)} %get-tuple-element.49), channel_id=1, source_target_pairs={{0,24},{4,28},{8,16},{12,20},{16,8},{20,12},{24,0},{28,4},{1,25},{... | collective-permute-start | bytes 196616 | tf_op jit(solution)/shard_map/ppermute | solution.py:353
  28.2 1.6 %collective-permute-start.8 = (bf16[16,2048]{1,0:T(8,128)(2,1)S(1)}, bf16[16,2048]{1,0:T(8,128)(2,1)S(1)}, u32[]{:S(2)}, u32[]{:S(2)}) collective-permute-start(bf16[16,2048]{1,0:T(8,128)(2,1)S(1)} %get-tuple-element.52), channel_id=1, source_target_pairs={{0,12},{4,8},{8,4},{12,0},{16,28},{20,24},{24,20},{28,16},{1,13},{... | collective-permute-start | bytes 196616 | tf_op jit(solution)/shard_map/ppermute | solution.py:353
  29.8 3.5 %collective-permute-done.4.refs_2_ = bf16[16,2048]{1,0:T(8,128)(2,1)S(1)} collective-permute-done((bf16[16,2048]{1,0:T(8,128)(2,1)S(1)}, bf16[16,2048]{1,0:T(8,128)(2,1)S(1)}, u32[]{:S(2)}, u32[]{:S(2)}) %collective-permute-start.4) | collective-permute-done | bytes 65568 | tf_op jit(solution)/shard_map/ppermute | solution.py:353
  33.9 2.7 %collective-permute-start.25 = (bf16[8,2048]{1,0:T(8,128)(2,1)S(1)}, bf16[8,2048]{1,0:T(8,128)(2,1)S(1)}, u32[]{:S(2)}, u32[]{:S(2)}) collective-permute-start(bf16[8,2048]{1,0:T(8,128)(2,1)S(1)} %get-tuple-element.66.refs_0_), channel_id=1, source_target_pairs={{0,12},{4,8},{8,4},{12,0},{16,28},{20,24},{24,20},{28,16},{1,13},{... | collective-permute-start | bytes 98312 | tf_op jit(solution)/shard_map/ppermute | solution.py:353
  37.1 2.2 %collective-permute-start.23 = (bf16[8,2048]{1,0:T(8,128)(2,1)S(1)}, bf16[8,2048]{1,0:T(8,128)(2,1)S(1)}, u32[]{:S(2)}, u32[]{:S(2)}) collective-permute-start(bf16[8,2048]{1,0:T(8,128)(2,1)S(1)} %get-tuple-element.66.refs_0_), channel_id=1, source_target_pairs={{0,28},{4,24},{8,20},{12,16},{16,12},{20,8},{24,4},{28,0},{1,29},{... | collective-permute-start | bytes 98312 | tf_op jit(solution)/shard_map/ppermute | solution.py:353
  39.3 2.2 %experts.1 = (bf16[16,2048]{1,0:T(8,128)(2,1)S(1)}, bf16[16,2048]{1,0:T(8,128)(2,1)S(1)}, bf16[16,2048]{1,0:T(8,128)(2,1)S(1)}, bf16[16,2048]{1,0:T(8,128)(2,1)S...) custom-call(bf16[16,2048]{1,0:T(8,128)(2,1)S(1)} %get-tuple-element., ...), custom_call_target="tpu_custom_call" | custom-call | tf_op jit(solution)/shard_map/experts/pallas_call | solution.py:475
  42.5 2.0 %collective-permute-start.11 = (bf16[16,2048]{1,0:T(8,128)(2,1)S(1)}, bf16[16,2048]{1,0:T(8,128)(2,1)S(1)}, u32[]{:S(2)}, u32[]{:S(2)}) collective-permute-start(bf16[16,2048]{1,0:T(8,128)(2,1)S(1)} %get-tuple-element.56), channel_id=1, source_target_pairs={{0,20},{4,16},{8,28},{12,24},{16,4},{20,0},{24,12},{28,8},{1,21},{... | collective-permute-start | bytes 196616 | tf_op jit(solution)/shard_map/ppermute | solution.py:353
  46.2 2.2 %collective-permute-start.20 = (bf16[8,2048]{1,0:T(8,128)(2,1)S(1)}, bf16[8,2048]{1,0:T(8,128)(2,1)S(1)}, u32[]{:S(2)}, u32[]{:S(2)}) collective-permute-start(bf16[8,2048]{1,0:T(8,128)(2,1)S(1)} %get-tuple-element.66.refs_0_), channel_id=1, source_target_pairs={{0,16},{4,20},{8,24},{12,28},{16,0},{20,4},{24,8},{28,12},{1,17},{... | collective-permute-start | bytes 98312 | tf_op jit(solution)/shard_map/ppermute | solution.py:353
  48.4 1.8 %collective-permute-done.22.refs_3_ = bf16[8,2048]{1,0:T(8,128)(2,1)S(1)} collective-permute-done((bf16[8,2048]{1,0:T(8,128)(2,1)S(1)}, bf16[8,2048]{1,0:T(8,128)(2,1)S(1)}, u32[]{:S(2)}, u32[]{:S(2)}) %collective-permute-start.22) | collective-permute-done | bytes 32800 | tf_op jit(solution)/shard_map/ppermute | solution.py:353
  50.2 1.4 %collective-permute-start.12 = (bf16[16,2048]{1,0:T(8,128)(2,1)S(1)}, bf16[16,2048]{1,0:T(8,128)(2,1)S(1)}, u32[]{:S(2)}, u32[]{:S(2)}) collective-permute-start(bf16[16,2048]{1,0:T(8,128)(2,1)S(1)} %get-tuple-element.57), channel_id=1, source_target_pairs={{0,24},{4,28},{8,16},{12,20},{16,8},{20,12},{24,0},{28,4},{1,25},{... | collective-permute-start | bytes 196616 | tf_op jit(solution)/shard_map/ppermute | solution.py:353
  51.6 3.6 %collective-permute-done.21.refs_2_ = bf16[8,2048]{1,0:T(8,128)(2,1)S(1)} collective-permute-done((bf16[8,2048]{1,0:T(8,128)(2,1)S(1)}, bf16[8,2048]{1,0:T(8,128)(2,1)S(1)}, u32[]{:S(2)}, u32[]{:S(2)}) %collective-permute-start.21) | collective-permute-done | bytes 32800 | tf_op jit(solution)/shard_map/ppermute | solution.py:353
  63.2 2.6 %collective-permute-start.29 = (bf16[8,2048]{1,0:T(8,128)(2,1)S(1)}, bf16[8,2048]{1,0:T(8,128)(2,1)S(1)}, u32[]{:S(2)}, u32[]{:S(2)}) collective-permute-start(bf16[8,2048]{1,0:T(8,128)(2,1)S(1)} %get-tuple-element.70), channel_id=1, source_target_pairs={{0,24},{4,28},{8,16},{12,20},{16,8},{20,12},{24,0},{28,4},{1,25},{... | collective-permute-start | bytes 98312 | tf_op jit(solution)/shard_map/ppermute | solution.py:353
  65.7 1.4 %collective-permute-start.30 = (bf16[8,2048]{1,0:T(8,128)(2,1)S(1)}, bf16[8,2048]{1,0:T(8,128)(2,1)S(1)}, u32[]{:S(2)}, u32[]{:S(2)}) collective-permute-start(bf16[8,2048]{1,0:T(8,128)(2,1)S(1)} %get-tuple-element.71), channel_id=1, source_target_pairs={{0,28},{4,24},{8,20},{12,16},{16,12},{20,8},{24,4},{28,0},{1,29},{... | collective-permute-start | bytes 98312 | tf_op jit(solution)/shard_map/ppermute | solution.py:353
  67.4 1.4 %collective-permute-start.32 = (bf16[8,2048]{1,0:T(8,128)(2,1)S(1)}, bf16[8,2048]{1,0:T(8,128)(2,1)S(1)}, u32[]{:S(2)}, u32[]{:S(2)}) collective-permute-start(bf16[8,2048]{1,0:T(8,128)(2,1)S(1)} %get-tuple-element.73), channel_id=1, source_target_pairs={{0,12},{4,8},{8,4},{12,0},{16,28},{20,24},{24,20},{28,16},{1,13},{... | collective-permute-start | bytes 98312 | tf_op jit(solution)/shard_map/ppermute | solution.py:353
  69.6 1.4 %collective-permute-done.30.refs_7_ = bf16[8,2048]{1,0:T(8,128)(2,1)S(1)} collective-permute-done((bf16[8,2048]{1,0:T(8,128)(2,1)S(1)}, bf16[8,2048]{1,0:T(8,128)(2,1)S(1)}, u32[]{:S(2)}, u32[]{:S(2)}) %collective-permute-start.30) | collective-permute-done | bytes 32800 | tf_op jit(solution)/shard_map/ppermute | solution.py:353
  71.0 1.6 %collective-permute-start.18 = (bf16[8,2048]{1,0:T(8,128)(2,1)S(1)}, bf16[8,2048]{1,0:T(8,128)(2,1)S(1)}, u32[]{:S(2)}, u32[]{:S(2)}) collective-permute-start(bf16[8,2048]{1,0:T(8,128)(2,1)S(1)} %get-tuple-element.64), channel_id=1, source_target_pairs={{0,3},{1,2},{2,1},{3,0},{4,7},{5,6},{6,5},{7,4},{8,11},{9,10},{10,... | collective-permute-start | bytes 98312 | tf_op jit(solution)/shard_map/ppermute | solution.py:353
  73.3 1.7 %update.1 = f32[32,4,4096]{2,1,0:T(4,128)} custom-call(f32[128,4096]{1,0:T(8,128)S(1)} %get-tuple-element.75.rows_ref, f32[128,256]{1,0:T(8,128)S(1)} %get-tuple-element.76.packed_ref, f32[128,128]{1,0:T(8,128)S(1)} %get-tuple-element.77.removed_ref), custom_call_target="tpu_custom_call" | custom-call | tf_op jit(solution)/shard_map/update/pallas_call | solution.py:448
  (65 shorter events, 17.5 us)
Async XLA Ops:
  9.2 6.9 %collective-permute-start.2 = (bf16[32,2048]{1,0:T(8,128)(2,1)S(1)}, bf16[32,2048]{1,0:T(8,128)(2,1)S(1)}, u32[]{:S(2)}, u32[]{:S(2)}) collective-permute-start(bf16[32,2048]{1,0:T(8,128)(2,1)S(1)} %get-tuple-element.40.refs_0_), channel_id=1, source_target_pairs={{0,1},{1,0},{2,3},{3,2},{4,5},{5,4},{6,7},{7,6},{8,9},{9,8},{10,11... | collective-permute-start | bytes 393224 | tf_op jit(solution)/shard_map/ppermute | solution.py:353
  12.2 7.6 %collective-permute-start.1 = (bf16[32,2048]{1,0:T(8,128)(2,1)S(1)}, bf16[32,2048]{1,0:T(8,128)(2,1)S(1)}, u32[]{:S(2)}, u32[]{:S(2)}) collective-permute-start(bf16[32,2048]{1,0:T(8,128)(2,1)S(1)} %get-tuple-element.40.refs_0_), channel_id=1, source_target_pairs={{0,3},{1,2},{2,1},{3,0},{4,7},{5,6},{6,5},{7,4},{8,11},{9,10},{10,... | collective-permute-start | bytes 393224 | tf_op jit(solution)/shard_map/ppermute | solution.py:353
  13.7 7.5 %collective-permute-start = (bf16[32,2048]{1,0:T(8,128)(2,1)S(1)}, bf16[32,2048]{1,0:T(8,128)(2,1)S(1)}, u32[]{:S(2)}, u32[]{:S(2)}) collective-permute-start(bf16[32,2048]{1,0:T(8,128)(2,1)S(1)} %get-tuple-element.40.refs_0_), channel_id=1, source_target_pairs={{0,2},{1,3},{2,0},{3,1},{4,6},{5,7},{6,4},{7,5},{8,10},{9,11},{10,... | collective-permute-start | bytes 393224 | tf_op jit(solution)/shard_map/ppermute | solution.py:353
  24.5 8.8 %collective-permute-start.4 = (bf16[16,2048]{1,0:T(8,128)(2,1)S(1)}, bf16[16,2048]{1,0:T(8,128)(2,1)S(1)}, u32[]{:S(2)}, u32[]{:S(2)}) collective-permute-start(bf16[16,2048]{1,0:T(8,128)(2,1)S(1)} %get-tuple-element.48), channel_id=1, source_target_pairs={{0,20},{4,16},{8,28},{12,24},{16,4},{20,0},{24,12},{28,8},{1,21},{... | collective-permute-start | bytes 196616 | tf_op jit(solution)/shard_map/ppermute | solution.py:353
  24.5 8.8 %collective-permute-start.5 = (bf16[16,2048]{1,0:T(8,128)(2,1)S(1)}, bf16[16,2048]{1,0:T(8,128)(2,1)S(1)}, u32[]{:S(2)}, u32[]{:S(2)}) collective-permute-start(bf16[16,2048]{1,0:T(8,128)(2,1)S(1)} %get-tuple-element.49), channel_id=1, source_target_pairs={{0,24},{4,28},{8,16},{12,20},{16,8},{20,12},{24,0},{28,4},{1,25},{... | collective-permute-start | bytes 196616 | tf_op jit(solution)/shard_map/ppermute | solution.py:353
  26.9 6.9 %collective-permute-start.6 = (bf16[16,2048]{1,0:T(8,128)(2,1)S(1)}, bf16[16,2048]{1,0:T(8,128)(2,1)S(1)}, u32[]{:S(2)}, u32[]{:S(2)}) collective-permute-start(bf16[16,2048]{1,0:T(8,128)(2,1)S(1)} %get-tuple-element.50), channel_id=1, source_target_pairs={{0,28},{4,24},{8,20},{12,16},{16,12},{20,8},{24,4},{28,0},{1,29},{... | collective-permute-start | bytes 196616 | tf_op jit(solution)/shard_map/ppermute | solution.py:353
  28.2 8.4 %collective-permute-start.7 = (bf16[16,2048]{1,0:T(8,128)(2,1)S(1)}, bf16[16,2048]{1,0:T(8,128)(2,1)S(1)}, u32[]{:S(2)}, u32[]{:S(2)}) collective-permute-start(bf16[16,2048]{1,0:T(8,128)(2,1)S(1)} %get-tuple-element.51), channel_id=1, source_target_pairs={{0,8},{4,12},{8,0},{12,4},{16,24},{20,28},{24,16},{28,20},{1,9},{5... | collective-permute-start | bytes 196616 | tf_op jit(solution)/shard_map/ppermute | solution.py:353
  28.2 8.9 %collective-permute-start.8 = (bf16[16,2048]{1,0:T(8,128)(2,1)S(1)}, bf16[16,2048]{1,0:T(8,128)(2,1)S(1)}, u32[]{:S(2)}, u32[]{:S(2)}) collective-permute-start(bf16[16,2048]{1,0:T(8,128)(2,1)S(1)} %get-tuple-element.52), channel_id=1, source_target_pairs={{0,12},{4,8},{8,4},{12,0},{16,28},{20,24},{24,20},{28,16},{1,13},{... | collective-permute-start | bytes 196616 | tf_op jit(solution)/shard_map/ppermute | solution.py:353
  33.3 9.1 %collective-permute-start.26 = (bf16[8,2048]{1,0:T(8,128)(2,1)S(1)}, bf16[8,2048]{1,0:T(8,128)(2,1)S(1)}, u32[]{:S(2)}, u32[]{:S(2)}) collective-permute-start(bf16[8,2048]{1,0:T(8,128)(2,1)S(1)} %get-tuple-element.66.refs_0_), channel_id=1, source_target_pairs={{0,4},{4,0},{8,12},{12,8},{16,20},{20,16},{24,28},{28,24},{1,5},{5... | collective-permute-start | bytes 98312 | tf_op jit(solution)/shard_map/ppermute | solution.py:353
  33.9 10.6 %collective-permute-start.25 = (bf16[8,2048]{1,0:T(8,128)(2,1)S(1)}, bf16[8,2048]{1,0:T(8,128)(2,1)S(1)}, u32[]{:S(2)}, u32[]{:S(2)}) collective-permute-start(bf16[8,2048]{1,0:T(8,128)(2,1)S(1)} %get-tuple-element.66.refs_0_), channel_id=1, source_target_pairs={{0,12},{4,8},{8,4},{12,0},{16,28},{20,24},{24,20},{28,16},{1,13},{... | collective-permute-start | bytes 98312 | tf_op jit(solution)/shard_map/ppermute | solution.py:353
  36.5 9.2 %collective-permute-start.24 = (bf16[8,2048]{1,0:T(8,128)(2,1)S(1)}, bf16[8,2048]{1,0:T(8,128)(2,1)S(1)}, u32[]{:S(2)}, u32[]{:S(2)}) collective-permute-start(bf16[8,2048]{1,0:T(8,128)(2,1)S(1)} %get-tuple-element.66.refs_0_), channel_id=1, source_target_pairs={{0,8},{4,12},{8,0},{12,4},{16,24},{20,28},{24,16},{28,20},{1,9},{5... | collective-permute-start | bytes 98312 | tf_op jit(solution)/shard_map/ppermute | solution.py:353
  37.1 9.1 %collective-permute-start.23 = (bf16[8,2048]{1,0:T(8,128)(2,1)S(1)}, bf16[8,2048]{1,0:T(8,128)(2,1)S(1)}, u32[]{:S(2)}, u32[]{:S(2)}) collective-permute-start(bf16[8,2048]{1,0:T(8,128)(2,1)S(1)} %get-tuple-element.66.refs_0_), channel_id=1, source_target_pairs={{0,28},{4,24},{8,20},{12,16},{16,12},{20,8},{24,4},{28,0},{1,29},{... | collective-permute-start | bytes 98312 | tf_op jit(solution)/shard_map/ppermute | solution.py:353
  41.6 15.8 %collective-permute-start.10 = (bf16[16,2048]{1,0:T(8,128)(2,1)S(1)}, bf16[16,2048]{1,0:T(8,128)(2,1)S(1)}, u32[]{:S(2)}, u32[]{:S(2)}) collective-permute-start(bf16[16,2048]{1,0:T(8,128)(2,1)S(1)} %get-tuple-element.55), channel_id=1, source_target_pairs={{0,16},{4,20},{8,24},{12,28},{16,0},{20,4},{24,8},{28,12},{1,17},{... | collective-permute-start | bytes 196616 | tf_op jit(solution)/shard_map/ppermute | solution.py:353
  42.5 15.7 %collective-permute-start.11 = (bf16[16,2048]{1,0:T(8,128)(2,1)S(1)}, bf16[16,2048]{1,0:T(8,128)(2,1)S(1)}, u32[]{:S(2)}, u32[]{:S(2)}) collective-permute-start(bf16[16,2048]{1,0:T(8,128)(2,1)S(1)} %get-tuple-element.56), channel_id=1, source_target_pairs={{0,20},{4,16},{8,28},{12,24},{16,4},{20,0},{24,12},{28,8},{1,21},{... | collective-permute-start | bytes 196616 | tf_op jit(solution)/shard_map/ppermute | solution.py:353
  45.7 9.5 %collective-permute-start.21 = (bf16[8,2048]{1,0:T(8,128)(2,1)S(1)}, bf16[8,2048]{1,0:T(8,128)(2,1)S(1)}, u32[]{:S(2)}, u32[]{:S(2)}) collective-permute-start(bf16[8,2048]{1,0:T(8,128)(2,1)S(1)} %get-tuple-element.66.refs_0_), channel_id=1, source_target_pairs={{0,20},{4,16},{8,28},{12,24},{16,4},{20,0},{24,12},{28,8},{1,21},{... | collective-permute-start | bytes 98312 | tf_op jit(solution)/shard_map/ppermute | solution.py:353
  46.2 11.2 %collective-permute-start.20 = (bf16[8,2048]{1,0:T(8,128)(2,1)S(1)}, bf16[8,2048]{1,0:T(8,128)(2,1)S(1)}, u32[]{:S(2)}, u32[]{:S(2)}) collective-permute-start(bf16[8,2048]{1,0:T(8,128)(2,1)S(1)} %get-tuple-element.66.refs_0_), channel_id=1, source_target_pairs={{0,16},{4,20},{8,24},{12,28},{16,0},{20,4},{24,8},{28,12},{1,17},{... | collective-permute-start | bytes 98312 | tf_op jit(solution)/shard_map/ppermute | solution.py:353
  50.2 10.6 %collective-permute-start.12 = (bf16[16,2048]{1,0:T(8,128)(2,1)S(1)}, bf16[16,2048]{1,0:T(8,128)(2,1)S(1)}, u32[]{:S(2)}, u32[]{:S(2)}) collective-permute-start(bf16[16,2048]{1,0:T(8,128)(2,1)S(1)} %get-tuple-element.57), channel_id=1, source_target_pairs={{0,24},{4,28},{8,16},{12,20},{16,8},{20,12},{24,0},{28,4},{1,25},{... | collective-permute-start | bytes 196616 | tf_op jit(solution)/shard_map/ppermute | solution.py:353
  55.2 6.9 %collective-permute-start.13 = (bf16[16,2048]{1,0:T(8,128)(2,1)S(1)}, bf16[16,2048]{1,0:T(8,128)(2,1)S(1)}, u32[]{:S(2)}, u32[]{:S(2)}) collective-permute-start(bf16[16,2048]{1,0:T(8,128)(2,1)S(1)} %get-tuple-element.58), channel_id=1, source_target_pairs={{0,28},{4,24},{8,20},{12,16},{16,12},{20,8},{24,4},{28,0},{1,29},{... | collective-permute-start | bytes 196616 | tf_op jit(solution)/shard_map/ppermute | solution.py:353
  57.3 8.4 %collective-permute-start.15 = (bf16[16,2048]{1,0:T(8,128)(2,1)S(1)}, bf16[16,2048]{1,0:T(8,128)(2,1)S(1)}, u32[]{:S(2)}, u32[]{:S(2)}) collective-permute-start(bf16[16,2048]{1,0:T(8,128)(2,1)S(1)} %get-tuple-element.60), channel_id=1, source_target_pairs={{0,12},{4,8},{8,4},{12,0},{16,28},{20,24},{24,20},{28,16},{1,13},{... | collective-permute-start | bytes 196616 | tf_op jit(solution)/shard_map/ppermute | solution.py:353
  58.2 8.9 %collective-permute-start.16 = (bf16[16,2048]{1,0:T(8,128)(2,1)S(1)}, bf16[16,2048]{1,0:T(8,128)(2,1)S(1)}, u32[]{:S(2)}, u32[]{:S(2)}) collective-permute-start(bf16[16,2048]{1,0:T(8,128)(2,1)S(1)} %get-tuple-element.61), channel_id=1, source_target_pairs={{0,4},{4,0},{8,12},{12,8},{16,20},{20,16},{24,28},{28,24},{1,5},{5... | collective-permute-start | bytes 196616 | tf_op jit(solution)/shard_map/ppermute | solution.py:353
  60.8 6.5 %collective-permute-start.27 = (bf16[8,2048]{1,0:T(8,128)(2,1)S(1)}, bf16[8,2048]{1,0:T(8,128)(2,1)S(1)}, u32[]{:S(2)}, u32[]{:S(2)}) collective-permute-start(bf16[8,2048]{1,0:T(8,128)(2,1)S(1)} %get-tuple-element.68), channel_id=1, source_target_pairs={{0,16},{4,20},{8,24},{12,28},{16,0},{20,4},{24,8},{28,12},{1,17},{... | collective-permute-start | bytes 98312 | tf_op jit(solution)/shard_map/ppermute | solution.py:353
  62.0 6.8 %collective-permute-start.28 = (bf16[8,2048]{1,0:T(8,128)(2,1)S(1)}, bf16[8,2048]{1,0:T(8,128)(2,1)S(1)}, u32[]{:S(2)}, u32[]{:S(2)}) collective-permute-start(bf16[8,2048]{1,0:T(8,128)(2,1)S(1)} %get-tuple-element.69), channel_id=1, source_target_pairs={{0,20},{4,16},{8,28},{12,24},{16,4},{20,0},{24,12},{28,8},{1,21},{... | collective-permute-start | bytes 98312 | tf_op jit(solution)/shard_map/ppermute | solution.py:353
  63.2 6.4 %collective-permute-start.29 = (bf16[8,2048]{1,0:T(8,128)(2,1)S(1)}, bf16[8,2048]{1,0:T(8,128)(2,1)S(1)}, u32[]{:S(2)}, u32[]{:S(2)}) collective-permute-start(bf16[8,2048]{1,0:T(8,128)(2,1)S(1)} %get-tuple-element.70), channel_id=1, source_target_pairs={{0,24},{4,28},{8,16},{12,20},{16,8},{20,12},{24,0},{28,4},{1,25},{... | collective-permute-start | bytes 98312 | tf_op jit(solution)/shard_map/ppermute | solution.py:353
  67.4 7.7 %collective-permute-start.32 = (bf16[8,2048]{1,0:T(8,128)(2,1)S(1)}, bf16[8,2048]{1,0:T(8,128)(2,1)S(1)}, u32[]{:S(2)}, u32[]{:S(2)}) collective-permute-start(bf16[8,2048]{1,0:T(8,128)(2,1)S(1)} %get-tuple-element.73), channel_id=1, source_target_pairs={{0,12},{4,8},{8,4},{12,0},{16,28},{20,24},{24,20},{28,16},{1,13},{... | collective-permute-start | bytes 98312 | tf_op jit(solution)/shard_map/ppermute | solution.py:353
  (17 other events, 172.9 us)
